TPU v7x, 32 devices: a whole 2x2x4 slice. The times are simulated.
32 devices in a mesh: ep: 4 (over y, x), tp: 8 (over z, core).
Axes of the slice: x: 2, y: 2, z: 4, core: 2. Of those that a mesh axis runs over, the one named last changes fastest.
Arguments:
- queries: bfloat16 [4096, 1024], P('ep', 'tp'), may hold values from -12 to 12
- keys: bfloat16 [4096, 1024], P('ep', 'tp'), may hold values from -12 to 12
- values: bfloat16 [4096, 2048], P('ep', 'tp'), may hold values from -6 to 6
- out_gate: bfloat16 [4096, 2048], P('ep', 'tp'), may hold values from -6 to 6
- in_gate: float32 [16, 4096], P('tp', 'ep'), may hold values from -8 to 100
- forget_gate: float32 [16, 4096], P('tp', 'ep'), may hold values from 0 to 16
- out_gain: float32 [2048], P('tp'), may hold values from 0.1 to 1.9
- out_weight: bfloat16 [2048, 4096], P('tp'), may hold values from -0.1875 to 0.1875
- moe_rows: bfloat16 [512, 4096], P('ep'), may hold values from -36 to 36
- moe_gain: float32 [4096], replicated, may hold values from 0.1 to 1.9
- routes: int32 [512, 2], P('ep'), may hold values from 0 to 3, all different within a row; in each aligned block of 128 rows (0 to 127, 128 to 255, ...) at most 96 rows name the same one
- route_weight: float32 [512, 2], P('ep'), may hold values from 0.2 to 1.2
- expert_gate: bfloat16 [4, 4096, 4096], P('ep', None, 'tp'), may hold values from -0.09375 to 0.09375
- expert_up: bfloat16 [4, 4096, 4096], P('ep', None, 'tp'), may hold values from -0.09375 to 0.09375
- expert_down: bfloat16 [4, 4096, 4096], P('ep', 'tp'), may hold values from -0.125 to 0.125
- shared_gate: bfloat16 [4096, 2048], P(None, 'tp'), may hold values from -0.09375 to 0.09375
- shared_up: bfloat16 [4096, 2048], P(None, 'tp'), may hold values from -0.09375 to 0.09375
- shared_down: bfloat16 [2048, 4096], P('tp'), may hold values from -0.1875 to 0.1875
Outputs:
- mixer_out: bfloat16 [4096, 4096], P('ep', 'tp')
- moe_out: bfloat16 [512, 4096], P('ep', 'tp')
Inputs may be any that keep to these rules, and one draw needn't show every extreme that they name: `routes`: each row names 2 different experts. Within the 128 rows of one index of ep no expert is named more than 96 times, a bound that some block reaches.
All inputs are finite; a program needn't handle non-finite values.
Results may differ from a plain program's by a relative error of at most 0.019.
Values may be sent and summed in bfloat16 or wider, within the bound.
No kernel may reach another device: no remote copies, remote signals or barrier semaphores. Data moves between devices by JAX's collectives and lax.ppermute only.
A program may use at most 128 MiB of HBM per device.

v0:
```python
import functools

import jax
import jax.numpy as jnp
from jax import lax
from jax.experimental import pallas as pl
from jax.experimental.pallas import tpu as pltpu
from jax.sharding import PartitionSpec as P


DK = 64
DV = 128
LANES = 128
SUB = 8
NEG = -1e30
EPS = 1e-06

F32 = jnp.float32
BF16 = jnp.bfloat16


def params(limit_mib=56, semantics=None):
    return pltpu.CompilerParams(vmem_limit_bytes=limit_mib << 20, dimension_semantics=semantics)


def cost(flops, nbytes, trans=0):
    return pl.CostEstimate(flops=int(flops), bytes_accessed=int(nbytes), transcendentals=int(trans))


def xor_pairs(n, k):
    return [(i, i ^ k) for i in range(n)]


def swap(x, axis, k):
    return lax.ppermute(x, axis, xor_pairs(lax.axis_size(axis), k))


def dot(a, b):
    return jnp.dot(a, b, preferred_element_type=F32)


def dot_nt(a, b):
    return lax.dot_general(a, b, (((1,), (1,)), ((), ())), preferred_element_type=F32)


def two_parts(x):
    high = x.astype(BF16)
    return high, (x - high.astype(F32)).astype(BF16)


def with_deps(kernel, n_deps, lead):
    def body(*refs):
        return kernel(*refs[:lead], *refs[lead + n_deps :])

    return body


def anywhere(deps):
    return [pl.BlockSpec(memory_space=pl.ANY) for _ in deps]


def prep_kernel(idx, rows, gain, routes, normed, dest, *outgoing):
    n_rows, width = rows.shape
    half = width // 2
    n_out = len(outgoing)
    cap = outgoing[0].shape[0]
    topk = routes.shape[0]
    me, core = idx[0], idx[1]
    step = 16
    for first in range(0, n_rows, step):
        wide = rows[first : first + step, :].astype(F32)
        inverse = lax.rsqrt(jnp.mean(wide * wide, axis=1, keepdims=True) + EPS)
        normed[first : first + step, :] = (wide * inverse * gain[...]).astype(BF16)
    n_tgt = max(SUB, n_out)
    target = lax.broadcasted_iota(jnp.int32, (n_tgt, n_rows), 0) ^ me
    named = [routes[k : k + 1, :] == target for k in range(topk)]
    member = functools.reduce(jnp.logical_or, named)
    earlier = lax.broadcasted_iota(jnp.int32, (n_rows, n_rows), 0) < lax.broadcasted_iota(
        jnp.int32, (n_rows, n_rows), 1
    )
    place = dot(member.astype(F32).astype(BF16), earlier.astype(F32).astype(BF16)).astype(jnp.int32)
    slot = lax.broadcasted_iota(jnp.int32, (n_tgt, n_rows), 0) * cap + place
    dest[...] = jnp.zeros(dest.shape, jnp.int32)
    for k in range(topk):
        dest[k : k + 1, :] = jnp.sum(jnp.where(named[k], slot, 0), axis=0, keepdims=True)
    mine = normed[:, pl.ds(pl.multiple_of(core * half, LANES), half)]
    spot = lax.broadcasted_iota(jnp.int32, (cap, n_rows), 0)
    member_i = jnp.where(member, place, -1)
    for j in range(n_out):
        pick = (member_i[j : j + 1, :] == spot).astype(F32).astype(BF16)
        outgoing[j][...] = dot(pick, mine).astype(BF16)


def prep(idx, rows, gain, routes, n_ep, cap, deps=()):
    n_rows, width = rows.shape
    shapes = [
        jax.ShapeDtypeStruct((n_rows, width), BF16),
        jax.ShapeDtypeStruct((SUB, n_rows), jnp.int32),
    ] + [jax.ShapeDtypeStruct((cap, width // 2), BF16) for _ in range(n_ep)]
    vm = pl.BlockSpec(memory_space=pltpu.VMEM)
    out = pl.pallas_call(
        with_deps(prep_kernel, len(deps), 1),
        out_shape=shapes,
        in_specs=[pl.BlockSpec(memory_space=pltpu.SMEM), *anywhere(deps), vm, vm, vm],
        out_specs=[vm] * len(shapes),
        compiler_params=params(),
        cost_estimate=cost(2 * n_ep * cap * n_rows * width // 2, 4 * n_rows * width),
        name="prep",
    )(idx, *deps, rows, gain, routes)
    return out[0], out[1], list(out[2:])


def ffn_kernel(idx, *refs, n_lhs, per_half, split):
    lhs, rest = refs[:n_lhs], refs[n_lhs:]
    gate, up, down, send, own, acc_g, acc_u, hidden = rest
    step = pl.program_id(0)
    n_k = 2 * per_half
    core = idx[0]

    def piece(group):
        return jnp.concatenate([r[...] for r in group], axis=0) if len(group) > 1 else group[0][...]

    def add(x):
        g = dot(x, gate[...].reshape(gate.shape[-2:]))
        u = dot(x, up[...].reshape(up.shape[-2:]))

        @pl.when(step == 0)
        def _():
            acc_g[...] = g
            acc_u[...] = u

        @pl.when(step > 0)
        def _():
            acc_g[...] += g
            acc_u[...] += u

    if split:
        n_own = n_lhs // 2

        @pl.when(step < per_half)
        def _():
            add(piece(lhs[:n_own]))

        @pl.when((step >= per_half) & (step < n_k))
        def _():
            add(piece(lhs[n_own:]))

    else:

        @pl.when(step < n_k)
        def _():
            add(piece(lhs))

    @pl.when(step == n_k - 1)
    def _():
        g = acc_g[...]
        hidden[...] = (g * jax.nn.sigmoid(g) * acc_u[...]).astype(BF16)

    @pl.when(step >= n_k)
    def _():
        y = dot(hidden[...], down[...].reshape(down.shape[-2:])).astype(BF16)
        wide = y.shape[1] // 2
        low, high = y[:, :wide], y[:, wide:]

        @pl.when(core == 0)
        def _():
            own[...] = low
            send[...] = high

        @pl.when(core != 0)
        def _():
            own[...] = high
            send[...] = low


def ffn(idx, lhs, gate, up, down, n_z, split, deps=()):
    rows = sum(a.shape[0] for a in lhs) // (2 if split else 1)
    width, hid = gate.shape[-2:]
    chunk = 512 if split else 1024
    half = width // 2
    per_half = half // chunk
    n_k = 2 * per_half
    pair = width // n_z
    lead = gate.ndim - 2

    def k_at(j, idx):
        j = jnp.minimum(j, n_k - 1)
        if not split:
            return j
        return jnp.bitwise_xor(j // per_half, idx[0]) * per_half + j % per_half

    zeros = (0,) * lead
    ones = (1,) * lead
    if split:
        n_own = len(lhs) // 2
        lhs_specs = [
            pl.BlockSpec((a.shape[0], chunk), lambda j, idx: (0, jnp.minimum(j, per_half - 1)))
            for a in lhs[:n_own]
        ] + [
            pl.BlockSpec((a.shape[0], chunk), lambda j, idx: (0, jnp.clip(j - per_half, 0, per_half - 1)))
            for a in lhs[n_own:]
        ]
    else:
        lhs_specs = [
            pl.BlockSpec((a.shape[0], chunk), lambda j, idx: (0, jnp.minimum(j, n_k - 1))) for a in lhs
        ]
    w_in = pl.BlockSpec(ones + (chunk, hid), lambda j, idx: zeros + (k_at(j, idx), 0))
    w_out = pl.BlockSpec(ones + (hid, pair), lambda j, idx: zeros + (0, jnp.maximum(j - n_k, 0)))
    o_spec = pl.BlockSpec((rows, pair // 2), lambda j, idx: (0, jnp.maximum(j - n_k, 0)))
    shape = jax.ShapeDtypeStruct((rows, half), BF16)
    return pl.pallas_call(
        with_deps(
            functools.partial(ffn_kernel, n_lhs=len(lhs), per_half=per_half, split=split), len(deps), 1
        ),
        out_shape=[shape, shape],
        grid_spec=pltpu.PrefetchScalarGridSpec(
            num_scalar_prefetch=1,
            grid=(n_k + n_z,),
            in_specs=anywhere(deps) + lhs_specs + [w_in, w_in, w_out],
            out_specs=[o_spec, o_spec],
            scratch_shapes=[
                pltpu.VMEM((rows, hid), F32),
                pltpu.VMEM((rows, hid), F32),
                pltpu.VMEM((rows, hid), BF16),
            ],
        ),
        compiler_params=params(semantics=("arbitrary",)),
        cost_estimate=cost(6 * rows * width * hid, 6 * width * hid + 4 * rows * width),
    )(idx, *deps, *lhs, gate, up, down)


def combine_kernel(idx, *refs, n_ep, topk):
    blocks, rest = refs[:n_ep], refs[n_ep:]
    shared_own, shared_other, dest, weight, out = rest
    cap = blocks[0].shape[0]
    n_rows = out.shape[1]
    back = jnp.concatenate([b[...] for b in blocks], axis=0)
    spot = lax.broadcasted_iota(jnp.int32, (n_rows, n_ep * cap), 1)
    total = shared_own[...].astype(F32) + shared_other[...].astype(F32)
    for k in range(topk):
        pick = (dest[:, k : k + 1] == spot).astype(F32).astype(BF16)
        total = total + weight[:, k : k + 1] * dot(pick, back)
    out[...] = total.astype(BF16).reshape(out.shape)


def combine(idx, blocks, shared_own, shared_other, dest, weight, n_z, deps=()):
    n_rows, half = shared_own.shape
    cap = blocks[0].shape[0]
    fw = half // n_z
    topk = weight.shape[1]
    col = lambda k, idx: (0, jnp.bitwise_xor(k, idx[0]))
    keep = lambda k, idx: (0, 0)
    return pl.pallas_call(
        with_deps(functools.partial(combine_kernel, n_ep=len(blocks), topk=topk), len(deps), 1),
        out_shape=jax.ShapeDtypeStruct((n_z, n_rows, fw), BF16),
        grid_spec=pltpu.PrefetchScalarGridSpec(
            num_scalar_prefetch=1,
            grid=(n_z,),
            in_specs=anywhere(deps)
            + [pl.BlockSpec((cap, fw), col) for _ in blocks]
            + [
                pl.BlockSpec((n_rows, fw), col),
                pl.BlockSpec((n_rows, fw), col),
                pl.BlockSpec(dest.shape, keep),
                pl.BlockSpec(weight.shape, keep),
            ],
            out_specs=pl.BlockSpec((1, n_rows, fw), lambda k, idx: (k, 0, 0)),
        ),
        compiler_params=params(semantics=("arbitrary",)),
        cost_estimate=cost(2 * topk * n_rows * len(blocks) * cap * half, 4 * n_rows * half),
        name="combine",
    )(idx, *deps, *blocks, shared_own, shared_other, dest, weight)


def gate_rows(in_gate, forget_gate):
    heads, length = in_gate.shape
    head_of = lax.broadcasted_iota(jnp.int32, (SUB, length), 0) * heads // SUB
    gate = jnp.broadcast_to(in_gate[0:1, :], (SUB, length))
    forget = jnp.broadcast_to(forget_gate[0:1, :], (SUB, length))
    for h in range(1, heads):
        gate = jnp.where(head_of >= h, in_gate[h : h + 1, :], gate)
        forget = jnp.where(head_of >= h, forget_gate[h : h + 1, :], forget)
    lane = lax.broadcasted_iota(jnp.int32, (SUB, length), 1)
    cum = jnp.minimum(forget, 0.0) - jnp.log1p(jnp.exp(-jnp.abs(forget)))
    shift = 1
    while shift < length:
        cum = cum + jnp.where(lane >= shift, pltpu.roll(cum, shift, 1), 0.0)
        shift *= 2
    return gate - cum, cum, lane


def state_kernel(keys, values, in_gate, forget_gate, pack):
    heads, length = in_gate.shape
    rise, cum, _ = gate_rows(in_gate[...], forget_gate[...])
    last = cum[:, length - 1 : length]
    top = jnp.max(rise, axis=1, keepdims=True)
    weight = jnp.exp(rise - top)
    key_t = jnp.transpose(keys[...].astype(F32))
    lane = lax.broadcasted_iota(jnp.int32, (1, LANES), 1)
    pack[...] = jnp.zeros(pack.shape, F32)
    columns = []
    decay_row = jnp.zeros((1, LANES), F32)
    stab_row = jnp.zeros((1, LANES), F32)
    for h in range(heads):
        r = h * SUB // heads
        scaled = key_t[h * DK : (h + 1) * DK, :] * weight[r : r + 1, :]
        high, low = two_parts(scaled)
        v = values[:, h * DV : (h + 1) * DV]
        pack[h * DK : (h + 1) * DK, :] = dot(high, v) + dot(low, v)
        columns.append(jnp.sum(scaled, axis=1, keepdims=True))
        here = lane // DK == h
        decay_row = jnp.where(here, last[r : r + 1, :], decay_row)
        stab_row = jnp.where(here, last[r : r + 1, :] + top[r : r + 1, :], stab_row)
    if heads * DK < LANES:
        columns.append(jnp.zeros((LANES - heads * DK, 1), F32))
    column = jnp.concatenate(columns, axis=0)
    normal = jnp.transpose(jnp.broadcast_to(column, (LANES, LANES)))
    base = heads * DK
    pack[base : base + 1, :] = normal[0:1, :]
    pack[base + 1 : base + 2, :] = decay_row
    pack[base + 2 : base + 3, :] = stab_row


def cell_state(keys, values, in_gate, forget_gate, deps=()):
    heads, length = in_gate.shape
    vm = pl.BlockSpec(memory_space=pltpu.VMEM)
    return pl.pallas_call(
        with_deps(state_kernel, len(deps), 0),
        in_specs=anywhere(deps) + [vm] * 4,
        out_shape=jax.ShapeDtypeStruct((heads * DK + SUB, DV), F32),
        compiler_params=params(),
        cost_estimate=cost(4 * heads * length * DK * DV, 4 * keys.size + 2 * values.size),
        name="cell_state",
    )(*deps, keys, values, in_gate, forget_gate)


def intra_kernel(queries, keys, values, in_gate, forget_gate, inner, stats, *, block):
    heads, length = in_gate.shape
    rise, cum, lane = gate_rows(in_gate[...], forget_gate[...])
    peak = rise
    shift = 1
    while shift < length:
        peak = jnp.maximum(peak, jnp.where(lane >= shift, pltpu.roll(peak, shift, 1), NEG))
        shift *= 2
    peak_col = jnp.transpose(peak)
    cum_col = jnp.transpose(cum)
    scale = DK ** (-0.5)
    place = lax.broadcasted_iota(jnp.int32, (block, LANES), 1)
    for first in range(0, length, block):
        seen = first + block
        row = lax.broadcasted_iota(jnp.int32, (block, seen), 0) + first
        col = lax.broadcasted_iota(jnp.int32, (block, seen), 1)
        causal = col <= row
        kept = jnp.zeros((block, LANES), F32)
        for h in range(heads):
            r = h * SUB // heads
            q = queries[first:seen, h * DK : (h + 1) * DK]
            k = keys[0:seen, h * DK : (h + 1) * DK]
            v = values[0:seen, h * DV : (h + 1) * DV]
            mu = peak_col[first:seen, r : r + 1]
            decay = jnp.exp(jnp.where(causal, rise[r : r + 1, 0:seen] - mu, NEG))
            scores = dot_nt(q, k) * scale * decay
            inner[first:seen, h * DV : (h + 1) * DV] = dot(scores.astype(BF16), v)
            total = jnp.sum(scores, axis=1, keepdims=True)
            kept = jnp.where(place == 3 * h, total, kept)
            kept = jnp.where(place == 3 * h + 1, mu, kept)
            kept = jnp.where(place == 3 * h + 2, cum_col[first:seen, r : r + 1], kept)
        stats[first:seen, :] = kept


def cell_intra(queries, keys, values, in_gate, forget_gate, deps=()):
    heads, length = in_gate.shape
    vm = pl.BlockSpec(memory_space=pltpu.VMEM)
    return pl.pallas_call(
        with_deps(functools.partial(intra_kernel, block=256), len(deps), 0),
        in_specs=anywhere(deps) + [vm] * 5,
        out_shape=[
            jax.ShapeDtypeStruct((length, heads * DV), F32),
            jax.ShapeDtypeStruct((length, LANES), F32),
        ],
        compiler_params=params(),
        cost_estimate=cost(heads * length * length * (DK + DV), 8 * values.size, heads * length * length),
        name="cell_intra",
    )(*deps, queries, keys, values, in_gate, forget_gate)


def finish_kernel(idx, *refs, n_packs, heads):
    packs, rest = refs[:n_packs], refs[n_packs:]
    queries, out_gate, gain, inner, stats, mixed, high, low, small = rest
    me = idx[0]
    base = heads * DK

    @pl.when(pl.program_id(0) == 0)
    def _():
        before = [jnp.bitwise_xor(me, k + 1) for k in range(n_packs)]
        decay = [p[base + 1 : base + 2, :] for p in packs]
        after = []
        anchor = jnp.zeros((1, LANES), F32)
        for k in range(n_packs):
            gone = jnp.zeros((1, LANES), F32)
            for other in range(n_packs):
                between = (before[other] > before[k]) & (before[other] < me)
                gone = gone + jnp.where(between, decay[other], 0.0)
            after.append(gone)
            anchor = anchor + jnp.where(before[k] < me, decay[k], 0.0)
        levels = [packs[k][base + 2 : base + 3, :] + after[k] for k in range(n_packs)]
        stab = anchor
        for k in range(n_packs):
            stab = jnp.maximum(stab, jnp.where(before[k] < me, levels[k], NEG))
        weights = [
            jnp.where(before[k] < me, jnp.exp(jnp.minimum(levels[k] - stab, 0.0)), 0.0)
            for k in range(n_packs)
        ]
        normal = jnp.zeros((1, LANES), F32)
        for k in range(n_packs):
            normal = normal + weights[k] * packs[k][base : base + 1, :]
        for h in range(heads):
            matrix = jnp.zeros((DK, DV), F32)
            for k in range(n_packs):
                matrix = matrix + weights[k][:, h * DK : h * DK + 1] * packs[k][h * DK : (h + 1) * DK, :]
            a, b = two_parts(matrix)
            high[h * DK : (h + 1) * DK, :] = a
            low[h * DK : (h + 1) * DK, :] = b
        small[0:1, :] = normal
        small[1:2, :] = stab

    scale = DK ** (-0.5)
    for h in range(heads):
        cols = slice(h * DV, (h + 1) * DV)
        ks = slice(h * DK, (h + 1) * DK)
        q = queries[:, ks]
        across = (dot(q, high[ks, :]) + dot(q, low[ks, :])) * scale
        normal_dot = jnp.sum(q.astype(F32) * small[0:1, ks], axis=1, keepdims=True) * scale
        stab_in = small[1:2, h * DK : h * DK + 1]
        total = stats[:, 3 * h : 3 * h + 1]
        local_mu = stats[:, 3 * h + 1 : 3 * h + 2]
        cum = stats[:, 3 * h + 2 : 3 * h + 3]
        mu = jnp.maximum(local_mu, stab_in)
        here = jnp.exp(local_mu - mu)
        there = jnp.exp(stab_in - mu)
        signed = total * here + there * normal_dot
        divisor = jnp.maximum(jnp.abs(signed), jnp.exp(-(cum + mu)))
        cells = (inner[:, cols] * here + there * across) / divisor
        gated = cells * jax.nn.sigmoid(out_gate[:, cols].astype(F32)) * gain[:, cols]
        mixed[:, cols] = gated.astype(BF16)


def cell_finish(idx, packs, queries, out_gate, gain, inner, stats, heads, deps=()):
    length, width = out_gate.shape
    block = 256
    row = lambda i, idx: (i, 0)
    keep = lambda i, idx: (0, 0)
    return pl.pallas_call(
        with_deps(functools.partial(finish_kernel, n_packs=len(packs), heads=heads), len(deps), 1),
        out_shape=jax.ShapeDtypeStruct((length, width), BF16),
        grid_spec=pltpu.PrefetchScalarGridSpec(
            num_scalar_prefetch=1,
            grid=(length // block,),
            in_specs=anywhere(deps)
            + [pl.BlockSpec(p.shape, keep) for p in packs]
            + [
                pl.BlockSpec((block, queries.shape[1]), row),
                pl.BlockSpec((block, width), row),
                pl.BlockSpec(gain.shape, keep),
                pl.BlockSpec((block, width), row),
                pl.BlockSpec((block, LANES), row),
            ],
            out_specs=pl.BlockSpec((block, width), row),
            scratch_shapes=[
                pltpu.VMEM((heads * DK, DV), BF16),
                pltpu.VMEM((heads * DK, DV), BF16),
                pltpu.VMEM((SUB, LANES), F32),
            ],
        ),
        compiler_params=params(semantics=("arbitrary",)),
        cost_estimate=cost(4 * heads * length * DK * DV, 12 * length * width, length * width),
        name="cell_finish",
    )(idx, *deps, *packs, queries, out_gate, gain, inner, stats)


def project_kernel(idx, *refs, n_tp):
    mixed, weight, out, joined = refs[:n_tp], refs[n_tp], refs[n_tp + 1], refs[n_tp + 2]
    me = idx[0]
    n_ep, _, part, _ = weight.shape
    own = n_ep * part

    @pl.when(pl.program_id(0) == 0)
    def _():
        for j in range(n_tp):
            source = jnp.bitwise_xor(me, j)
            for e in range(n_ep):
                first = j * own + e * part
                joined[first : first + part, :] = weight[e, source]

    lhs = jnp.concatenate([m[...] for m in mixed], axis=1)
    out[...] = dot(lhs, joined[...]).astype(BF16)


def project(idx, mixed, weight, deps=()):
    length, own = mixed[0].shape
    n_tp = len(mixed)
    cols = weight.shape[-1]
    block = 256
    return pl.pallas_call(
        with_deps(functools.partial(project_kernel, n_tp=n_tp), len(deps), 1),
        out_shape=jax.ShapeDtypeStruct((length, cols), BF16),
        grid_spec=pltpu.PrefetchScalarGridSpec(
            num_scalar_prefetch=1,
            grid=(length // block,),
            in_specs=anywhere(deps)
            + [pl.BlockSpec((block, own), lambda i, idx: (i, 0)) for _ in mixed]
            + [pl.BlockSpec(weight.shape, lambda i, idx: (0, 0, 0, 0))],
            out_specs=pl.BlockSpec((block, cols), lambda i, idx: (i, 0)),
            scratch_shapes=[pltpu.VMEM((n_tp * own, cols), BF16)],
        ),
        compiler_params=params(semantics=("arbitrary",)),
        cost_estimate=cost(2 * length * n_tp * own * cols, 2 * length * n_tp * own),
        name="project",
    )(idx, *deps, *mixed, weight)


def local(
    queries,
    keys,
    values,
    out_gate,
    in_gate,
    forget_gate,
    out_gain,
    out_weight,
    moe_rows,
    moe_gain,
    routes,
    route_weight,
    expert_gate,
    expert_up,
    expert_down,
    shared_gate,
    shared_up,
    shared_down,
):
    n_tp, n_ep = lax.axis_size("tp"), lax.axis_size("ep")
    n_z = n_tp // 2
    me_tp, me_ep = lax.axis_index("tp"), lax.axis_index("ep")
    me_z, core = me_tp // 2, me_tp % 2
    heads = in_gate.shape[0]
    routed_rows, _ = moe_rows.shape
    topk = routes.shape[1]
    exact = 3 * routed_rows * topk // (2 * n_ep)
    cap = -(-exact // 16) * 16

    idx = jnp.stack([me_ep, core]).astype(jnp.int32)
    core_idx = core.reshape(1).astype(jnp.int32)
    z_idx = me_z.reshape(1).astype(jnp.int32)
    tp_idx = me_tp.reshape(1).astype(jnp.int32)
    ep_idx = me_ep.reshape(1).astype(jnp.int32)

    normed, dest, outgoing = prep(
        idx, moe_rows, moe_gain.reshape(1, -1), routes.astype(jnp.int32).T, n_ep, cap
    )
    arrived = [outgoing[0]]
    for k in range(1, n_ep):
        arrived.append(swap(outgoing[k], "ep", k))

    own_rows, cols = out_weight.shape
    part = own_rows // n_ep
    share, _ = lax.optimization_barrier((out_weight, dest))
    share = lax.dynamic_slice_in_dim(share, me_ep * part, part, 0)
    share = share.reshape(part, n_tp, cols // n_tp).transpose(1, 0, 2)
    share = lax.all_to_all(share, "tp", 0, 0, tiled=True)

    pack = cell_state(keys, values, in_gate, forget_gate, [dest])
    packs = []
    for k in range(1, n_ep):
        packs.append(swap(pack, "ep", k))
    inner, stats = cell_intra(queries, keys, values, in_gate, forget_gate, [pack])
    mixed = cell_finish(
        ep_idx, packs, queries, out_gate, out_gain.reshape(1, -1), inner, stats, heads
    )
    gathered = [mixed]
    for k in range(1, n_z):
        gathered.append(swap(mixed, "tp", 2 * k))
    pieces = []
    for g in gathered:
        pieces += [g, swap(g, "tp", 1)]
    share, mixed_dep = lax.optimization_barrier((share, mixed))
    everyone = jnp.broadcast_to(share[None], (n_ep,) + share.shape)
    columns = lax.all_to_all(everyone, "ep", 0, 0, tiled=True)

    others = []
    for a in arrived:
        others.append(swap(a, "tp", 1))
    send, own = ffn(
        core_idx, arrived + others, expert_gate, expert_up, expert_down, n_z, True, [mixed_dep]
    )
    got = swap(send, "tp", 1)
    back = []
    for k in range(n_ep):
        rows = slice(k * cap, (k + 1) * cap)
        pair = (own[rows].astype(F32) + got[rows].astype(F32)).astype(BF16)
        back.append(swap(pair, "ep", k) if k else pair)
    shared_send, shared_own = ffn(
        core_idx, [normed], shared_gate, shared_up, shared_down, n_z, False, [back[0]]
    )
    shared_other = swap(shared_send, "tp", 1)
    part_out = combine(z_idx, back, shared_own, shared_other, dest.T, route_weight, n_z)
    total = part_out[0].astype(F32)
    for k in range(1, n_z):
        total = total + swap(part_out[k], "tp", 2 * k).astype(F32)
    moe_out = total.astype(BF16)
    mixer_out = project(tp_idx, pieces, columns, [part_out])
    return (mixer_out, moe_out)


def solution(mesh):
    return jax.shard_map(
        local,
        mesh=mesh,
        in_specs=(
            P("ep", "tp"),
            P("ep", "tp"),
            P("ep", "tp"),
            P("ep", "tp"),
            P("tp", "ep"),
            P("tp", "ep"),
            P("tp"),
            P("tp", None),
            P("ep", None),
            P(),
            P("ep", None),
            P("ep", None),
            P("ep", None, "tp"),
            P("ep", None, "tp"),
            P("ep", "tp", None),
            P(None, "tp"),
            P(None, "tp"),
            P("tp", None),
        ),
        out_specs=(P("ep", "tp"), P("ep", "tp")),
        check_vma=False,
    )
```

profile of v0, /device:TPU:0, one launch (start us, length us, event | category | flops | bytes accessed | tf_op | source)
XLA Modules:
  0.0 157.2 jit_solution(9918217330129436043)
XLA Ops:
  0.7 0.6 pad_add_fusion.refs_0_
  1.2 3.2 %prep.1 = (bf16[128,4096]{1,0:T(8,128)(2,1)}, s32[8,128]{1,0:T(8,128)}, bf16[96,2048]{1,0:T(8,128)(2,1)}, bf16[96,2048]{1,0:T(8,128)(2,1)}, bf16[96,2048]{1,0:T(8,128)(2,1)}, /*index=5*/bf16[96,2048]{1,0:T(8,128)(2,1)}) custom-call(s32[2]{0:T(128)} %pad_add_fusion.refs_0_, bf16[128,4096]{1,0:T(8,128)(2,1)} %refs_1_.3, f32[1,4096]{1,0:T(1,128)} %bitcast.26, ...), custom_call_target="tpu_custom_call" | custom-call | flops 201326592 | bytes 2097152 | tf_op jit(solution)/shard_map/prep/pallas_call | solution.py:101
  4.5 0.2 copy.28
  4.7 0.9 copy.25
  5.6 6.4 %all-to-all-start = ((bf16[8,64,512]{2,1,0:T(8,128)(2,1)}), bf16[8,64,512]{2,1,0:T(8,128)(2,1)S(1)}, u32[]{:S(2)}, u32[]{:S(2)}) async-start(bf16[8,64,512]{2,1,0:T(8,128)(2,1)} %copy.25), calls=%async_computation | async-start | bytes 1048576 | tf_op jit(solution)/shard_map/all_to_all | solution.py:570
  12.0 1.5 collective-permute-start.3
  13.5 1.5 collective-permute-start.4
  15.0 0.5 collective-permute-start.5
  15.5 8.7 %collective-permute-done.3.refs_3_ = bf16[96,2048]{1,0:T(8,128)(2,1)S(1)} collective-permute-done((bf16[96,2048]{1,0:T(8,128)(2,1)}, bf16[96,2048]{1,0:T(8,128)(2,1)S(1)}, u32[]{:S(2)}, u32[]{:S(2)}) %collective-permute-start.3) | collective-permute-done | bytes 393248 | tf_op jit(solution)/shard_map/ppermute | solution.py:35
  24.2 9.3 %collective-permute-done.4.refs_4_ = bf16[96,2048]{1,0:T(8,128)(2,1)} collective-permute-done((bf16[96,2048]{1,0:T(8,128)(2,1)}, bf16[96,2048]{1,0:T(8,128)(2,1)}, u32[]{:S(2)}, u32[]{:S(2)}) %collective-permute-start.4) | collective-permute-done | bytes 393248 | tf_op jit(solution)/shard_map/ppermute | solution.py:35
  33.4 0.5 collective-permute-start.9
  34.0 2.7 %cell_state.1.refs_0_ = f32[136,128]{1,0:T(8,128)} custom-call(s32[8,128]{1,0:T(8,128)} %get-tuple-element.17.refs_0_, bf16[1024,128]{1,0:T(8,128)(2,1)} %refs_2_.3, bf16[1024,256]{1,0:T(8,128)(2,1)} %refs_3_.4, f32[2,1024]{1,0:T(2,128)} %refs_4_.5, f32[2,1024]{1,0:T(2,128)} %refs_5_.3), custom_call_target="tpu_custom_call" | custom-call | flops 67108864 | bytes 1048576 | tf_op jit(solution)/shard_map/cell_state/pallas_call | solution.py:327
  36.6 0.7 collective-permute-start
  37.4 3.8 %collective-permute-done.refs_1_ = f32[136,128]{1,0:T(8,128)S(1)} collective-permute-done((f32[136,128]{1,0:T(8,128)}, f32[136,128]{1,0:T(8,128)S(1)}, u32[]{:S(2)}, u32[]{:S(2)}) %collective-permute-start) | collective-permute-done | bytes 69664 | tf_op jit(solution)/shard_map/ppermute | solution.py:35
  41.2 1.5 collective-permute-start.1
  42.7 3.0 %collective-permute-done.1.refs_2_ = f32[136,128]{1,0:T(8,128)S(1)} collective-permute-done((f32[136,128]{1,0:T(8,128)}, f32[136,128]{1,0:T(8,128)S(1)}, u32[]{:S(2)}, u32[]{:S(2)}) %collective-permute-start.1) | collective-permute-done | bytes 69664 | tf_op jit(solution)/shard_map/ppermute | solution.py:35
  45.7 1.5 collective-permute-start.2
  47.2 5.8 %cell_intra.1 = (f32[1024,256]{1,0:T(8,128)}, f32[1024,128]{1,0:T(8,128)}) custom-call(f32[136,128]{1,0:T(8,128)} %cell_state.1.refs_0_, bf16[1024,128]{1,0:T(8,128)(2,1)} %refs_4_.6, bf16[1024,128]{1,0:T(8,128)(2,1)} %refs_2_.3, bf16[1024,256]{1,0:T(8,128)(2,1)} %refs_3_.4, f32[2,1024]{1,0:T(2,128)} %refs_4_.5, f32[2,1024]{1,0:T(2,128)} %refs_5_.3), custom_call_target="tpu_custom_call" | custom-call | flops 402653184 | bytes 2097152 | tf_op jit(solution)/shard_map/cell_intra/pallas_call | solution.py:374
  53.0 0.6 copy-done.8
  53.6 6.3 %cell_finish.1.refs_1_.refs_2_ = bf16[1024,256]{1,0:T(8,128)(2,1)} custom-call(s32[1]{0:T(128)} %bitcast.3.refs_0_, f32[136,128]{1,0:T(8,128)} %copy-done.6, f32[136,128]{1,0:T(8,128)} %copy-done.7, f32[136,128]{1,0:T(8,128)} %copy-done.8, bf16[1024,128]{1,0:T(8,128)(2,1)} %refs_4_.6, bf16[1024,256]{1,0:T(8,128)(2,1)} %refs_5_.4, f32[1,256]{1,0:T(1,128)} %bitcast.28, ...), custom_call_target="tpu_custom_call" | custom-call | flops 67108864 | bytes 3145728 | tf_op jit(solution)/shard_map/cell_finish/pallas_call | solution.py:453
  59.9 15.3 %shard_map.185 = (bf16[384,2048]{1,0:T(8,128)(2,1)}, bf16[384,2048]{1,0:T(8,128)(2,1)}) custom-call(s32[1]{0:T(128)} %bitcast.2.refs_0_, bf16[1024,256]{1,0:T(8,128)(2,1)} %cell_finish.1.refs_1_.refs_2_, bf16[96,2048]{1,0:T(8,128)(2,1)} %get-tuple-element.22.refs_2_, bf16[96,2048]{1,0:T(8,128)(2,1)} %copy-done.12, ...), custom_call_target="tpu_custom_call" | custom-call | flops 4831838208 | bytes 18874368 | tf_op jit(solution)/shard_map/pallas_call | solution.py:211
  75.3 1.6 %broadcast_in_dim.2 = bf16[4,8,64,512]{3,2,1,0:T(8,128)(2,1)} broadcast(bf16[8,64,512]{2,1,0:T(8,128)(2,1)S(1)} %all-to-all-done), dimensions={1,2,3} | broadcast | bytes 2621440 | tf_op jit(solution)/shard_map/broadcast_in_dim | solution.py:587
  76.9 4.8 %all-to-all-start.1 = ((bf16[4,8,64,512]{3,2,1,0:T(8,128)(2,1)}), bf16[4,8,64,512]{3,2,1,0:T(8,128)(2,1)}, u32[]{:S(2)}, u32[]{:S(2)}) async-start(bf16[4,8,64,512]{3,2,1,0:T(8,128)(2,1)} %broadcast_in_dim.2), calls=%async_computation.1 | async-start | bytes 4194304 | tf_op jit(solution)/shard_map/all_to_all | solution.py:588
  81.7 1.7 %collective-permute-start.16 = (bf16[1024,256]{1,0:T(8,128)(2,1)S(1)}, bf16[1024,256]{1,0:T(8,128)(2,1)}, u32[]{:S(2)}, u32[]{:S(2)}) collective-permute-start(bf16[1024,256]{1,0:T(8,128)(2,1)S(1)} %copy-done.1), channel_id=1, source_target_pairs={{0,2},{1,3},{2,0},{3,1},{4,6},{5,7},{6,4},{7,5},{8,10},{9,11},{10,... | collective-permute-start | bytes 1572872 | tf_op jit(solution)/shard_map/ppermute | solution.py:35
  83.4 2.4 %collective-permute-start.18 = (bf16[1024,256]{1,0:T(8,128)(2,1)S(1)}, bf16[1024,256]{1,0:T(8,128)(2,1)}, u32[]{:S(2)}, u32[]{:S(2)}) collective-permute-start(bf16[1024,256]{1,0:T(8,128)(2,1)S(1)} %copy-done.1), channel_id=1, source_target_pairs={{0,4},{1,5},{2,6},{3,7},{4,0},{5,1},{6,2},{7,3},{8,12},{9,13},{10,... | collective-permute-start | bytes 1572872 | tf_op jit(solution)/shard_map/ppermute | solution.py:35
  85.7 0.4 collective-permute-start.20
  86.1 3.2 %add_convert_fusion = (bf16[96,2048]{1,0:T(8,128)(2,1)S(1)}, bf16[96,2048]{1,0:T(8,128)(2,1)S(1)}, bf16[96,2048]{1,0:T(8,128)(2,1)S(1)}, bf16[96,2048]{1,0:T(8,128)(2,1)}) fusion(bf16[384,2048]{1,0:T(8,128)(2,1)} %collective-permute-done.10, bf16[384,2048]{1,0:T(8,128)(2,1)} %get-tuple-element.26), kind=kLoop, calls=%fused_computation | loop fusion | flops 3145728 | bytes 4718592 | tf_op jit(solution)/shard_map/convert_element_type | solution.py:600
  89.4 1.7 %collective-permute-start.11 = (bf16[96,2048]{1,0:T(8,128)(2,1)S(1)}, bf16[96,2048]{1,0:T(8,128)(2,1)S(1)}, u32[]{:S(2)}, u32[]{:S(2)}) collective-permute-start(bf16[96,2048]{1,0:T(8,128)(2,1)S(1)} %get-tuple-element.34), channel_id=1, source_target_pairs={{0,8},{8,0},{16,24},{24,16},{1,9},{9,1},{17,25},{25,17},{2,10},{10... | collective-permute-start | bytes 1179656 | tf_op jit(solution)/shard_map/ppermute | solution.py:35
  91.1 1.5 collective-permute-start.12
  92.6 14.3 %collective-permute-done.16.refs_4_ = bf16[1024,256]{1,0:T(8,128)(2,1)} collective-permute-done((bf16[1024,256]{1,0:T(8,128)(2,1)S(1)}, bf16[1024,256]{1,0:T(8,128)(2,1)}, u32[]{:S(2)}, u32[]{:S(2)}) %collective-permute-start.16) | collective-permute-done | bytes 524320 | tf_op jit(solution)/shard_map/ppermute | solution.py:35
  106.9 2.2 %collective-permute-start.13 = (bf16[96,2048]{1,0:T(8,128)(2,1)S(1)}, bf16[96,2048]{1,0:T(8,128)(2,1)S(1)}, u32[]{:S(2)}, u32[]{:S(2)}) collective-permute-start(bf16[96,2048]{1,0:T(8,128)(2,1)S(1)} %get-tuple-element.32), channel_id=1, source_target_pairs={{0,24},{8,16},{16,8},{24,0},{1,25},{9,17},{17,9},{25,1},{2,26},{10... | collective-permute-start | bytes 1179656 | tf_op jit(solution)/shard_map/ppermute | solution.py:35
  109.1 7.5 %shard_map.186 = (bf16[128,2048]{1,0:T(8,128)(2,1)}, bf16[128,2048]{1,0:T(8,128)(2,1)}) custom-call(s32[1]{0:T(128)} %bitcast.2.refs_0_, bf16[96,2048]{1,0:T(8,128)(2,1)} %get-tuple-element.35.refs_1_, bf16[128,4096]{1,0:T(8,128)(2,1)} %get-tuple-element.28.refs_2_, bf16[4096,256]{1,0:T(8,128)(2,1)} %refs_3_.5, bf16[4096,256]{1,0:T(8,128)(2,1)} %refs_4_.7, ...), custom_call_target="tpu_custom_call" | custom-call | flops 805306368 | bytes 8388608 | tf_op jit(solution)/shard_map/pallas_call | solution.py:211
  116.6 5.0 %collective-permute-done.18.refs_6_ = bf16[1024,256]{1,0:T(8,128)(2,1)} collective-permute-done((bf16[1024,256]{1,0:T(8,128)(2,1)S(1)}, bf16[1024,256]{1,0:T(8,128)(2,1)}, u32[]{:S(2)}, u32[]{:S(2)}) %collective-permute-start.18) | collective-permute-done | bytes 524320 | tf_op jit(solution)/shard_map/ppermute | solution.py:35
  121.7 0.5 collective-permute-start.15
  122.3 0.4 collective-permute-start.19
  122.7 2.3 %collective-permute-done.13.refs_4_ = bf16[96,2048]{1,0:T(8,128)(2,1)S(1)} collective-permute-done((bf16[96,2048]{1,0:T(8,128)(2,1)S(1)}, bf16[96,2048]{1,0:T(8,128)(2,1)S(1)}, u32[]{:S(2)}, u32[]{:S(2)}) %collective-permute-start.13) | collective-permute-done | bytes 393248 | tf_op jit(solution)/shard_map/ppermute | solution.py:35
  125.0 0.7 copy-done.5
  125.7 0.7 copy.26
  126.5 0.7 copy.27.refs_8_
  127.2 0.8 copy-done.2
  128.0 4.4 %combine.1.refs_1_ = bf16[4,128,512]{2,1,0:T(8,128)(2,1)} custom-call(s32[1]{0:T(128)} %bitcast.1.refs_0_, bf16[96,2048]{1,0:T(8,128)(2,1)} %get-tuple-element.35.refs_1_, bf16[96,2048]{1,0:T(8,128)(2,1)} %copy-done.3, bf16[96,2048]{1,0:T(8,128)(2,1)} %copy-done.4, bf16[96,2048]{1,0:T(8,128)(2,1)} %copy-done.5, bf16[128,2048]{1,0:T(8,128)(2,1)} %get-tuple-element.29.refs_5_, ...), custom_call_target="tpu_custom_call" | custom-call | flops 402653184 | bytes 1048576 | tf_op jit(solution)/shard_map/combine/pallas_call | solution.py:253
  132.4 1.1 slice_bitcast_fusion.2
  133.5 9.2 %collective-permute-start.22 = (bf16[128,512]{1,0:T(8,128)(2,1)S(1)}, bf16[128,512]{1,0:T(8,128)(2,1)S(1)}, u32[]{:S(2)}, u32[]{:S(2)}) collective-permute-start(bf16[128,512]{1,0:T(8,128)(2,1)S(1)} %get-tuple-element.36), channel_id=1, source_target_pairs={{0,2},{1,3},{2,0},{3,1},{4,6},{5,7},{6,4},{7,5},{8,10},{9,11},{10,... | collective-permute-start | bytes 393224 | tf_op jit(solution)/shard_map/ppermute | solution.py:35
  142.7 1.0 collective-permute-start.23
  143.7 1.5 collective-permute-start.24
  145.1 6.6 %project.1 = bf16[1024,512]{1,0:T(8,128)(2,1)} custom-call(s32[1]{0:T(128)} %bitcast.refs_0_, bf16[4,128,512]{2,1,0:T(8,128)(2,1)} %combine.1.refs_1_, bf16[1024,256]{1,0:T(8,128)(2,1)} %cell_finish.1.refs_1_.refs_2_, bf16[1024,256]{1,0:T(8,128)(2,1)} %collective-permute-done.15.refs_3_, bf16[1024,256]{1,0:T(8,128)(2,1)} %collective-permute-done.16.refs_4_, ...), custom_call_target="tpu_custom_call" | custom-call | flops 2147483648 | bytes 4194304 | tf_op jit(solution)/shard_map/project/pallas_call | solution.py:504
  151.7 3.9 %collective-permute-done.23 = bf16[128,512]{1,0:T(8,128)(2,1)S(1)} collective-permute-done((bf16[128,512]{1,0:T(8,128)(2,1)S(1)}, bf16[128,512]{1,0:T(8,128)(2,1)S(1)}, u32[]{:S(2)}, u32[]{:S(2)}) %collective-permute-start.23) | collective-permute-done | bytes 131104 | tf_op jit(solution)/shard_map/ppermute | solution.py:35
  155.6 1.6 %fusion.2 = bf16[128,512]{1,0:T(8,128)(2,1)} fusion(bf16[128,512]{1,0:T(8,128)(2,1)S(1)} %collective-permute-done.24, bf16[128,512]{1,0:T(8,128)(2,1)S(1)} %collective-permute-done.23, bf16[128,512]{1,0:T(8,128)(2,1)S(1)} %collective-permute-done.22, bf16[4,128,512]{2,1,0:T(8,128)(2,1)} %combine.1.refs_1_), kind=kLoop, calls=%fused_computation.7 | loop fusion | flops 524288 | bytes 655360 | tf_op jit(solution)/shard_map/convert_element_type | solution.py:610
  (50 shorter events, 0.3 us)
Async XLA Ops:
  0.6 3.8 %copy-start = (bf16[256,4096]{1,0:T(8,128)(2,1)S(1)}, bf16[256,4096]{1,0:T(8,128)(2,1)}, u32[]{:S(2)}) copy-start(bf16[256,4096]{1,0:T(8,128)(2,1)} %param.25) | copy-start | bytes 6291460
  4.4 11.0 %copy-start.11 = (bf16[96,2048]{1,0:T(8,128)(2,1)S(1)}, bf16[96,2048]{1,0:T(8,128)(2,1)}, u32[]{:S(2)}) copy-start(bf16[96,2048]{1,0:T(8,128)(2,1)} %get-tuple-element.22.refs_2_) | copy-start | bytes 1179652
  5.6 54.3 %all-to-all-start = ((bf16[8,64,512]{2,1,0:T(8,128)(2,1)}), bf16[8,64,512]{2,1,0:T(8,128)(2,1)S(1)}, u32[]{:S(2)}, u32[]{:S(2)}) async-start(bf16[8,64,512]{2,1,0:T(8,128)(2,1)} %copy.25), calls=%async_computation | async-start | bytes 1048576 | tf_op jit(solution)/shard_map/all_to_all | solution.py:570
  12.0 12.2 %collective-permute-start.3 = (bf16[96,2048]{1,0:T(8,128)(2,1)}, bf16[96,2048]{1,0:T(8,128)(2,1)S(1)}, u32[]{:S(2)}, u32[]{:S(2)}) collective-permute-start(bf16[96,2048]{1,0:T(8,128)(2,1)} %get-tuple-element.23), channel_id=1, source_target_pairs={{0,8},{8,0},{16,24},{24,16},{1,9},{9,1},{17,25},{25,17},{2,10},{10... | collective-permute-start | bytes 1179656 | tf_op jit(solution)/shard_map/ppermute | solution.py:35
  13.5 20.0 %collective-permute-start.4 = (bf16[96,2048]{1,0:T(8,128)(2,1)}, bf16[96,2048]{1,0:T(8,128)(2,1)}, u32[]{:S(2)}, u32[]{:S(2)}) collective-permute-start(bf16[96,2048]{1,0:T(8,128)(2,1)} %get-tuple-element.24), channel_id=1, source_target_pairs={{0,16},{8,24},{16,0},{24,8},{1,17},{9,25},{17,1},{25,9},{2,18},{10... | collective-permute-start | bytes 1179656 | tf_op jit(solution)/shard_map/ppermute | solution.py:35
  15.0 18.5 %collective-permute-start.5 = (bf16[96,2048]{1,0:T(8,128)(2,1)}, bf16[96,2048]{1,0:T(8,128)(2,1)}, u32[]{:S(2)}, u32[]{:S(2)}) collective-permute-start(bf16[96,2048]{1,0:T(8,128)(2,1)} %get-tuple-element.25), channel_id=1, source_target_pairs={{0,24},{8,16},{16,8},{24,0},{1,25},{9,17},{17,9},{25,1},{2,26},{10... | collective-permute-start | bytes 1179656 | tf_op jit(solution)/shard_map/ppermute | solution.py:35
  15.5 44.4 %collective-permute-start.6 = (bf16[96,2048]{1,0:T(8,128)(2,1)S(1)}, bf16[96,2048]{1,0:T(8,128)(2,1)}, u32[]{:S(2)}, u32[]{:S(2)}) collective-permute-start(bf16[96,2048]{1,0:T(8,128)(2,1)S(1)} %copy-done.11), channel_id=1, source_target_pairs={{0,1},{1,0},{2,3},{3,2},{4,5},{5,4},{6,7},{7,6},{8,9},{9,8},{10,11... | collective-permute-start | bytes 1179656 | tf_op jit(solution)/shard_map/ppermute | solution.py:35
  24.2 28.8 %copy-start.12 = (bf16[96,2048]{1,0:T(8,128)(2,1)}, bf16[96,2048]{1,0:T(8,128)(2,1)S(1)}, u32[]{:S(2)}) copy-start(bf16[96,2048]{1,0:T(8,128)(2,1)S(1)} %collective-permute-done.3.refs_3_) | copy-start | bytes 1179652
  24.2 35.7 %collective-permute-start.7 = (bf16[96,2048]{1,0:T(8,128)(2,1)S(1)}, bf16[96,2048]{1,0:T(8,128)(2,1)}, u32[]{:S(2)}, u32[]{:S(2)}) collective-permute-start(bf16[96,2048]{1,0:T(8,128)(2,1)S(1)} %collective-permute-done.3.refs_3_), channel_id=1, source_target_pairs={{0,1},{1,0},{2,3},{3,2},{4,5},{5,4},{6,7},{7,6},{8,9},{9,8},{10,11... | collective-permute-start | bytes 1179656 | tf_op jit(solution)/shard_map/ppermute | solution.py:35
  33.4 26.5 %collective-permute-start.8 = (bf16[96,2048]{1,0:T(8,128)(2,1)}, bf16[96,2048]{1,0:T(8,128)(2,1)}, u32[]{:S(2)}, u32[]{:S(2)}) collective-permute-start(bf16[96,2048]{1,0:T(8,128)(2,1)} %collective-permute-done.4.refs_4_), channel_id=1, source_target_pairs={{0,1},{1,0},{2,3},{3,2},{4,5},{5,4},{6,7},{7,6},{8,9},{9,8},{10,11... | collective-permute-start | bytes 1179656 | tf_op jit(solution)/shard_map/ppermute | solution.py:35
  33.4 26.5 %collective-permute-start.9 = (bf16[96,2048]{1,0:T(8,128)(2,1)}, bf16[96,2048]{1,0:T(8,128)(2,1)}, u32[]{:S(2)}, u32[]{:S(2)}) collective-permute-start(bf16[96,2048]{1,0:T(8,128)(2,1)} %collective-permute-done.5.refs_5_), channel_id=1, source_target_pairs={{0,1},{1,0},{2,3},{3,2},{4,5},{5,4},{6,7},{7,6},{8,9},{9,8},{10,11... | collective-permute-start | bytes 1179656 | tf_op jit(solution)/shard_map/ppermute | solution.py:35
  36.6 4.5 %collective-permute-start = (f32[136,128]{1,0:T(8,128)}, f32[136,128]{1,0:T(8,128)S(1)}, u32[]{:S(2)}, u32[]{:S(2)}) collective-permute-start(f32[136,128]{1,0:T(8,128)} %cell_state.1.refs_0_), channel_id=1, source_target_pairs={{0,8},{8,0},{16,24},{24,16},{1,9},{9,1},{17,25},{25,17},{2,10},{10... | collective-permute-start | bytes 208904 | tf_op jit(solution)/shard_map/ppermute | solution.py:35
  41.2 11.9 %copy-start.6 = (f32[136,128]{1,0:T(8,128)}, f32[136,128]{1,0:T(8,128)S(1)}, u32[]{:S(2)}) copy-start(f32[136,128]{1,0:T(8,128)S(1)} %collective-permute-done.refs_1_) | copy-start | bytes 208900
  41.2 4.5 %collective-permute-start.1 = (f32[136,128]{1,0:T(8,128)}, f32[136,128]{1,0:T(8,128)S(1)}, u32[]{:S(2)}, u32[]{:S(2)}) collective-permute-start(f32[136,128]{1,0:T(8,128)} %cell_state.1.refs_0_), channel_id=1, source_target_pairs={{0,16},{8,24},{16,0},{24,8},{1,17},{9,25},{17,1},{25,9},{2,18},{10... | collective-permute-start | bytes 208904 | tf_op jit(solution)/shard_map/ppermute | solution.py:35
  45.7 7.3 %copy-start.7 = (f32[136,128]{1,0:T(8,128)}, f32[136,128]{1,0:T(8,128)S(1)}, u32[]{:S(2)}) copy-start(f32[136,128]{1,0:T(8,128)S(1)} %collective-permute-done.1.refs_2_) | copy-start | bytes 208900
  45.7 7.3 %collective-permute-start.2 = (f32[136,128]{1,0:T(8,128)}, f32[136,128]{1,0:T(8,128)S(1)}, u32[]{:S(2)}, u32[]{:S(2)}) collective-permute-start(f32[136,128]{1,0:T(8,128)} %cell_state.1.refs_0_), channel_id=1, source_target_pairs={{0,24},{8,16},{16,8},{24,0},{1,25},{9,17},{17,9},{25,1},{2,26},{10... | collective-permute-start | bytes 208904 | tf_op jit(solution)/shard_map/ppermute | solution.py:35
  53.0 0.6 copy-start.8
  75.2 10.9 %collective-permute-start.10 = (bf16[384,2048]{1,0:T(8,128)(2,1)}, bf16[384,2048]{1,0:T(8,128)(2,1)}, u32[]{:S(2)}, u32[]{:S(2)}) collective-permute-start(bf16[384,2048]{1,0:T(8,128)(2,1)} %get-tuple-element.27), channel_id=1, source_target_pairs={{0,1},{1,0},{2,3},{3,2},{4,5},{5,4},{6,7},{7,6},{8,9},{9,8},{10,11... | collective-permute-start | bytes 4718600 | tf_op jit(solution)/shard_map/ppermute | solution.py:35
  76.9 4.8 %copy-start.1 = (bf16[1024,256]{1,0:T(8,128)(2,1)S(1)}, bf16[1024,256]{1,0:T(8,128)(2,1)}, u32[]{:S(2)}) copy-start(bf16[1024,256]{1,0:T(8,128)(2,1)} %cell_finish.1.refs_1_.refs_2_) | copy-start | bytes 1572868
  76.9 68.3 %all-to-all-start.1 = ((bf16[4,8,64,512]{3,2,1,0:T(8,128)(2,1)}), bf16[4,8,64,512]{3,2,1,0:T(8,128)(2,1)}, u32[]{:S(2)}, u32[]{:S(2)}) async-start(bf16[4,8,64,512]{3,2,1,0:T(8,128)(2,1)} %broadcast_in_dim.2), calls=%async_computation.1 | async-start | bytes 4194304 | tf_op jit(solution)/shard_map/all_to_all | solution.py:588
  81.7 25.2 %collective-permute-start.16 = (bf16[1024,256]{1,0:T(8,128)(2,1)S(1)}, bf16[1024,256]{1,0:T(8,128)(2,1)}, u32[]{:S(2)}, u32[]{:S(2)}) collective-permute-start(bf16[1024,256]{1,0:T(8,128)(2,1)S(1)} %copy-done.1), channel_id=1, source_target_pairs={{0,2},{1,3},{2,0},{3,1},{4,6},{5,7},{6,4},{7,5},{8,10},{9,11},{10,... | collective-permute-start | bytes 1572872 | tf_op jit(solution)/shard_map/ppermute | solution.py:35
  83.4 38.3 %collective-permute-start.18 = (bf16[1024,256]{1,0:T(8,128)(2,1)S(1)}, bf16[1024,256]{1,0:T(8,128)(2,1)}, u32[]{:S(2)}, u32[]{:S(2)}) collective-permute-start(bf16[1024,256]{1,0:T(8,128)(2,1)S(1)} %copy-done.1), channel_id=1, source_target_pairs={{0,4},{1,5},{2,6},{3,7},{4,0},{5,1},{6,2},{7,3},{8,12},{9,13},{10,... | collective-permute-start | bytes 1572872 | tf_op jit(solution)/shard_map/ppermute | solution.py:35
  85.7 36.0 %collective-permute-start.20 = (bf16[1024,256]{1,0:T(8,128)(2,1)S(1)}, bf16[1024,256]{1,0:T(8,128)(2,1)}, u32[]{:S(2)}, u32[]{:S(2)}) collective-permute-start(bf16[1024,256]{1,0:T(8,128)(2,1)S(1)} %copy-done.1), channel_id=1, source_target_pairs={{0,6},{1,7},{2,4},{3,5},{4,2},{5,3},{6,0},{7,1},{8,14},{9,15},{10,... | collective-permute-start | bytes 1572872 | tf_op jit(solution)/shard_map/ppermute | solution.py:35
  89.4 32.8 %collective-permute-start.11 = (bf16[96,2048]{1,0:T(8,128)(2,1)S(1)}, bf16[96,2048]{1,0:T(8,128)(2,1)S(1)}, u32[]{:S(2)}, u32[]{:S(2)}) collective-permute-start(bf16[96,2048]{1,0:T(8,128)(2,1)S(1)} %get-tuple-element.34), channel_id=1, source_target_pairs={{0,8},{8,0},{16,24},{24,16},{1,9},{9,1},{17,25},{25,17},{2,10},{10... | collective-permute-start | bytes 1179656 | tf_op jit(solution)/shard_map/ppermute | solution.py:35
  91.1 31.2 %collective-permute-start.12 = (bf16[96,2048]{1,0:T(8,128)(2,1)S(1)}, bf16[96,2048]{1,0:T(8,128)(2,1)S(1)}, u32[]{:S(2)}, u32[]{:S(2)}) collective-permute-start(bf16[96,2048]{1,0:T(8,128)(2,1)S(1)} %get-tuple-element.33), channel_id=1, source_target_pairs={{0,16},{8,24},{16,0},{24,8},{1,17},{9,25},{17,1},{25,9},{2,18},{10... | collective-permute-start | bytes 1179656 | tf_op jit(solution)/shard_map/ppermute | solution.py:35
  106.9 18.1 %collective-permute-start.13 = (bf16[96,2048]{1,0:T(8,128)(2,1)S(1)}, bf16[96,2048]{1,0:T(8,128)(2,1)S(1)}, u32[]{:S(2)}, u32[]{:S(2)}) collective-permute-start(bf16[96,2048]{1,0:T(8,128)(2,1)S(1)} %get-tuple-element.32), channel_id=1, source_target_pairs={{0,24},{8,16},{16,8},{24,0},{1,25},{9,17},{17,9},{25,1},{2,26},{10... | collective-permute-start | bytes 1179656 | tf_op jit(solution)/shard_map/ppermute | solution.py:35
  109.1 16.6 %copy-start.9 = (s32[8,128]{1,0:T(8,128)S(1)}, s32[8,128]{1,0:T(8,128)}, u32[]{:S(2)}) copy-start(s32[8,128]{1,0:T(8,128)} %get-tuple-element.17.refs_0_) | copy-start | bytes 12292
  109.1 17.4 %copy-start.10 = (f32[128,2]{0,1:T(2,128)S(1)}, f32[128,2]{0,1:T(2,128)}, u32[]{:S(2)}) copy-start(f32[128,2]{0,1:T(2,128)} %param.29) | copy-start | bytes 3076
  121.7 5.6 %collective-permute-start.14 = (bf16[128,2048]{1,0:T(8,128)(2,1)}, bf16[128,2048]{1,0:T(8,128)(2,1)S(1)}, u32[]{:S(2)}, u32[]{:S(2)}) collective-permute-start(bf16[128,2048]{1,0:T(8,128)(2,1)} %get-tuple-element.30), channel_id=1, source_target_pairs={{0,1},{1,0},{2,3},{3,2},{4,5},{5,4},{6,7},{7,6},{8,9},{9,8},{10,11... | collective-permute-start | bytes 1572872 | tf_op jit(solution)/shard_map/ppermute | solution.py:35
  121.7 21.0 %collective-permute-start.15 = (bf16[1024,256]{1,0:T(8,128)(2,1)S(1)}, bf16[1024,256]{1,0:T(8,128)(2,1)}, u32[]{:S(2)}, u32[]{:S(2)}) collective-permute-start(bf16[1024,256]{1,0:T(8,128)(2,1)S(1)} %copy-done.1), channel_id=1, source_target_pairs={{0,1},{1,0},{2,3},{3,2},{4,5},{5,4},{6,7},{7,6},{8,9},{9,8},{10,11... | collective-permute-start | bytes 1572872 | tf_op jit(solution)/shard_map/ppermute | solution.py:35
  122.2 5.0 %copy-start.3 = (bf16[96,2048]{1,0:T(8,128)(2,1)}, bf16[96,2048]{1,0:T(8,128)(2,1)S(1)}, u32[]{:S(2)}) copy-start(bf16[96,2048]{1,0:T(8,128)(2,1)S(1)} %collective-permute-done.11.refs_2_) | copy-start | bytes 1179652
  122.2 21.5 %collective-permute-start.17 = (bf16[1024,256]{1,0:T(8,128)(2,1)}, bf16[1024,256]{1,0:T(8,128)(2,1)}, u32[]{:S(2)}, u32[]{:S(2)}) collective-permute-start(bf16[1024,256]{1,0:T(8,128)(2,1)} %collective-permute-done.16.refs_4_), channel_id=1, source_target_pairs={{0,1},{1,0},{2,3},{3,2},{4,5},{5,4},{6,7},{7,6},{8,9},{9,8},{10,11... | collective-permute-start | bytes 1572872 | tf_op jit(solution)/shard_map/ppermute | solution.py:35
  122.3 2.7 %copy-start.4 = (bf16[96,2048]{1,0:T(8,128)(2,1)}, bf16[96,2048]{1,0:T(8,128)(2,1)S(1)}, u32[]{:S(2)}) copy-start(bf16[96,2048]{1,0:T(8,128)(2,1)S(1)} %collective-permute-done.12.refs_3_) | copy-start | bytes 1179652
  122.3 22.8 %collective-permute-start.19 = (bf16[1024,256]{1,0:T(8,128)(2,1)}, bf16[1024,256]{1,0:T(8,128)(2,1)}, u32[]{:S(2)}, u32[]{:S(2)}) collective-permute-start(bf16[1024,256]{1,0:T(8,128)(2,1)} %collective-permute-done.18.refs_6_), channel_id=1, source_target_pairs={{0,1},{1,0},{2,3},{3,2},{4,5},{5,4},{6,7},{7,6},{8,9},{9,8},{10,11... | collective-permute-start | bytes 1572872 | tf_op jit(solution)/shard_map/ppermute | solution.py:35
  125.0 0.7 copy-start.5
  125.7 19.4 %collective-permute-start.21 = (bf16[1024,256]{1,0:T(8,128)(2,1)}, bf16[1024,256]{1,0:T(8,128)(2,1)}, u32[]{:S(2)}, u32[]{:S(2)}) collective-permute-start(bf16[1024,256]{1,0:T(8,128)(2,1)} %collective-permute-done.20.refs_8_), channel_id=1, source_target_pairs={{0,1},{1,0},{2,3},{3,2},{4,5},{5,4},{6,7},{7,6},{8,9},{9,8},{10,11... | collective-permute-start | bytes 1572872 | tf_op jit(solution)/shard_map/ppermute | solution.py:35
  127.2 0.8 copy-start.2
  133.5 18.2 %collective-permute-start.22 = (bf16[128,512]{1,0:T(8,128)(2,1)S(1)}, bf16[128,512]{1,0:T(8,128)(2,1)S(1)}, u32[]{:S(2)}, u32[]{:S(2)}) collective-permute-start(bf16[128,512]{1,0:T(8,128)(2,1)S(1)} %get-tuple-element.36), channel_id=1, source_target_pairs={{0,2},{1,3},{2,0},{3,1},{4,6},{5,7},{6,4},{7,5},{8,10},{9,11},{10,... | collective-permute-start | bytes 393224 | tf_op jit(solution)/shard_map/ppermute | solution.py:35
  142.7 12.9 %collective-permute-start.23 = (bf16[128,512]{1,0:T(8,128)(2,1)S(1)}, bf16[128,512]{1,0:T(8,128)(2,1)S(1)}, u32[]{:S(2)}, u32[]{:S(2)}) collective-permute-start(bf16[128,512]{1,0:T(8,128)(2,1)S(1)} %get-tuple-element.38), channel_id=1, source_target_pairs={{0,4},{1,5},{2,6},{3,7},{4,0},{5,1},{6,2},{7,3},{8,12},{9,13},{10,... | collective-permute-start | bytes 393224 | tf_op jit(solution)/shard_map/ppermute | solution.py:35
  143.7 11.9 %collective-permute-start.24 = (bf16[128,512]{1,0:T(8,128)(2,1)S(1)}, bf16[128,512]{1,0:T(8,128)(2,1)S(1)}, u32[]{:S(2)}, u32[]{:S(2)}) collective-permute-start(bf16[128,512]{1,0:T(8,128)(2,1)S(1)} %get-tuple-element.37), channel_id=1, source_target_pairs={{0,6},{1,7},{2,4},{3,5},{4,2},{5,3},{6,0},{7,1},{8,14},{9,15},{10,... | collective-permute-start | bytes 393224 | tf_op jit(solution)/shard_map/ppermute | solution.py:35
where the time goes:
time: 158 us; the launch traced here: 157 us
  Pallas kernels  51.6 us (33%)
  waiting for transfers between devices  50.4 us (32%)
  starting transfers between devices  41.5 us (26%)
  local copies, waits for them, and re-layouts  7.47 us (5%)
  other arithmetic  5.46 us (3%)
    ppermute x25, waiting for transfers between devices, swap(): return lax.ppermute(x, axis, xor_pairs(lax.axis_size(axis), k))  50.4 us
    ppermute x25, starting transfers between devices, swap(): return lax.ppermute(x, axis, xor_pairs(lax.axis_size(axis), k))  30.3 us
    pallas_call x2, Pallas kernels, ffn(): pl.pallas_call(with_deps(functools.partial(ffn_kernel, n_lhs=len(lhs), pe...  22.8 us
    pallas_call x1, Pallas kernels, project(): pl.pallas_call(with_deps(functools.partial(project_kernel, n_tp=n_tp), le...  6.57 us
    all_to_all x1, starting transfers between devices, local(): share = lax.all_to_all(share, 'tp', 0, 0, tiled=True)  6.35 us
    pallas_call x1, Pallas kernels, cell_finish(): pl.pallas_call(with_deps(functools.partial(finish_kernel, n_packs=len(pac...  6.25 us
    pallas_call x1, Pallas kernels, cell_intra(): pl.pallas_call(with_deps(functools.partial(intra_kernel, block=256), len(...  5.82 us
    all_to_all x1, starting transfers between devices, local(): columns = lax.all_to_all(everyone, 'ep', 0, 0, tiled=True)  4.78 us
  transfers between devices with their start and end apart: 27, of which 8 were waited for; matrix products, arithmetic and copies ran while one was open for 5% of the time, Pallas kernels for 21%

commit v1 on v0

v1 whole, which is shorter than its diff:
```python
import functools

import jax
import jax.numpy as jnp
from jax import lax
from jax.experimental import pallas as pl
from jax.experimental.pallas import tpu as pltpu
from jax.sharding import PartitionSpec as P


DK = 64
DV = 128
LANES = 128
SUB = 8
NEG = -1e30
EPS = 1e-06

F32 = jnp.float32
BF16 = jnp.bfloat16


def params(limit_mib=56, semantics=None):
    return pltpu.CompilerParams(vmem_limit_bytes=limit_mib << 20, dimension_semantics=semantics)


def cost(flops, nbytes, trans=0):
    return pl.CostEstimate(flops=int(flops), bytes_accessed=int(nbytes), transcendentals=int(trans))


def xor_pairs(n, k):
    return [(i, i ^ k) for i in range(n)]


def swap(x, axis, k):
    return lax.ppermute(x, axis, xor_pairs(lax.axis_size(axis), k))


def dot(a, b):
    return jnp.dot(a, b, preferred_element_type=F32)


def dot_nt(a, b):
    return lax.dot_general(a, b, (((1,), (1,)), ((), ())), preferred_element_type=F32)


def two_parts(x):
    high = x.astype(BF16)
    return high, (x - high.astype(F32)).astype(BF16)


def with_deps(kernel, n_deps, lead):
    def body(*refs):
        return kernel(*refs[:lead], *refs[lead + n_deps :])

    return body


def anywhere(deps):
    return [pl.BlockSpec(memory_space=pl.ANY) for _ in deps]


def prep_kernel(idx, rows, gain, routes, weight, normed, dest, share, *outgoing_and_sems):
    *outgoing, buf, sems = outgoing_and_sems
    n_rows, width = rows.shape
    n_tp, part, cols = share.shape
    wanted = pl.ds(pl.multiple_of(idx[2] * part, part), part)
    coming = pltpu.make_async_copy(weight.at[wanted, :], buf, sems.at[n_tp])
    coming.start()
    half = width // 2
    n_out = len(outgoing)
    cap = outgoing[0].shape[0]
    topk = routes.shape[0]
    me, core = idx[0], idx[1]
    step = 16
    for first in range(0, n_rows, step):
        wide = rows[first : first + step, :].astype(F32)
        inverse = lax.rsqrt(jnp.mean(wide * wide, axis=1, keepdims=True) + EPS)
        normed[first : first + step, :] = (wide * inverse * gain[...]).astype(BF16)
    coming.wait()
    leaving = start_all(
        [
            pltpu.make_async_copy(buf.at[:, pl.ds(t * cols, cols)], share.at[t], sems.at[t])
            for t in range(n_tp)
        ]
    )
    n_tgt = max(SUB, n_out)
    target = lax.broadcasted_iota(jnp.int32, (n_tgt, n_rows), 0) ^ me
    named = [routes[k : k + 1, :] == target for k in range(topk)]
    member = functools.reduce(jnp.logical_or, named)
    earlier = lax.broadcasted_iota(jnp.int32, (n_rows, n_rows), 0) < lax.broadcasted_iota(
        jnp.int32, (n_rows, n_rows), 1
    )
    place = dot(member.astype(F32).astype(BF16), earlier.astype(F32).astype(BF16)).astype(jnp.int32)
    slot = lax.broadcasted_iota(jnp.int32, (n_tgt, n_rows), 0) * cap + place
    dest[...] = jnp.zeros(dest.shape, jnp.int32)
    for k in range(topk):
        dest[k : k + 1, :] = jnp.sum(jnp.where(named[k], slot, 0), axis=0, keepdims=True)
    mine = normed[:, pl.ds(pl.multiple_of(core * half, LANES), half)]
    spot = lax.broadcasted_iota(jnp.int32, (cap, n_rows), 0)
    member_i = jnp.where(member, place, -1)
    for j in range(n_out):
        pick = (member_i[j : j + 1, :] == spot).astype(F32).astype(BF16)
        outgoing[j][...] = dot(pick, mine).astype(BF16)
    wait_all(leaving)


def prep(idx, rows, gain, routes, weight, n_ep, n_tp, cap, deps=()):
    n_rows, width = rows.shape
    shapes = [
        jax.ShapeDtypeStruct((n_rows, width), BF16),
        jax.ShapeDtypeStruct((SUB, n_rows), jnp.int32),
        jax.ShapeDtypeStruct((n_tp, weight.shape[0] // 2, weight.shape[1] // n_tp), BF16),
    ] + [jax.ShapeDtypeStruct((cap, width // 2), BF16) for _ in range(n_ep)]
    vm = pl.BlockSpec(memory_space=pltpu.VMEM)
    hbm = pl.BlockSpec(memory_space=pl.ANY)
    out = pl.pallas_call(
        with_deps(prep_kernel, len(deps), 1),
        out_shape=shapes,
        in_specs=[pl.BlockSpec(memory_space=pltpu.SMEM), *anywhere(deps), vm, vm, vm, hbm],
        out_specs=[vm, vm, hbm] + [vm] * n_ep,
        scratch_shapes=[
            pltpu.VMEM((weight.shape[0] // 2, weight.shape[1]), BF16),
            pltpu.SemaphoreType.DMA((n_tp + 1,)),
        ],
        compiler_params=params(),
        cost_estimate=cost(2 * n_ep * cap * n_rows * width // 2, 4 * n_rows * width),
        name="prep",
    )(idx, *deps, rows, gain, routes, weight)
    return out[0], out[1], out[2], list(out[3:])


def start_all(copies):
    for c in copies:
        c.start()
    return copies


def wait_all(copies):
    for c in copies:
        c.wait()


def gated(x, gate_buf, up_buf, arrivals, chunk):
    g = u = None
    for i, waiting in enumerate(arrivals):
        wait_all(waiting)
        rows = slice(i * chunk, (i + 1) * chunk)
        left = x[:, rows]
        g_part, u_part = dot(left, gate_buf[rows, :]), dot(left, up_buf[rows, :])
        g = g_part if g is None else g + g_part
        u = u_part if u is None else u + u_part
    return (g * jax.nn.sigmoid(g) * u).astype(BF16)


def expert_kernel(core_idx, *refs, n_ep, n_z, chunk):
    own, other, rest = refs[:n_ep], refs[n_ep : 2 * n_ep], refs[2 * n_ep :]
    gate, up, down, send, hidden, x, gate_buf, up_buf, down_buf, stage, sems = rest
    core = core_idx[0]
    cap, half = own[0].shape
    pair = down_buf.shape[1] // n_z
    count = iter(range(sems.shape[0]))

    def copy(src, dst):
        return pltpu.make_async_copy(src, dst, sems.at[next(count)])

    per_half = half // chunk
    arrivals = []
    for h, group in enumerate((own, other)):
        lhs = start_all(
            [
                copy(r, x.at[pl.ds(k * cap, cap), pl.ds(h * half, half)])
                for k, r in enumerate(group)
            ]
        )
        for i in range(per_half):
            src = pl.ds(pl.multiple_of((core ^ h) * half + i * chunk, chunk), chunk)
            dst = pl.ds(h * half + i * chunk, chunk)
            weights = start_all(
                [
                    copy(gate.at[0, src, :], gate_buf.at[dst, :]),
                    copy(up.at[0, src, :], up_buf.at[dst, :]),
                ]
            )
            arrivals.append((lhs if i == 0 else []) + weights)
    tail = start_all(
        [
            copy(
                down.at[0, :, pl.ds(pl.multiple_of((2 * n + 1 - core) * pair, LANES), pair)],
                down_buf.at[:, pl.ds(n * pair, pair)],
            )
            for n in range(n_z)
        ]
    )
    hidden[...] = gated(x, gate_buf, up_buf, arrivals, chunk)
    leaving = []
    for n in range(n_z):
        tail[n].wait()
        cols = pl.ds(n * pair, pair)
        stage[:, cols] = dot(hidden[...], down_buf[:, cols]).astype(BF16)
        leaving += start_all([copy(stage.at[:, cols], send.at[:, cols])])
    wait_all(leaving)


def expert(core_idx, own, other, gate, up, down, n_z, deps=()):
    n_ep = len(own)
    cap, half = own[0].shape
    rows = n_ep * cap
    width, hid = gate.shape[-2:]
    chunk = 512
    n_sems = 2 * n_ep + 2 * (width // chunk) + 2 * n_z
    hbm = pl.BlockSpec(memory_space=pl.ANY)
    vm = pl.BlockSpec(memory_space=pltpu.VMEM)
    return pl.pallas_call(
        with_deps(
            functools.partial(expert_kernel, n_ep=n_ep, n_z=n_z, chunk=chunk), len(deps), 1
        ),
        out_shape=[
            jax.ShapeDtypeStruct((rows, half), BF16),
            jax.ShapeDtypeStruct((rows, hid), BF16),
        ],
        in_specs=[pl.BlockSpec(memory_space=pltpu.SMEM)] + anywhere(deps) + [hbm] * (2 * n_ep + 3),
        out_specs=[hbm, vm],
        scratch_shapes=[
            pltpu.VMEM((rows, width), BF16),
            pltpu.VMEM((width, hid), BF16),
            pltpu.VMEM((width, hid), BF16),
            pltpu.VMEM((hid, half), BF16),
            pltpu.VMEM((rows, half), BF16),
            pltpu.SemaphoreType.DMA((n_sems,)),
        ],
        compiler_params=params(),
        cost_estimate=cost(5 * rows * width * hid, 5 * width * hid + 4 * rows * width),
        name="expert",
    )(core_idx, *deps, *own, *other, gate, up, down)


def pair_kernel(core_idx, hidden, got, down, *refs, n_z):
    back, down_buf, sems = refs[:-2], refs[-2], refs[-1]
    core = core_idx[0]
    cap, half = back[0].shape
    pair = half // n_z
    copies = start_all(
        [
            pltpu.make_async_copy(
                down.at[0, :, pl.ds(pl.multiple_of((2 * n + core) * pair, LANES), pair)],
                down_buf.at[:, pl.ds(n * pair, pair)],
                sems.at[n],
            )
            for n in range(n_z)
        ]
    )
    for n in range(n_z):
        copies[n].wait()
        cols = pl.ds(n * pair, pair)
        both = (dot(hidden[...], down_buf[:, cols]) + got[:, cols].astype(F32)).astype(BF16)
        for k, out in enumerate(back):
            out[:, cols] = both[k * cap : (k + 1) * cap, :]


def pair_sum(core_idx, hidden, got, down, n_ep, n_z, deps=()):
    rows, half = got.shape
    hid = hidden.shape[1]
    hbm = pl.BlockSpec(memory_space=pl.ANY)
    vm = pl.BlockSpec(memory_space=pltpu.VMEM)
    return pl.pallas_call(
        with_deps(functools.partial(pair_kernel, n_z=n_z), len(deps), 1),
        out_shape=[jax.ShapeDtypeStruct((rows // n_ep, half), BF16) for _ in range(n_ep)],
        in_specs=[pl.BlockSpec(memory_space=pltpu.SMEM)] + anywhere(deps) + [vm, vm, hbm],
        out_specs=[vm] * n_ep,
        scratch_shapes=[pltpu.VMEM((hid, half), BF16), pltpu.SemaphoreType.DMA((n_z,))],
        compiler_params=params(),
        cost_estimate=cost(2 * rows * hid * half, 2 * hid * half + 4 * rows * half),
        name="pair_sum",
    )(core_idx, *deps, hidden, got, down)


def shared_kernel(core_idx, x, gate, up, down, send, own, gate_buf, up_buf, down_buf, sems, *, n_z, chunk):
    core = core_idx[0]
    width = x.shape[1]
    pair = own.shape[1] // n_z
    count = iter(range(sems.shape[0]))

    def copy(src, dst):
        return pltpu.make_async_copy(src, dst, sems.at[next(count)])

    arrivals = []
    for i in range(width // chunk):
        rows = pl.ds(i * chunk, chunk)
        arrivals.append(
            start_all(
                [copy(gate.at[rows, :], gate_buf.at[rows, :]), copy(up.at[rows, :], up_buf.at[rows, :])]
            )
        )
    tail = start_all([copy(down, down_buf)])
    hidden = gated(x, gate_buf, up_buf, arrivals, chunk)
    wait_all(tail)
    for n in range(n_z):
        cols = pl.ds(n * pair, pair)
        for out, side in ((send, 1 - core), (own, core)):
            there = pl.ds(pl.multiple_of((2 * n + side) * pair, LANES), pair)
            out[:, cols] = dot(hidden, down_buf[:, there]).astype(BF16)


def shared(core_idx, x, gate, up, down, n_z, deps=()):
    rows, width = x.shape
    hid = gate.shape[1]
    chunk = 1024
    hbm = pl.BlockSpec(memory_space=pl.ANY)
    vm = pl.BlockSpec(memory_space=pltpu.VMEM)
    shape = jax.ShapeDtypeStruct((rows, width // 2), BF16)
    return pl.pallas_call(
        with_deps(functools.partial(shared_kernel, n_z=n_z, chunk=chunk), len(deps), 1),
        out_shape=[shape, shape],
        in_specs=[pl.BlockSpec(memory_space=pltpu.SMEM)] + anywhere(deps) + [vm, hbm, hbm, hbm],
        out_specs=[vm, vm],
        scratch_shapes=[
            pltpu.VMEM((width, hid), BF16),
            pltpu.VMEM((width, hid), BF16),
            pltpu.VMEM((hid, width), BF16),
            pltpu.SemaphoreType.DMA((2 * (width // chunk) + 1,)),
        ],
        compiler_params=params(),
        cost_estimate=cost(6 * rows * width * hid, 6 * width * hid + 4 * rows * width),
        name="shared",
    )(core_idx, *deps, x, gate, up, down)


def combine_kernel(z_idx, *refs, n_ep, n_z, topk):
    blocks, rest = refs[:n_ep], refs[n_ep:]
    shared_own, shared_other, dest, weight, outs = *rest[:4], rest[4:]
    z = z_idx[0]
    cap = blocks[0].shape[0]
    n_rows, wide = outs[0].shape
    spot = lax.broadcasted_iota(jnp.int32, (n_rows, n_ep * cap), 1)
    picks = [(dest[:, k : k + 1] == spot).astype(F32).astype(BF16) for k in range(topk)]
    shares = [jnp.broadcast_to(weight[:, k : k + 1], (n_rows, wide)) for k in range(topk)]
    for j in range(n_z):
        cols = pl.ds(pl.multiple_of((z ^ j) * wide, LANES), wide)
        back = jnp.concatenate([b[:, cols] for b in blocks], axis=0)
        total = shared_own[:, cols].astype(F32) + shared_other[:, cols].astype(F32)
        for k in range(topk):
            total = total + shares[k] * dot(picks[k], back)
        outs[j][...] = total.astype(BF16)


def combine(z_idx, blocks, shared_own, shared_other, dest, weight, n_z, deps=()):
    n_rows, half = shared_own.shape
    cap = blocks[0].shape[0]
    topk = weight.shape[1]
    vm = pl.BlockSpec(memory_space=pltpu.VMEM)
    return pl.pallas_call(
        with_deps(
            functools.partial(combine_kernel, n_ep=len(blocks), n_z=n_z, topk=topk), len(deps), 1
        ),
        out_shape=[jax.ShapeDtypeStruct((n_rows, half // n_z), BF16) for _ in range(n_z)],
        in_specs=[pl.BlockSpec(memory_space=pltpu.SMEM)]
        + anywhere(deps)
        + [vm] * (len(blocks) + 4),
        out_specs=[vm] * n_z,
        compiler_params=params(),
        cost_estimate=cost(2 * topk * n_rows * len(blocks) * cap * half, 4 * n_rows * half),
        name="combine",
    )(z_idx, *deps, *blocks, shared_own, shared_other, dest, weight)


def gate_rows(in_gate, forget_gate):
    heads, length = in_gate.shape
    head_of = lax.broadcasted_iota(jnp.int32, (SUB, length), 0) * heads // SUB
    gate = jnp.broadcast_to(in_gate[0:1, :], (SUB, length))
    forget = jnp.broadcast_to(forget_gate[0:1, :], (SUB, length))
    for h in range(1, heads):
        gate = jnp.where(head_of >= h, in_gate[h : h + 1, :], gate)
        forget = jnp.where(head_of >= h, forget_gate[h : h + 1, :], forget)
    log_forget = jnp.minimum(forget, 0.0) - jnp.log1p(jnp.exp(-jnp.abs(forget)))
    n_chunks = length // LANES
    stacked = jnp.concatenate(
        [log_forget[:, c * LANES : (c + 1) * LANES] for c in range(n_chunks)], axis=0
    )
    row = lax.broadcasted_iota(jnp.int32, (LANES, 2 * LANES), 0)
    col = lax.broadcasted_iota(jnp.int32, (LANES, 2 * LANES), 1)
    summing = ((row <= col) | (col >= LANES)).astype(F32).astype(BF16)
    first, rest = two_parts(stacked)
    second = rest
    third = ((stacked - first.astype(F32)) - second.astype(F32)).astype(BF16)
    sums = dot(first, summing) + dot(second, summing) + dot(third, summing)
    offset = jnp.zeros((SUB, LANES), F32)
    parts = []
    for c in range(n_chunks):
        rows = slice(c * SUB, (c + 1) * SUB)
        parts.append(sums[rows, :LANES] + offset)
        offset = offset + sums[rows, LANES:]
    cum = jnp.concatenate(parts, axis=1)
    return gate - cum, cum


def running_max(rise):
    length = rise.shape[1]
    n_chunks = length // LANES
    lane = lax.broadcasted_iota(jnp.int32, (n_chunks * SUB, LANES), 1)
    peak = jnp.concatenate([rise[:, c * LANES : (c + 1) * LANES] for c in range(n_chunks)], axis=0)
    shift = 1
    while shift < LANES:
        peak = jnp.maximum(peak, jnp.where(lane >= shift, pltpu.roll(peak, shift, 1), NEG))
        shift *= 2
    tops = jnp.broadcast_to(peak[:, LANES - 1 : LANES], peak.shape)
    so_far = jnp.full((SUB, LANES), NEG, F32)
    parts = []
    for c in range(n_chunks):
        rows = slice(c * SUB, (c + 1) * SUB)
        parts.append(jnp.maximum(peak[rows, :], so_far))
        so_far = jnp.maximum(so_far, tops[rows, :])
    return jnp.concatenate(parts, axis=1)


def state_kernel(keys, values, in_gate, forget_gate, pack, rows):
    heads, length = in_gate.shape
    rise, cum = gate_rows(in_gate[...], forget_gate[...])
    rows[0:SUB, :] = rise
    rows[SUB : 2 * SUB, :] = cum
    last = cum[:, length - 1 : length]
    top = jnp.max(rise, axis=1, keepdims=True)
    weight = jnp.exp(rise - top)
    key_t = jnp.transpose(keys[...].astype(F32))
    lane = lax.broadcasted_iota(jnp.int32, (1, LANES), 1)
    pack[...] = jnp.zeros(pack.shape, F32)
    columns = []
    decay_row = jnp.zeros((1, LANES), F32)
    stab_row = jnp.zeros((1, LANES), F32)
    for h in range(heads):
        r = h * SUB // heads
        scaled = key_t[h * DK : (h + 1) * DK, :] * weight[r : r + 1, :]
        high, low = two_parts(scaled)
        v = values[:, h * DV : (h + 1) * DV]
        pack[h * DK : (h + 1) * DK, :] = dot(high, v) + dot(low, v)
        columns.append(jnp.sum(scaled, axis=1, keepdims=True))
        here = lane // DK == h
        decay_row = jnp.where(here, last[r : r + 1, :], decay_row)
        stab_row = jnp.where(here, last[r : r + 1, :] + top[r : r + 1, :], stab_row)
    if heads * DK < LANES:
        columns.append(jnp.zeros((LANES - heads * DK, 1), F32))
    column = jnp.concatenate(columns, axis=0)
    normal = jnp.transpose(jnp.broadcast_to(column, (LANES, LANES)))
    base = heads * DK
    pack[base : base + 1, :] = normal[0:1, :]
    pack[base + 1 : base + 2, :] = decay_row
    pack[base + 2 : base + 3, :] = stab_row


def cell_state(keys, values, in_gate, forget_gate, deps=()):
    heads, length = in_gate.shape
    vm = pl.BlockSpec(memory_space=pltpu.VMEM)
    return pl.pallas_call(
        with_deps(state_kernel, len(deps), 0),
        in_specs=anywhere(deps) + [vm] * 4,
        out_shape=[
            jax.ShapeDtypeStruct((heads * DK + SUB, DV), F32),
            jax.ShapeDtypeStruct((2 * SUB, length), F32),
        ],
        compiler_params=params(),
        cost_estimate=cost(4 * heads * length * DK * DV, 4 * keys.size + 2 * values.size),
        name="cell_state",
    )(*deps, keys, values, in_gate, forget_gate)


def intra_kernel(queries, keys, values, rows, inner, stats, *, block, heads):
    length = queries.shape[0]
    rise = rows[0:SUB, :]
    peak = running_max(rise)
    peak_col = jnp.transpose(peak)
    scale = DK ** (-0.5)
    causal = lax.broadcasted_iota(jnp.int32, (block, block), 1) <= lax.broadcasted_iota(
        jnp.int32, (block, block), 0
    )
    place = lax.broadcasted_iota(jnp.int32, (block, SUB), 1)
    totals = []
    for first in range(0, length, block):
        seen = first + block
        kept = jnp.zeros((block, SUB), F32)
        for h in range(heads):
            r = h * SUB // heads
            ks, vs = slice(h * DK, (h + 1) * DK), slice(h * DV, (h + 1) * DV)
            q = (queries[first:seen, ks].astype(F32) * scale).astype(BF16)
            mu = peak_col[first:seen, r : r + 1]
            level = jnp.where(causal, rise[r : r + 1, first:seen] - mu, NEG)
            scores = dot_nt(q, keys[first:seen, ks]) * jnp.exp(level)
            total = jnp.sum(scores, axis=1, keepdims=True)
            part = dot(scores.astype(BF16), values[first:seen, vs])
            if first:
                scores = dot_nt(q, keys[0:first, ks]) * jnp.exp(rise[r : r + 1, 0:first] - mu)
                total = total + jnp.sum(scores, axis=1, keepdims=True)
                part = part + dot(scores.astype(BF16), values[0:first, vs])
            inner[first:seen, vs] = part
            kept = jnp.where(place * heads // SUB == h, total, kept)
        totals.append(kept)
    stats[0:SUB, :] = jnp.transpose(jnp.concatenate(totals, axis=0))
    stats[SUB : 2 * SUB, :] = peak


def cell_intra(queries, keys, values, rows, heads, deps=()):
    length = queries.shape[0]
    vm = pl.BlockSpec(memory_space=pltpu.VMEM)
    return pl.pallas_call(
        with_deps(functools.partial(intra_kernel, block=256, heads=heads), len(deps), 0),
        in_specs=anywhere(deps) + [vm] * 4,
        out_shape=[
            jax.ShapeDtypeStruct((length, heads * DV), F32),
            jax.ShapeDtypeStruct((2 * SUB, length), F32),
        ],
        compiler_params=params(),
        cost_estimate=cost(heads * length * length * (DK + DV), 8 * values.size, heads * length * length),
        name="cell_intra",
    )(*deps, queries, keys, values, rows)


def finish_kernel(ep_idx, *refs, n_packs, heads, block):
    packs, rest = refs[:n_packs], refs[n_packs:]
    queries, out_gate, gain, inner, stats, rows, mixed = rest
    me = ep_idx[0]
    base = heads * DK
    length = queries.shape[0]
    before = [jnp.bitwise_xor(me, k + 1) for k in range(n_packs)]
    decay = [p[base + 1 : base + 2, :] for p in packs]
    after = []
    anchor = jnp.zeros((1, LANES), F32)
    for k in range(n_packs):
        gone = jnp.zeros((1, LANES), F32)
        for other in range(n_packs):
            between = (before[other] > before[k]) & (before[other] < me)
            gone = gone + jnp.where(between, decay[other], 0.0)
        after.append(gone)
        anchor = anchor + jnp.where(before[k] < me, decay[k], 0.0)
    levels = [packs[k][base + 2 : base + 3, :] + after[k] for k in range(n_packs)]
    stab = anchor
    for k in range(n_packs):
        stab = jnp.maximum(stab, jnp.where(before[k] < me, levels[k], NEG))
    weights = [
        jnp.where(before[k] < me, jnp.exp(jnp.minimum(levels[k] - stab, 0.0)), 0.0)
        for k in range(n_packs)
    ]
    normal = jnp.zeros((1, LANES), F32)
    for k in range(n_packs):
        normal = normal + weights[k] * packs[k][base : base + 1, :]
    scale = DK ** (-0.5)
    total, peak, cum = stats[0:SUB, :], stats[SUB : 2 * SUB, :], rows[SUB : 2 * SUB, :]
    head_of = lax.broadcasted_iota(jnp.int32, (SUB, length), 0) * heads // SUB
    stab_in = jnp.broadcast_to(stab[:, 0:1], (SUB, length))
    normal_dot = jnp.zeros((SUB, length), F32)
    states = []
    for h in range(heads):
        ks = slice(h * DK, (h + 1) * DK)
        matrix = jnp.zeros((DK, DV), F32)
        for k in range(n_packs):
            matrix = matrix + weights[k][:, h * DK : h * DK + 1] * packs[k][ks, :]
        states.append(two_parts(matrix))
        n_high, n_low = two_parts(jnp.broadcast_to(normal[:, ks], (SUB, DK)))
        q = queries[:, ks]
        along = (dot_nt(n_high, q) + dot_nt(n_low, q)) * scale
        normal_dot = jnp.where(head_of == h, along, normal_dot)
        stab_in = jnp.where(head_of == h, stab[:, h * DK : h * DK + 1], stab_in)
    mu = jnp.maximum(peak, stab_in)
    here = jnp.exp(peak - mu)
    there = jnp.exp(stab_in - mu)
    divisor = jnp.maximum(jnp.abs(total * here + there * normal_dot), jnp.exp(-(cum + mu)))
    here_col = jnp.transpose(here / divisor)
    there_col = jnp.transpose(there / divisor * scale)
    for first in range(0, length, block):
        span = slice(first, first + block)
        for h in range(heads):
            r = h * SUB // heads
            cols, ks = slice(h * DV, (h + 1) * DV), slice(h * DK, (h + 1) * DK)
            q = queries[span, ks]
            across = dot(q, states[h][0]) + dot(q, states[h][1])
            cells = inner[span, cols] * here_col[span, r : r + 1] + across * there_col[span, r : r + 1]
            opened = jax.nn.sigmoid(out_gate[span, cols].astype(F32)) * gain[:, cols]
            mixed[span, cols] = (cells * opened).astype(BF16)


def cell_finish(ep_idx, packs, queries, out_gate, gain, inner, stats, rows, heads, deps=()):
    length, width = out_gate.shape
    vm = pl.BlockSpec(memory_space=pltpu.VMEM)
    return pl.pallas_call(
        with_deps(
            functools.partial(finish_kernel, n_packs=len(packs), heads=heads, block=256), len(deps), 1
        ),
        out_shape=jax.ShapeDtypeStruct((length, width), BF16),
        in_specs=[pl.BlockSpec(memory_space=pltpu.SMEM)]
        + anywhere(deps)
        + [vm] * (len(packs) + 6),
        compiler_params=params(),
        cost_estimate=cost(4 * heads * length * DK * DV, 12 * length * width, length * width),
        name="cell_finish",
    )(ep_idx, *deps, *packs, queries, out_gate, gain, inner, stats, rows)


def project_kernel(idx, *refs, n_tp):
    mixed, (share, low_part, high_part, out, joined, sems) = refs[:n_tp], refs[n_tp:]
    me = idx[0]
    _, part, _ = share.shape
    half_tp = n_tp // 2

    @pl.when(pl.program_id(0) == 0)
    def _():
        waits = []
        for j in range(n_tp):
            source = me ^ j
            low = source < half_tp
            bit = jnp.where(low, idx[1], idx[2])
            for h in range(2):
                first = pl.multiple_of(j * 2 * part + (bit ^ h) * part, part)
                dst, sem = joined.at[pl.ds(first, part), :], sems.at[2 * j + h]
                if h == 0:
                    pltpu.make_async_copy(share.at[source], dst, sem).start()
                else:

                    @pl.when(low)
                    def _():
                        pltpu.make_async_copy(low_part.at[source], dst, sem).start()

                    @pl.when(jnp.logical_not(low))
                    def _():
                        pltpu.make_async_copy(high_part.at[source - half_tp], dst, sem).start()

                waits.append(pltpu.make_async_copy(share.at[source], dst, sem))
        wait_all(waits)

    lhs = jnp.concatenate([m[...] for m in mixed], axis=1)
    out[...] = dot(lhs, joined[...]).astype(BF16)


def project(idx, mixed, share, low_part, high_part, deps=()):
    length, own = mixed[0].shape
    n_tp = len(mixed)
    cols = share.shape[-1]
    block = 256
    return pl.pallas_call(
        with_deps(functools.partial(project_kernel, n_tp=n_tp), len(deps), 1),
        out_shape=jax.ShapeDtypeStruct((length, cols), BF16),
        grid_spec=pltpu.PrefetchScalarGridSpec(
            num_scalar_prefetch=1,
            grid=(length // block,),
            in_specs=anywhere(deps)
            + [pl.BlockSpec((block, own), lambda i, idx: (i, 0)) for _ in mixed]
            + anywhere((share, low_part, high_part)),
            out_specs=pl.BlockSpec((block, cols), lambda i, idx: (i, 0)),
            scratch_shapes=[
                pltpu.VMEM((n_tp * own, cols), BF16),
                pltpu.SemaphoreType.DMA((2 * n_tp,)),
            ],
        ),
        compiler_params=params(semantics=("arbitrary",)),
        cost_estimate=cost(2 * length * n_tp * own * cols, 2 * length * n_tp * own),
        name="project",
    )(idx, *deps, *mixed, share, low_part, high_part)


def local(
    queries,
    keys,
    values,
    out_gate,
    in_gate,
    forget_gate,
    out_gain,
    out_weight,
    moe_rows,
    moe_gain,
    routes,
    route_weight,
    expert_gate,
    expert_up,
    expert_down,
    shared_gate,
    shared_up,
    shared_down,
):
    n_tp, n_ep = lax.axis_size("tp"), lax.axis_size("ep")
    n_z = n_tp // 2
    me_tp, me_ep = lax.axis_index("tp"), lax.axis_index("ep")
    me_z, core = me_tp // 2, me_tp % 2
    heads = in_gate.shape[0]
    routed_rows, _ = moe_rows.shape
    topk = routes.shape[1]
    exact = 3 * routed_rows * topk // (2 * n_ep)
    cap = -(-exact // 16) * 16

    low_bit, high_bit = me_ep % 2, me_ep // (n_ep // 2)
    half_tp = n_tp // 2
    own_bit = jnp.where(me_tp < half_tp, low_bit, high_bit)
    idx = jnp.stack([me_ep, core, own_bit]).astype(jnp.int32)
    core_idx = core.reshape(1).astype(jnp.int32)
    z_idx = me_z.reshape(1).astype(jnp.int32)
    ep_idx = me_ep.reshape(1).astype(jnp.int32)

    normed, dest, share, outgoing = prep(
        idx,
        moe_rows,
        moe_gain.reshape(1, -1),
        routes.astype(jnp.int32).T,
        out_weight,
        n_ep,
        n_tp,
        cap,
    )
    arrived = [outgoing[0]]
    for k in range(1, n_ep):
        arrived.append(swap(outgoing[k], "ep", k))

    share = lax.all_to_all(share, "tp", 0, 0, tiled=True)

    pack, gate_info = cell_state(keys, values, in_gate, forget_gate, [dest])
    packs = []
    for k in range(1, n_ep):
        packs.append(swap(pack, "ep", k))
    inner, stats = cell_intra(queries, keys, values, gate_info, heads, [pack])
    mixed = cell_finish(
        ep_idx, packs, queries, out_gate, out_gain.reshape(1, -1), inner, stats, gate_info, heads
    )
    gathered = [mixed]
    for k in range(1, n_z):
        gathered.append(swap(mixed, "tp", 2 * k))
    pieces = []
    for g in gathered:
        pieces += [g, swap(g, "tp", 1)]
    others = []
    for a in arrived:
        others.append(swap(a, "tp", 1))
    send, hidden = expert(
        core_idx, arrived, others, expert_gate, expert_up, expert_down, n_z, [mixed]
    )
    got = swap(send, "tp", 1)
    low_part = swap(share[:half_tp], "ep", 1)
    high_part = swap(share[half_tp:], "ep", n_ep // 2)
    sums = pair_sum(core_idx, hidden, got, expert_down, n_ep, n_z)
    back = [sums[0]]
    for k in range(1, n_ep):
        back.append(swap(sums[k], "ep", k))
    shared_send, shared_own = shared(
        core_idx, normed, shared_gate, shared_up, shared_down, n_z, [sums[0]]
    )
    shared_other = swap(shared_send, "tp", 1)
    part_out = combine(z_idx, back, shared_own, shared_other, dest.T, route_weight, n_z)
    total = part_out[0].astype(F32)
    for k in range(1, n_z):
        total = total + swap(part_out[k], "tp", 2 * k).astype(F32)
    moe_out = total.astype(BF16)
    mixer_out = project(
        jnp.stack([me_tp, low_bit, high_bit]).astype(jnp.int32), pieces, share, low_part, high_part
    )
    return (mixer_out, moe_out)


def solution(mesh):
    return jax.shard_map(
        local,
        mesh=mesh,
        in_specs=(
            P("ep", "tp"),
            P("ep", "tp"),
            P("ep", "tp"),
            P("ep", "tp"),
            P("tp", "ep"),
            P("tp", "ep"),
            P("tp"),
            P("tp", None),
            P("ep", None),
            P(),
            P("ep", None),
            P("ep", None),
            P("ep", None, "tp"),
            P("ep", None, "tp"),
            P("ep", "tp", None),
            P(None, "tp"),
            P(None, "tp"),
            P("tp", None),
        ),
        out_specs=(P("ep", "tp"), P("ep", "tp")),
        check_vma=False,
    )
```

time: 158 us -> 173 us (1.095)
  waiting for transfers between devices: 50.4 us -> 83.5 us
  starting transfers between devices: 41.5 us -> 32.9 us
  other arithmetic: 5.46 us -> 1.99 us
  Pallas kernels: 51.6 us -> 48.3 us
  local copies, waits for them, and re-layouts: 7.47 us -> 5.06 us
    ppermute x25 -> x27, waiting for transfers between devices: 50.4 us -> 83.5 us  [swap(): return lax.ppermute(x, axis, xor_pairs(lax.axis_size(axis), k))]
    all_to_all x1 -> x0, starting transfers between devices: 4.78 us -> none  [local(): columns = lax.all_to_all(everyone, 'ep', 0, 0, tiled=True)]
    convert_element_type x1 -> x0, other arithmetic: 3.25 us -> none  [local(): pair = (own[rows].astype(F32) + got[rows].astype(F32)).astype(BF16)]
    pallas_call x3 -> x4, Pallas kernels: 28.6 us -> 26 us  [the longest x1 9.06 us: expert(): pl.pallas_call(with_deps(functools.partial(expert_kernel, n_ep=n_ep, n_z=...]
    ppermute x25 -> x27, starting transfers between devices: 30.3 us -> 27.8 us  [swap(): return lax.ppermute(x, axis, xor_pairs(lax.axis_size(axis), k))]
    pallas_call x1, Pallas kernels: 6.25 us -> 3.9 us  [cell_finish(): pl.pallas_call(with_deps(functools.partial(finish_kernel, n_packs=len(pac...]
    pallas_call x1, Pallas kernels: 3.19 us -> 5.05 us  [prep(): pl.pallas_call(with_deps(prep_kernel, len(deps), 1), out_shape=shapes, in...]
    unnamed x28 -> x39, local copies, waits for them, and re-layouts: 3.11 us -> 4.27 us
  transfers between devices with their start and end apart: 27 -> 28, of which waited for: 8 -> 9; matrix products, arithmetic and copies ran while one was open for 5% -> 1% of each run, Pallas kernels for 21% -> 20%
where the time goes in v1:
time: 173 us
  waiting for transfers between devices  83.5 us (48%)
  Pallas kernels  48.3 us (28%)
  starting transfers between devices  32.9 us (19%)
  local copies, waits for them, and re-layouts  5.06 us (3%)
  other arithmetic  1.99 us (1%)
    ppermute x27, waiting for transfers between devices, swap(): return lax.ppermute(x, axis, xor_pairs(lax.axis_size(axis), k))  83.5 us
    ppermute x27, starting transfers between devices, swap(): return lax.ppermute(x, axis, xor_pairs(lax.axis_size(axis), k))  27.8 us
    pallas_call x1, Pallas kernels, expert(): pl.pallas_call(with_deps(functools.partial(expert_kernel, n_ep=n_ep, n_z=...  9.06 us
    pallas_call x1, Pallas kernels, project(): pl.pallas_call(with_deps(functools.partial(project_kernel, n_tp=n_tp), le...  7.93 us
    pallas_call x1, Pallas kernels, cell_intra(): pl.pallas_call(with_deps(functools.partial(intra_kernel, block=256, heads...  6.03 us
    pallas_call x1, Pallas kernels, shared(): pl.pallas_call(with_deps(functools.partial(shared_kernel, n_z=n_z, chunk=...  5.58 us
    pallas_call x1, Pallas kernels, pair_sum(): pl.pallas_call(with_deps(functools.partial(pair_kernel, n_z=n_z), len(dep...  5.29 us
    pallas_call x1, Pallas kernels, prep(): pl.pallas_call(with_deps(prep_kernel, len(deps), 1), out_shape=shapes, in...  5.05 us
  transfers between devices with their start and end apart: 28, of which 9 were waited for; matrix products, arithmetic and copies ran while one was open for 1% of the time, Pallas kernels for 20%

profile of v1, /device:TPU:0, one launch (start us, length us, event | category | flops | bytes accessed | tf_op | source)
XLA Modules:
  0.0 172.7 jit_solution(16564551595055028931)
XLA Ops:
  0.7 0.6 pad_add_fusion.1.refs_0_
  1.3 5.0 %prep.1 = (bf16[128,4096]{1,0:T(8,128)(2,1)}, s32[8,128]{1,0:T(8,128)}, bf16[8,128,512]{2,1,0:T(8,128)(2,1)}, bf16[96,2048]{1,0:T(8,128)(2,1)}, bf16[96,2048]{1,...) custom-call(s32[3]{0:T(128)} %pad_add_fusion.1.refs_0_, bf16[128,4096]{1,0:T(8,128)(2,1)} %refs_1_.3, ...), custom_call_target="tpu_custom_call" | custom-call | flops 201326592 | bytes 2097152 | tf_op jit(solution)/shard_map/prep/pallas_call | solution.py:116
  6.3 3.0 %collective-permute-start.12 = (bf16[96,2048]{1,0:T(8,128)(2,1)}, bf16[96,2048]{1,0:T(8,128)(2,1)S(1)}, u32[]{:S(2)}, u32[]{:S(2)}) collective-permute-start(bf16[96,2048]{1,0:T(8,128)(2,1)} %get-tuple-element.32), channel_id=1, source_target_pairs={{0,8},{8,0},{16,24},{24,16},{1,9},{9,1},{17,25},{25,17},{2,10},{10... | collective-permute-start | bytes 1179656 | tf_op jit(solution)/shard_map/ppermute | solution.py:35
  9.4 1.5 collective-permute-start.13
  10.9 8.6 %collective-permute-done.12.refs_3_ = bf16[96,2048]{1,0:T(8,128)(2,1)S(1)} collective-permute-done((bf16[96,2048]{1,0:T(8,128)(2,1)}, bf16[96,2048]{1,0:T(8,128)(2,1)S(1)}, u32[]{:S(2)}, u32[]{:S(2)}) %collective-permute-start.12) | collective-permute-done | bytes 393248 | tf_op jit(solution)/shard_map/ppermute | solution.py:35
  19.6 9.0 %collective-permute-done.13.refs_4_ = bf16[96,2048]{1,0:T(8,128)(2,1)S(1)} collective-permute-done((bf16[96,2048]{1,0:T(8,128)(2,1)}, bf16[96,2048]{1,0:T(8,128)(2,1)S(1)}, u32[]{:S(2)}, u32[]{:S(2)}) %collective-permute-start.13) | collective-permute-done | bytes 393248 | tf_op jit(solution)/shard_map/ppermute | solution.py:35
  28.6 0.5 collective-permute-start.18
  29.1 2.4 %cell_state.1 = (f32[136,128]{1,0:T(8,128)}, f32[16,1024]{1,0:T(8,128)}) custom-call(s32[8,128]{1,0:T(8,128)} %get-tuple-element.25.refs_0_, bf16[1024,128]{1,0:T(8,128)(2,1)} %refs_2_.3, bf16[1024,256]{1,0:T(8,128)(2,1)} %refs_3_.5, f32[2,1024]{1,0:T(2,128)} %refs_3_.4, f32[2,1024]{1,0:T(2,128)} %refs_4_.5), custom_call_target="tpu_custom_call" | custom-call | flops 67108864 | bytes 1048576 | tf_op jit(solution)/shard_map/cell_state/pallas_call | solution.py:452
  31.5 0.9 collective-permute-start
  32.4 3.7 %collective-permute-done.refs_1_ = f32[136,128]{1,0:T(8,128)S(1)} collective-permute-done((f32[136,128]{1,0:T(8,128)}, f32[136,128]{1,0:T(8,128)S(1)}, u32[]{:S(2)}, u32[]{:S(2)}) %collective-permute-start) | collective-permute-done | bytes 69664 | tf_op jit(solution)/shard_map/ppermute | solution.py:35
  36.0 1.5 collective-permute-start.1
  37.5 3.0 %collective-permute-done.1.refs_2_ = f32[136,128]{1,0:T(8,128)S(1)} collective-permute-done((f32[136,128]{1,0:T(8,128)}, f32[136,128]{1,0:T(8,128)S(1)}, u32[]{:S(2)}, u32[]{:S(2)}) %collective-permute-start.1) | collective-permute-done | bytes 69664 | tf_op jit(solution)/shard_map/ppermute | solution.py:35
  40.5 1.5 collective-permute-start.2
  42.0 6.0 %cell_intra.1 = (f32[1024,256]{1,0:T(8,128)}, f32[16,1024]{1,0:T(8,128)}) custom-call(f32[136,128]{1,0:T(8,128)} %get-tuple-element.26.refs_0_, bf16[1024,128]{1,0:T(8,128)(2,1)} %refs_4_.6, bf16[1024,128]{1,0:T(8,128)(2,1)} %refs_2_.3, bf16[1024,256]{1,0:T(8,128)(2,1)} %refs_3_.5, f32[16,1024]{1,0:T(8,128)} %get-tuple-element.27.refs_4_.refs_9_), custom_call_target="tpu_custom_call" | custom-call | flops 402653184 | bytes 2097152 | tf_op jit(solution)/shard_map/cell_intra/pallas_call | solution.py:502
  48.1 0.6 copy-done.15
  48.7 3.9 %cell_finish.1.refs_1_ = bf16[1024,256]{1,0:T(8,128)(2,1)} custom-call(s32[1]{0:T(128)} %bitcast.3.refs_0_, f32[136,128]{1,0:T(8,128)} %copy-done.13, f32[136,128]{1,0:T(8,128)} %copy-done.14, f32[136,128]{1,0:T(8,128)} %copy-done.15, bf16[1024,128]{1,0:T(8,128)(2,1)} %refs_4_.6, bf16[1024,256]{1,0:T(8,128)(2,1)} %refs_5_.2, f32[1,256]{1,0:T(1,128)} %bitcast.14, ...), custom_call_target="tpu_custom_call" | custom-call | flops 67108864 | bytes 3145728 | tf_op jit(solution)/shard_map/cell_finish/pallas_call | solution.py:581
  52.7 0.7 copy-done.8
  53.4 0.1 copy-done.9
  53.5 0.1 copy-done.10
  53.6 0.7 copy-done.11
  54.4 9.1 %expert.1 = (bf16[384,2048]{1,0:T(8,128)(2,1)}, bf16[384,512]{1,0:T(8,128)(2,1)}) custom-call(s32[1]{0:T(128)} %bitcast.4.refs_0_, bf16[1024,256]{1,0:T(8,128)(2,1)} %cell_finish.1.refs_1_, bf16[96,2048]{1,0:T(8,128)(2,1)} %get-tuple-element.31.refs_2_, bf16[96,2048]{1,0:T(8,128)(2,1)} %copy-done.5, bf16[96,2048]{1,0:T(8,128)(2,1)} %copy-done.6, ...), custom_call_target="tpu_custom_call" | custom-call | flops 4026531840 | bytes 16777216 | tf_op jit(solution)/shard_map/expert/pallas_call | solution.py:213
  63.5 5.0 %all-to-all-start = ((bf16[8,128,512]{2,1,0:T(8,128)(2,1)}), bf16[8,128,512]{2,1,0:T(8,128)(2,1)S(1)}, u32[]{:S(2)}, u32[]{:S(2)}) async-start(bf16[8,128,512]{2,1,0:T(8,128)(2,1)} %get-tuple-element.30), calls=%async_computation | async-start | bytes 2097152 | tf_op jit(solution)/shard_map/all_to_all | solution.py:708
  68.6 2.0 %collective-permute-start.4 = (bf16[1024,256]{1,0:T(8,128)(2,1)S(1)}, bf16[1024,256]{1,0:T(8,128)(2,1)}, u32[]{:S(2)}, u32[]{:S(2)}) collective-permute-start(bf16[1024,256]{1,0:T(8,128)(2,1)S(1)} %copy-done.1), channel_id=1, source_target_pairs={{0,2},{1,3},{2,0},{3,1},{4,6},{5,7},{6,4},{7,5},{8,10},{9,11},{10,... | collective-permute-start | bytes 1572872 | tf_op jit(solution)/shard_map/ppermute | solution.py:35
  70.6 2.4 %collective-permute-start.6 = (bf16[1024,256]{1,0:T(8,128)(2,1)S(1)}, bf16[1024,256]{1,0:T(8,128)(2,1)}, u32[]{:S(2)}, u32[]{:S(2)}) collective-permute-start(bf16[1024,256]{1,0:T(8,128)(2,1)S(1)} %copy-done.1), channel_id=1, source_target_pairs={{0,4},{1,5},{2,6},{3,7},{4,0},{5,1},{6,2},{7,3},{8,12},{9,13},{10,... | collective-permute-start | bytes 1572872 | tf_op jit(solution)/shard_map/ppermute | solution.py:35
  73.0 1.2 copy-done.2
  74.2 5.3 %pair_sum.1 = (bf16[96,2048]{1,0:T(8,128)(2,1)}, bf16[96,2048]{1,0:T(8,128)(2,1)}, bf16[96,2048]{1,0:T(8,128)(2,1)}, bf16[96,2048]{1,0:T(8,128)(2,1)}) custom-call(s32[1]{0:T(128)} %bitcast.4.refs_0_, bf16[384,512]{1,0:T(8,128)(2,1)} %get-tuple-element.35.refs_1_, bf16[384,2048]{1,0:T(8,128)(2,1)} %copy-done.2, bf16[1,512,4096]{2,1,0:T(8,128)(2,1)} %refs_3_.6), custom_call_target="tpu_custom_call" | custom-call | flops 805306368 | bytes 5242880 | tf_op jit(solution)/shard_map/pair_sum/pallas_call | solution.py:265
  79.5 5.6 %shared.1 = (bf16[128,2048]{1,0:T(8,128)(2,1)}, bf16[128,2048]{1,0:T(8,128)(2,1)}) custom-call(s32[1]{0:T(128)} %bitcast.4.refs_0_, bf16[96,2048]{1,0:T(8,128)(2,1)} %get-tuple-element.37.refs_1_, bf16[128,4096]{1,0:T(8,128)(2,1)} %get-tuple-element.41.refs_2_, bf16[4096,256]{1,0:T(8,128)(2,1)} %refs_3_.7, bf16[4096,256]{1,0:T(8,128)(2,1)} %refs_4_.7, ...), custom_call_target="tpu_custom_call" | custom-call | flops 805306368 | bytes 8388608 | tf_op jit(solution)/shard_map/shared/pallas_call | solution.py:311
  85.1 0.6 collective-permute-start.23
  85.7 20.9 %collective-permute-done.4.refs_3_ = bf16[1024,256]{1,0:T(8,128)(2,1)} collective-permute-done((bf16[1024,256]{1,0:T(8,128)(2,1)S(1)}, bf16[1024,256]{1,0:T(8,128)(2,1)}, u32[]{:S(2)}, u32[]{:S(2)}) %collective-permute-start.4) | collective-permute-done | bytes 524320 | tf_op jit(solution)/shard_map/ppermute | solution.py:35
  106.6 1.5 collective-permute-start.20
  108.1 21.4 %collective-permute-done.6.refs_5_ = bf16[1024,256]{1,0:T(8,128)(2,1)} collective-permute-done((bf16[1024,256]{1,0:T(8,128)(2,1)S(1)}, bf16[1024,256]{1,0:T(8,128)(2,1)}, u32[]{:S(2)}, u32[]{:S(2)}) %collective-permute-start.6) | collective-permute-done | bytes 524320 | tf_op jit(solution)/shard_map/ppermute | solution.py:35
  129.5 1.0 collective-permute-start.21
  130.5 2.0 %collective-permute-start.22 = (bf16[96,2048]{1,0:T(8,128)(2,1)}, bf16[96,2048]{1,0:T(8,128)(2,1)}, u32[]{:S(2)}, u32[]{:S(2)}) collective-permute-start(bf16[96,2048]{1,0:T(8,128)(2,1)} %get-tuple-element.40), channel_id=1, source_target_pairs={{0,24},{8,16},{16,8},{24,0},{1,25},{9,17},{17,9},{25,1},{2,26},{10... | collective-permute-start | bytes 1179656 | tf_op jit(solution)/shard_map/ppermute | solution.py:35
  132.7 0.5 collective-permute-start.7
  133.2 15.1 %collective-permute-done.21.refs_3_ = bf16[96,2048]{1,0:T(8,128)(2,1)} collective-permute-done((bf16[96,2048]{1,0:T(8,128)(2,1)}, bf16[96,2048]{1,0:T(8,128)(2,1)}, u32[]{:S(2)}, u32[]{:S(2)}) %collective-permute-start.21) | collective-permute-done | bytes 393248 | tf_op jit(solution)/shard_map/ppermute | solution.py:35
  148.3 1.5 collective-permute-start.10
  149.8 0.5 collective-permute-start.11
  150.3 0.7 copy.20
  151.0 0.7 copy.21.refs_8_
  151.7 0.7 pad_add_fusion.refs_0_
  152.4 3.1 %combine.1 = (bf16[128,512]{1,0:T(8,128)(2,1)}, bf16[128,512]{1,0:T(8,128)(2,1)}, bf16[128,512]{1,0:T(8,128)(2,1)}, bf16[128,512]{1,0:T(8,128)(2,1)}) custom-call(s32[1]{0:T(128)} %bitcast.9.refs_0_, bf16[96,2048]{1,0:T(8,128)(2,1)} %get-tuple-element.37.refs_1_, bf16[96,2048]{1,0:T(8,128)(2,1)} %copy-done.4, ...), custom_call_target="tpu_custom_call" | custom-call | flops 402653184 | bytes 1048576 | tf_op jit(solution)/shard_map/combine/pallas_call | solution.py:351
  155.5 4.3 %collective-permute-start.24 = (bf16[128,512]{1,0:T(8,128)(2,1)}, bf16[128,512]{1,0:T(8,128)(2,1)S(1)}, u32[]{:S(2)}, u32[]{:S(2)}) collective-permute-start(bf16[128,512]{1,0:T(8,128)(2,1)} %get-tuple-element.45), channel_id=1, source_target_pairs={{0,2},{1,3},{2,0},{3,1},{4,6},{5,7},{6,4},{7,5},{8,10},{9,11},{10,... | collective-permute-start | bytes 393224 | tf_op jit(solution)/shard_map/ppermute | solution.py:35
  159.9 0.4 collective-permute-start.25
  160.3 2.0 %collective-permute-start.26 = (bf16[128,512]{1,0:T(8,128)(2,1)}, bf16[128,512]{1,0:T(8,128)(2,1)S(1)}, u32[]{:S(2)}, u32[]{:S(2)}) collective-permute-start(bf16[128,512]{1,0:T(8,128)(2,1)} %get-tuple-element.47), channel_id=1, source_target_pairs={{0,6},{1,7},{2,4},{3,5},{4,2},{5,3},{6,0},{7,1},{8,14},{9,15},{10,... | collective-permute-start | bytes 393224 | tf_op jit(solution)/shard_map/ppermute | solution.py:35
  162.3 0.4 collective-permute-done.10.refs_10_
  162.7 1.2 collective-permute-done.11.refs_11_
  164.0 7.9 %project.1 = bf16[1024,512]{1,0:T(8,128)(2,1)} custom-call(s32[3]{0:T(128)} %pad_add_fusion.refs_0_, bf16[1024,256]{1,0:T(8,128)(2,1)} %cell_finish.1.refs_1_, bf16[1024,256]{1,0:T(8,128)(2,1)} %collective-permute-done.3.refs_2_, bf16[1024,256]{1,0:T(8,128)(2,1)} %collective-permute-done.4.refs_3_, bf16[1024,256]{1,0:T(8,128)(2,1)} %copy-done.18, ...), custom_call_target="tpu_custom_call" | custom-call | flops 2147483648 | bytes 4194304 | tf_op jit(solution)/shard_map/project/pallas_call | solution.py:635
  171.9 0.7 add_convert_fusion
  (61 shorter events, 0.4 us)
Async XLA Ops:
  6.3 13.2 %collective-permute-start.12 = (bf16[96,2048]{1,0:T(8,128)(2,1)}, bf16[96,2048]{1,0:T(8,128)(2,1)S(1)}, u32[]{:S(2)}, u32[]{:S(2)}) collective-permute-start(bf16[96,2048]{1,0:T(8,128)(2,1)} %get-tuple-element.32), channel_id=1, source_target_pairs={{0,8},{8,0},{16,24},{24,16},{1,9},{9,1},{17,25},{25,17},{2,10},{10... | collective-permute-start | bytes 1179656 | tf_op jit(solution)/shard_map/ppermute | solution.py:35
  9.4 19.2 %collective-permute-start.13 = (bf16[96,2048]{1,0:T(8,128)(2,1)}, bf16[96,2048]{1,0:T(8,128)(2,1)S(1)}, u32[]{:S(2)}, u32[]{:S(2)}) collective-permute-start(bf16[96,2048]{1,0:T(8,128)(2,1)} %get-tuple-element.33), channel_id=1, source_target_pairs={{0,16},{8,24},{16,0},{24,8},{1,17},{9,25},{17,1},{25,9},{2,18},{10... | collective-permute-start | bytes 1179656 | tf_op jit(solution)/shard_map/ppermute | solution.py:35
  10.9 17.7 %collective-permute-start.14 = (bf16[96,2048]{1,0:T(8,128)(2,1)}, bf16[96,2048]{1,0:T(8,128)(2,1)S(1)}, u32[]{:S(2)}, u32[]{:S(2)}) collective-permute-start(bf16[96,2048]{1,0:T(8,128)(2,1)} %get-tuple-element.34), channel_id=1, source_target_pairs={{0,24},{8,16},{16,8},{24,0},{1,25},{9,17},{17,9},{25,1},{2,26},{10... | collective-permute-start | bytes 1179656 | tf_op jit(solution)/shard_map/ppermute | solution.py:35
  10.9 41.7 %collective-permute-start.15 = (bf16[96,2048]{1,0:T(8,128)(2,1)}, bf16[96,2048]{1,0:T(8,128)(2,1)S(1)}, u32[]{:S(2)}, u32[]{:S(2)}) collective-permute-start(bf16[96,2048]{1,0:T(8,128)(2,1)} %get-tuple-element.31.refs_2_), channel_id=1, source_target_pairs={{0,1},{1,0},{2,3},{3,2},{4,5},{5,4},{6,7},{7,6},{8,9},{9,8},{10,11... | collective-permute-start | bytes 1179656 | tf_op jit(solution)/shard_map/ppermute | solution.py:35
  19.5 28.5 %copy-start.5 = (bf16[96,2048]{1,0:T(8,128)(2,1)}, bf16[96,2048]{1,0:T(8,128)(2,1)S(1)}, u32[]{:S(2)}) copy-start(bf16[96,2048]{1,0:T(8,128)(2,1)S(1)} %collective-permute-done.12.refs_3_) | copy-start | bytes 1179652
  19.5 33.1 %collective-permute-start.16 = (bf16[96,2048]{1,0:T(8,128)(2,1)S(1)}, bf16[96,2048]{1,0:T(8,128)(2,1)S(1)}, u32[]{:S(2)}, u32[]{:S(2)}) collective-permute-start(bf16[96,2048]{1,0:T(8,128)(2,1)S(1)} %collective-permute-done.12.refs_3_), channel_id=1, source_target_pairs={{0,1},{1,0},{2,3},{3,2},{4,5},{5,4},{6,7},{7,6},{8,9},{9,8},{10,11... | collective-permute-start | bytes 1179656 | tf_op jit(solution)/shard_map/ppermute | solution.py:35
  28.6 19.5 %copy-start.6 = (bf16[96,2048]{1,0:T(8,128)(2,1)}, bf16[96,2048]{1,0:T(8,128)(2,1)S(1)}, u32[]{:S(2)}) copy-start(bf16[96,2048]{1,0:T(8,128)(2,1)S(1)} %collective-permute-done.13.refs_4_) | copy-start | bytes 1179652
  28.6 24.0 %collective-permute-start.17 = (bf16[96,2048]{1,0:T(8,128)(2,1)S(1)}, bf16[96,2048]{1,0:T(8,128)(2,1)S(1)}, u32[]{:S(2)}, u32[]{:S(2)}) collective-permute-start(bf16[96,2048]{1,0:T(8,128)(2,1)S(1)} %collective-permute-done.13.refs_4_), channel_id=1, source_target_pairs={{0,1},{1,0},{2,3},{3,2},{4,5},{5,4},{6,7},{7,6},{8,9},{9,8},{10,11... | collective-permute-start | bytes 1179656 | tf_op jit(solution)/shard_map/ppermute | solution.py:35
  28.6 19.5 %copy-start.7 = (bf16[96,2048]{1,0:T(8,128)(2,1)}, bf16[96,2048]{1,0:T(8,128)(2,1)S(1)}, u32[]{:S(2)}) copy-start(bf16[96,2048]{1,0:T(8,128)(2,1)S(1)} %collective-permute-done.14.refs_5_) | copy-start | bytes 1179652
  28.6 24.1 %collective-permute-start.18 = (bf16[96,2048]{1,0:T(8,128)(2,1)S(1)}, bf16[96,2048]{1,0:T(8,128)(2,1)S(1)}, u32[]{:S(2)}, u32[]{:S(2)}) collective-permute-start(bf16[96,2048]{1,0:T(8,128)(2,1)S(1)} %collective-permute-done.14.refs_5_), channel_id=1, source_target_pairs={{0,1},{1,0},{2,3},{3,2},{4,5},{5,4},{6,7},{7,6},{8,9},{9,8},{10,11... | collective-permute-start | bytes 1179656 | tf_op jit(solution)/shard_map/ppermute | solution.py:35
  31.5 4.5 %collective-permute-start = (f32[136,128]{1,0:T(8,128)}, f32[136,128]{1,0:T(8,128)S(1)}, u32[]{:S(2)}, u32[]{:S(2)}) collective-permute-start(f32[136,128]{1,0:T(8,128)} %get-tuple-element.26.refs_0_), channel_id=1, source_target_pairs={{0,8},{8,0},{16,24},{24,16},{1,9},{9,1},{17,25},{25,17},{2,10},{10... | collective-permute-start | bytes 208904 | tf_op jit(solution)/shard_map/ppermute | solution.py:35
  36.0 12.1 %copy-start.13 = (f32[136,128]{1,0:T(8,128)}, f32[136,128]{1,0:T(8,128)S(1)}, u32[]{:S(2)}) copy-start(f32[136,128]{1,0:T(8,128)S(1)} %collective-permute-done.refs_1_) | copy-start | bytes 208900
  36.0 4.5 %collective-permute-start.1 = (f32[136,128]{1,0:T(8,128)}, f32[136,128]{1,0:T(8,128)S(1)}, u32[]{:S(2)}, u32[]{:S(2)}) collective-permute-start(f32[136,128]{1,0:T(8,128)} %get-tuple-element.26.refs_0_), channel_id=1, source_target_pairs={{0,16},{8,24},{16,0},{24,8},{1,17},{9,25},{17,1},{25,9},{2,18},{10... | collective-permute-start | bytes 208904 | tf_op jit(solution)/shard_map/ppermute | solution.py:35
  40.5 7.6 %copy-start.14 = (f32[136,128]{1,0:T(8,128)}, f32[136,128]{1,0:T(8,128)S(1)}, u32[]{:S(2)}) copy-start(f32[136,128]{1,0:T(8,128)S(1)} %collective-permute-done.1.refs_2_) | copy-start | bytes 208900
  40.5 7.5 %collective-permute-start.2 = (f32[136,128]{1,0:T(8,128)}, f32[136,128]{1,0:T(8,128)S(1)}, u32[]{:S(2)}, u32[]{:S(2)}) collective-permute-start(f32[136,128]{1,0:T(8,128)} %get-tuple-element.26.refs_0_), channel_id=1, source_target_pairs={{0,24},{8,16},{16,8},{24,0},{1,25},{9,17},{17,9},{25,1},{2,26},{10... | collective-permute-start | bytes 208904 | tf_op jit(solution)/shard_map/ppermute | solution.py:35
  48.1 0.6 copy-start.15
  52.6 0.8 copy-start.8
  52.6 0.9 copy-start.9
  52.6 1.0 copy-start.10
  53.6 0.7 copy-start.11
  63.4 5.1 %copy-start.1 = (bf16[1024,256]{1,0:T(8,128)(2,1)S(1)}, bf16[1024,256]{1,0:T(8,128)(2,1)}, u32[]{:S(2)}) copy-start(bf16[1024,256]{1,0:T(8,128)(2,1)} %cell_finish.1.refs_1_) | copy-start | bytes 1572868
  63.5 9.6 %collective-permute-start.19 = (bf16[384,2048]{1,0:T(8,128)(2,1)}, bf16[384,2048]{1,0:T(8,128)(2,1)S(1)}, u32[]{:S(2)}, u32[]{:S(2)}) collective-permute-start(bf16[384,2048]{1,0:T(8,128)(2,1)} %get-tuple-element.36), channel_id=1, source_target_pairs={{0,1},{1,0},{2,3},{3,2},{4,5},{5,4},{6,7},{7,6},{8,9},{9,8},{10,11... | collective-permute-start | bytes 4718600 | tf_op jit(solution)/shard_map/ppermute | solution.py:35
  63.5 69.0 %all-to-all-start = ((bf16[8,128,512]{2,1,0:T(8,128)(2,1)}), bf16[8,128,512]{2,1,0:T(8,128)(2,1)S(1)}, u32[]{:S(2)}, u32[]{:S(2)}) async-start(bf16[8,128,512]{2,1,0:T(8,128)(2,1)} %get-tuple-element.30), calls=%async_computation | async-start | bytes 2097152 | tf_op jit(solution)/shard_map/all_to_all | solution.py:708
  68.6 38.0 %collective-permute-start.4 = (bf16[1024,256]{1,0:T(8,128)(2,1)S(1)}, bf16[1024,256]{1,0:T(8,128)(2,1)}, u32[]{:S(2)}, u32[]{:S(2)}) collective-permute-start(bf16[1024,256]{1,0:T(8,128)(2,1)S(1)} %copy-done.1), channel_id=1, source_target_pairs={{0,2},{1,3},{2,0},{3,1},{4,6},{5,7},{6,4},{7,5},{8,10},{9,11},{10,... | collective-permute-start | bytes 1572872 | tf_op jit(solution)/shard_map/ppermute | solution.py:35
  70.6 59.0 %collective-permute-start.6 = (bf16[1024,256]{1,0:T(8,128)(2,1)S(1)}, bf16[1024,256]{1,0:T(8,128)(2,1)}, u32[]{:S(2)}, u32[]{:S(2)}) collective-permute-start(bf16[1024,256]{1,0:T(8,128)(2,1)S(1)} %copy-done.1), channel_id=1, source_target_pairs={{0,4},{1,5},{2,6},{3,7},{4,0},{5,1},{6,2},{7,3},{8,12},{9,13},{10,... | collective-permute-start | bytes 1572872 | tf_op jit(solution)/shard_map/ppermute | solution.py:35
  72.9 57.6 %collective-permute-start.8 = (bf16[1024,256]{1,0:T(8,128)(2,1)S(1)}, bf16[1024,256]{1,0:T(8,128)(2,1)}, u32[]{:S(2)}, u32[]{:S(2)}) collective-permute-start(bf16[1024,256]{1,0:T(8,128)(2,1)S(1)} %copy-done.1), channel_id=1, source_target_pairs={{0,6},{1,7},{2,4},{3,5},{4,2},{5,3},{6,0},{7,1},{8,14},{9,15},{10,... | collective-permute-start | bytes 1572872 | tf_op jit(solution)/shard_map/ppermute | solution.py:35
  73.0 59.6 %collective-permute-start.3 = (bf16[1024,256]{1,0:T(8,128)(2,1)S(1)}, bf16[1024,256]{1,0:T(8,128)(2,1)}, u32[]{:S(2)}, u32[]{:S(2)}) collective-permute-start(bf16[1024,256]{1,0:T(8,128)(2,1)S(1)} %copy-done.1), channel_id=1, source_target_pairs={{0,1},{1,0},{2,3},{3,2},{4,5},{5,4},{6,7},{7,6},{8,9},{9,8},{10,11... | collective-permute-start | bytes 1572872 | tf_op jit(solution)/shard_map/ppermute | solution.py:35
  73.0 1.2 copy-start.2
  85.1 65.2 %copy-start.16 = (s32[8,128]{1,0:T(8,128)S(1)}, s32[8,128]{1,0:T(8,128)}, u32[]{:S(2)}) copy-start(s32[8,128]{1,0:T(8,128)} %get-tuple-element.25.refs_0_) | copy-start | bytes 12292
  85.1 65.9 %copy-start.17 = (f32[128,2]{0,1:T(2,128)S(1)}, f32[128,2]{0,1:T(2,128)}, u32[]{:S(2)}) copy-start(f32[128,2]{0,1:T(2,128)} %param.29) | copy-start | bytes 3076
  85.1 64.7 %collective-permute-start.23 = (bf16[128,2048]{1,0:T(8,128)(2,1)}, bf16[128,2048]{1,0:T(8,128)(2,1)S(1)}, u32[]{:S(2)}, u32[]{:S(2)}) collective-permute-start(bf16[128,2048]{1,0:T(8,128)(2,1)} %get-tuple-element.43), channel_id=1, source_target_pairs={{0,1},{1,0},{2,3},{3,2},{4,5},{5,4},{6,7},{7,6},{8,9},{9,8},{10,11... | collective-permute-start | bytes 1572872 | tf_op jit(solution)/shard_map/ppermute | solution.py:35
  106.6 26.1 %collective-permute-start.20 = (bf16[96,2048]{1,0:T(8,128)(2,1)}, bf16[96,2048]{1,0:T(8,128)(2,1)S(1)}, u32[]{:S(2)}, u32[]{:S(2)}) collective-permute-start(bf16[96,2048]{1,0:T(8,128)(2,1)} %get-tuple-element.38), channel_id=1, source_target_pairs={{0,8},{8,0},{16,24},{24,16},{1,9},{9,1},{17,25},{25,17},{2,10},{10... | collective-permute-start | bytes 1179656 | tf_op jit(solution)/shard_map/ppermute | solution.py:35
  129.5 18.7 %collective-permute-start.21 = (bf16[96,2048]{1,0:T(8,128)(2,1)}, bf16[96,2048]{1,0:T(8,128)(2,1)}, u32[]{:S(2)}, u32[]{:S(2)}) collective-permute-start(bf16[96,2048]{1,0:T(8,128)(2,1)} %get-tuple-element.39), channel_id=1, source_target_pairs={{0,16},{8,24},{16,0},{24,8},{1,17},{9,25},{17,1},{25,9},{2,18},{10... | collective-permute-start | bytes 1179656 | tf_op jit(solution)/shard_map/ppermute | solution.py:35
  130.5 17.8 %collective-permute-start.22 = (bf16[96,2048]{1,0:T(8,128)(2,1)}, bf16[96,2048]{1,0:T(8,128)(2,1)}, u32[]{:S(2)}, u32[]{:S(2)}) collective-permute-start(bf16[96,2048]{1,0:T(8,128)(2,1)} %get-tuple-element.40), channel_id=1, source_target_pairs={{0,24},{8,16},{16,8},{24,0},{1,25},{9,17},{17,9},{25,1},{2,26},{10... | collective-permute-start | bytes 1179656 | tf_op jit(solution)/shard_map/ppermute | solution.py:35
  132.5 23.0 %copy-start = (bf16[8,128,512]{2,1,0:T(8,128)(2,1)}, bf16[8,128,512]{2,1,0:T(8,128)(2,1)S(1)}, u32[]{:S(2)}) copy-start(bf16[8,128,512]{2,1,0:T(8,128)(2,1)S(1)} %all-to-all-done.refs_9_) | copy-start | bytes 3145732
  132.6 22.9 %collective-permute-start.5 = (bf16[1024,256]{1,0:T(8,128)(2,1)}, bf16[1024,256]{1,0:T(8,128)(2,1)S(1)}, u32[]{:S(2)}, u32[]{:S(2)}) collective-permute-start(bf16[1024,256]{1,0:T(8,128)(2,1)} %collective-permute-done.4.refs_3_), channel_id=1, source_target_pairs={{0,1},{1,0},{2,3},{3,2},{4,5},{5,4},{6,7},{7,6},{8,9},{9,8},{10,11... | collective-permute-start | bytes 1572872 | tf_op jit(solution)/shard_map/ppermute | solution.py:35
  132.7 19.7 %copy-start.4 = (bf16[96,2048]{1,0:T(8,128)(2,1)}, bf16[96,2048]{1,0:T(8,128)(2,1)S(1)}, u32[]{:S(2)}) copy-start(bf16[96,2048]{1,0:T(8,128)(2,1)S(1)} %collective-permute-done.20.refs_2_) | copy-start | bytes 1179652
  132.7 27.2 %collective-permute-start.7 = (bf16[1024,256]{1,0:T(8,128)(2,1)}, bf16[1024,256]{1,0:T(8,128)(2,1)}, u32[]{:S(2)}, u32[]{:S(2)}) collective-permute-start(bf16[1024,256]{1,0:T(8,128)(2,1)} %collective-permute-done.6.refs_5_), channel_id=1, source_target_pairs={{0,1},{1,0},{2,3},{3,2},{4,5},{5,4},{6,7},{7,6},{8,9},{9,8},{10,11... | collective-permute-start | bytes 1572872 | tf_op jit(solution)/shard_map/ppermute | solution.py:35
  148.3 12.0 %collective-permute-start.9 = (bf16[1024,256]{1,0:T(8,128)(2,1)}, bf16[1024,256]{1,0:T(8,128)(2,1)}, u32[]{:S(2)}, u32[]{:S(2)}) collective-permute-start(bf16[1024,256]{1,0:T(8,128)(2,1)} %collective-permute-done.8.refs_7_), channel_id=1, source_target_pairs={{0,1},{1,0},{2,3},{3,2},{4,5},{5,4},{6,7},{7,6},{8,9},{9,8},{10,11... | collective-permute-start | bytes 1572872 | tf_op jit(solution)/shard_map/ppermute | solution.py:35
  148.3 14.4 %collective-permute-start.10 = (bf16[4,128,512]{2,1,0:T(8,128)(2,1)S(1)}, bf16[4,128,512]{2,1,0:T(8,128)(2,1)}, u32[]{:S(2)}, u32[]{:S(2)}) collective-permute-start(bf16[4,128,512]{2,1,0:T(8,128)(2,1)S(1)} %get-tuple-element.49), channel_id=1, source_target_pairs={{0,8},{8,0},{16,24},{24,16},{1,9},{9,1},{17,25},{25,17},{2,10},{10... | collective-permute-start | bytes 1572872 | tf_op jit(solution)/shard_map/ppermute | solution.py:35
  149.8 2.6 %copy-start.3 = (bf16[128,2048]{1,0:T(8,128)(2,1)}, bf16[128,2048]{1,0:T(8,128)(2,1)S(1)}, u32[]{:S(2)}) copy-start(bf16[128,2048]{1,0:T(8,128)(2,1)S(1)} %collective-permute-done.23.refs_6_) | copy-start | bytes 1572868
  149.8 14.2 %collective-permute-start.11 = (bf16[4,128,512]{2,1,0:T(8,128)(2,1)S(1)}, bf16[4,128,512]{2,1,0:T(8,128)(2,1)}, u32[]{:S(2)}, u32[]{:S(2)}) collective-permute-start(bf16[4,128,512]{2,1,0:T(8,128)(2,1)S(1)} %get-tuple-element.48), channel_id=1, source_target_pairs={{0,16},{8,24},{16,0},{24,8},{1,17},{9,25},{17,1},{25,9},{2,18},{10... | collective-permute-start | bytes 1572872 | tf_op jit(solution)/shard_map/ppermute | solution.py:35
  155.5 8.4 %copy-start.18 = (bf16[1024,256]{1,0:T(8,128)(2,1)}, bf16[1024,256]{1,0:T(8,128)(2,1)S(1)}, u32[]{:S(2)}) copy-start(bf16[1024,256]{1,0:T(8,128)(2,1)S(1)} %collective-permute-done.5.refs_4_) | copy-start | bytes 1572868
  155.5 16.4 %collective-permute-start.24 = (bf16[128,512]{1,0:T(8,128)(2,1)}, bf16[128,512]{1,0:T(8,128)(2,1)S(1)}, u32[]{:S(2)}, u32[]{:S(2)}) collective-permute-start(bf16[128,512]{1,0:T(8,128)(2,1)} %get-tuple-element.45), channel_id=1, source_target_pairs={{0,2},{1,3},{2,0},{3,1},{4,6},{5,7},{6,4},{7,5},{8,10},{9,11},{10,... | collective-permute-start | bytes 393224 | tf_op jit(solution)/shard_map/ppermute | solution.py:35
  159.9 12.0 %collective-permute-start.25 = (bf16[128,512]{1,0:T(8,128)(2,1)}, bf16[128,512]{1,0:T(8,128)(2,1)S(1)}, u32[]{:S(2)}, u32[]{:S(2)}) collective-permute-start(bf16[128,512]{1,0:T(8,128)(2,1)} %get-tuple-element.46), channel_id=1, source_target_pairs={{0,4},{1,5},{2,6},{3,7},{4,0},{5,1},{6,2},{7,3},{8,12},{9,13},{10,... | collective-permute-start | bytes 393224 | tf_op jit(solution)/shard_map/ppermute | solution.py:35
  160.3 11.6 %copy-start.12 = (bf16[128,512]{1,0:T(8,128)(2,1)S(1)}, bf16[128,512]{1,0:T(8,128)(2,1)}, u32[]{:S(2)}) copy-start(bf16[128,512]{1,0:T(8,128)(2,1)} %get-tuple-element.44) | copy-start | bytes 393220
  160.3 11.6 %collective-permute-start.26 = (bf16[128,512]{1,0:T(8,128)(2,1)}, bf16[128,512]{1,0:T(8,128)(2,1)S(1)}, u32[]{:S(2)}, u32[]{:S(2)}) collective-permute-start(bf16[128,512]{1,0:T(8,128)(2,1)} %get-tuple-element.47), channel_id=1, source_target_pairs={{0,6},{1,7},{2,4},{3,5},{4,2},{5,3},{6,0},{7,1},{8,14},{9,15},{10,... | collective-permute-start | bytes 393224 | tf_op jit(solution)/shard_map/ppermute | solution.py:35

commit v2 on v1

--- a/solution.py
+++ b/solution.py
@@ -19,7 +19,7 @@
 BF16 = jnp.bfloat16
 
 
-def params(limit_mib=56, semantics=None):
+def params(limit_mib=16, semantics=None):
     return pltpu.CompilerParams(vmem_limit_bytes=limit_mib << 20, dimension_semantics=semantics)
 
 
@@ -33,6 +33,10 @@
 
 def swap(x, axis, k):
     return lax.ppermute(x, axis, xor_pairs(lax.axis_size(axis), k))
+
+
+def put(xs, space):
+    return [pltpu.with_memory_space_constraint(x, space) for x in xs]
 
 
 def dot(a, b):
@@ -140,23 +144,29 @@
         c.wait()
 
 
-def gated(x, gate_buf, up_buf, arrivals, chunk):
+def gated(left_of, gate_buf, up_buf, arrivals, chunk):
     g = u = None
     for i, waiting in enumerate(arrivals):
         wait_all(waiting)
         rows = slice(i * chunk, (i + 1) * chunk)
-        left = x[:, rows]
+        left = left_of(i)
         g_part, u_part = dot(left, gate_buf[rows, :]), dot(left, up_buf[rows, :])
         g = g_part if g is None else g + g_part
         u = u_part if u is None else u + u_part
     return (g * jax.nn.sigmoid(g) * u).astype(BF16)
 
 
-def expert_kernel(core_idx, *refs, n_ep, n_z, chunk):
+def block_at(n, n_z, top, side, pair):
+    near = n // (n_z // 2)
+    block = (top ^ (1 - near)) * (n_z // 2) + n % (n_z // 2)
+    return pl.ds(pl.multiple_of((2 * block + side) * pair, LANES), pair)
+
+
+def expert_kernel(idx, *refs, n_ep, n_z, chunk):
     own, other, rest = refs[:n_ep], refs[n_ep : 2 * n_ep], refs[2 * n_ep :]
-    gate, up, down, send, hidden, x, gate_buf, up_buf, down_buf, stage, sems = rest
-    core = core_idx[0]
-    cap, half = own[0].shape
+    gate, up, down, send_a, send_b, hidden, gate_buf, up_buf, down_buf, stage, sems = rest
+    core, top = idx[0], idx[1]
+    _, half = own[0].shape
     pair = down_buf.shape[1] // n_z
     count = iter(range(sems.shape[0]))
 
@@ -165,39 +175,42 @@
 
     per_half = half // chunk
     arrivals = []
-    for h, group in enumerate((own, other)):
-        lhs = start_all(
-            [
-                copy(r, x.at[pl.ds(k * cap, cap), pl.ds(h * half, half)])
-                for k, r in enumerate(group)
-            ]
-        )
+    for h in range(2):
         for i in range(per_half):
             src = pl.ds(pl.multiple_of((core ^ h) * half + i * chunk, chunk), chunk)
             dst = pl.ds(h * half + i * chunk, chunk)
-            weights = start_all(
-                [
-                    copy(gate.at[0, src, :], gate_buf.at[dst, :]),
-                    copy(up.at[0, src, :], up_buf.at[dst, :]),
-                ]
+            arrivals.append(
+                start_all(
+                    [
+                        copy(gate.at[0, src, :], gate_buf.at[dst, :]),
+                        copy(up.at[0, src, :], up_buf.at[dst, :]),
+                    ]
+                )
             )
-            arrivals.append((lhs if i == 0 else []) + weights)
     tail = start_all(
         [
             copy(
-                down.at[0, :, pl.ds(pl.multiple_of((2 * n + 1 - core) * pair, LANES), pair)],
+                down.at[0, :, block_at(n, n_z, top, 1 - core, pair)],
                 down_buf.at[:, pl.ds(n * pair, pair)],
             )
             for n in range(n_z)
         ]
     )
-    hidden[...] = gated(x, gate_buf, up_buf, arrivals, chunk)
+
+    def rows_of(i):
+        group = own if i < per_half else other
+        cols = slice(i % per_half * chunk, (i % per_half + 1) * chunk)
+        return jnp.concatenate([r[:, cols] for r in group], axis=0)
+
+    hidden[...] = gated(rows_of, gate_buf, up_buf, arrivals, chunk)
     leaving = []
     for n in range(n_z):
         tail[n].wait()
         cols = pl.ds(n * pair, pair)
         stage[:, cols] = dot(hidden[...], down_buf[:, cols]).astype(BF16)
-        leaving += start_all([copy(stage.at[:, cols], send.at[:, cols])])
+        send = (send_a, send_b)[n // (n_z // 2)]
+        there = pl.ds(n % (n_z // 2) * pair, pair)
+        leaving += start_all([copy(stage.at[:, cols], send.at[:, there])])
     wait_all(leaving)
 
 
@@ -207,7 +220,7 @@
     rows = n_ep * cap
     width, hid = gate.shape[-2:]
     chunk = 512
-    n_sems = 2 * n_ep + 2 * (width // chunk) + 2 * n_z
+    n_sems = 2 * (width // chunk) + 2 * n_z
     hbm = pl.BlockSpec(memory_space=pl.ANY)
     vm = pl.BlockSpec(memory_space=pltpu.VMEM)
     return pl.pallas_call(
@@ -215,41 +228,42 @@
             functools.partial(expert_kernel, n_ep=n_ep, n_z=n_z, chunk=chunk), len(deps), 1
         ),
         out_shape=[
-            jax.ShapeDtypeStruct((rows, half), BF16),
+            jax.ShapeDtypeStruct((rows, half // 2), BF16),
+            jax.ShapeDtypeStruct((rows, half // 2), BF16),
             jax.ShapeDtypeStruct((rows, hid), BF16),
         ],
-        in_specs=[pl.BlockSpec(memory_space=pltpu.SMEM)] + anywhere(deps) + [hbm] * (2 * n_ep + 3),
-        out_specs=[hbm, vm],
+        in_specs=[pl.BlockSpec(memory_space=pltpu.SMEM)] + anywhere(deps) + [vm] * (2 * n_ep) + [hbm] * 3,
+        out_specs=[hbm, hbm, vm],
         scratch_shapes=[
-            pltpu.VMEM((rows, width), BF16),
             pltpu.VMEM((width, hid), BF16),
             pltpu.VMEM((width, hid), BF16),
             pltpu.VMEM((hid, half), BF16),
             pltpu.VMEM((rows, half), BF16),
             pltpu.SemaphoreType.DMA((n_sems,)),
         ],
-        compiler_params=params(),
+        compiler_params=params(36),
         cost_estimate=cost(5 * rows * width * hid, 5 * width * hid + 4 * rows * width),
         name="expert",
     )(core_idx, *deps, *own, *other, gate, up, down)
 
 
-def pair_kernel(core_idx, hidden, got, down, *refs, n_z):
+def pair_kernel(idx, hidden, got, down, *refs, n_z, part):
     back, down_buf, sems = refs[:-2], refs[-2], refs[-1]
-    core = core_idx[0]
-    cap, half = back[0].shape
-    pair = half // n_z
+    core, top = idx[0], idx[1]
+    cap, width = back[0].shape
+    n_here = n_z // 2
+    pair = width // n_here
     copies = start_all(
         [
             pltpu.make_async_copy(
-                down.at[0, :, pl.ds(pl.multiple_of((2 * n + core) * pair, LANES), pair)],
+                down.at[0, :, block_at(part * n_here + n, n_z, top, core, pair)],
                 down_buf.at[:, pl.ds(n * pair, pair)],
                 sems.at[n],
             )
-            for n in range(n_z)
+            for n in range(n_here)
         ]
     )
-    for n in range(n_z):
+    for n in range(n_here):
         copies[n].wait()
         cols = pl.ds(n * pair, pair)
         both = (dot(hidden[...], down_buf[:, cols]) + got[:, cols].astype(F32)).astype(BF16)
@@ -257,21 +271,21 @@
             out[:, cols] = both[k * cap : (k + 1) * cap, :]
 
 
-def pair_sum(core_idx, hidden, got, down, n_ep, n_z, deps=()):
-    rows, half = got.shape
+def pair_sum(idx, hidden, got, down, n_ep, n_z, part, deps=()):
+    rows, width = got.shape
     hid = hidden.shape[1]
     hbm = pl.BlockSpec(memory_space=pl.ANY)
     vm = pl.BlockSpec(memory_space=pltpu.VMEM)
     return pl.pallas_call(
-        with_deps(functools.partial(pair_kernel, n_z=n_z), len(deps), 1),
-        out_shape=[jax.ShapeDtypeStruct((rows // n_ep, half), BF16) for _ in range(n_ep)],
+        with_deps(functools.partial(pair_kernel, n_z=n_z, part=part), len(deps), 1),
+        out_shape=[jax.ShapeDtypeStruct((rows // n_ep, width), BF16) for _ in range(n_ep)],
         in_specs=[pl.BlockSpec(memory_space=pltpu.SMEM)] + anywhere(deps) + [vm, vm, hbm],
         out_specs=[vm] * n_ep,
-        scratch_shapes=[pltpu.VMEM((hid, half), BF16), pltpu.SemaphoreType.DMA((n_z,))],
+        scratch_shapes=[pltpu.VMEM((hid, width), BF16), pltpu.SemaphoreType.DMA((n_z // 2,))],
         compiler_params=params(),
-        cost_estimate=cost(2 * rows * hid * half, 2 * hid * half + 4 * rows * half),
+        cost_estimate=cost(2 * rows * hid * width, 2 * hid * width + 4 * rows * width),
         name="pair_sum",
-    )(core_idx, *deps, hidden, got, down)
+    )(idx, *deps, hidden, got, down)
 
 
 def shared_kernel(core_idx, x, gate, up, down, send, own, gate_buf, up_buf, down_buf, sems, *, n_z, chunk):
@@ -292,7 +306,9 @@
             )
         )
     tail = start_all([copy(down, down_buf)])
-    hidden = gated(x, gate_buf, up_buf, arrivals, chunk)
+    hidden = gated(
+        lambda i: x[:, i * chunk : (i + 1) * chunk], gate_buf, up_buf, arrivals, chunk
+    )
     wait_all(tail)
     for n in range(n_z):
         cols = pl.ds(n * pair, pair)
@@ -319,46 +335,52 @@
             pltpu.VMEM((hid, width), BF16),
             pltpu.SemaphoreType.DMA((2 * (width // chunk) + 1,)),
         ],
-        compiler_params=params(),
+        compiler_params=params(24),
         cost_estimate=cost(6 * rows * width * hid, 6 * width * hid + 4 * rows * width),
         name="shared",
     )(core_idx, *deps, x, gate, up, down)
 
 
-def combine_kernel(z_idx, *refs, n_ep, n_z, topk):
+def combine_kernel(z_idx, *refs, n_ep, n_z, topk, part):
     blocks, rest = refs[:n_ep], refs[n_ep:]
     shared_own, shared_other, dest, weight, outs = *rest[:4], rest[4:]
     z = z_idx[0]
     cap = blocks[0].shape[0]
     n_rows, wide = outs[0].shape
+    n_here = n_z // 2
     spot = lax.broadcasted_iota(jnp.int32, (n_rows, n_ep * cap), 1)
     picks = [(dest[:, k : k + 1] == spot).astype(F32).astype(BF16) for k in range(topk)]
     shares = [jnp.broadcast_to(weight[:, k : k + 1], (n_rows, wide)) for k in range(topk)]
-    for j in range(n_z):
-        cols = pl.ds(pl.multiple_of((z ^ j) * wide, LANES), wide)
-        back = jnp.concatenate([b[:, cols] for b in blocks], axis=0)
+    for j in range(n_here):
+        block = z ^ (j if part else j + n_here)
+        there = pl.ds(pl.multiple_of((block & (n_here - 1)) * wide, LANES), wide)
+        cols = pl.ds(pl.multiple_of(block * wide, LANES), wide)
+        back = jnp.concatenate([b[:, there] for b in blocks], axis=0)
         total = shared_own[:, cols].astype(F32) + shared_other[:, cols].astype(F32)
         for k in range(topk):
             total = total + shares[k] * dot(picks[k], back)
         outs[j][...] = total.astype(BF16)
 
 
-def combine(z_idx, blocks, shared_own, shared_other, dest, weight, n_z, deps=()):
+def combine(z_idx, blocks, shared_own, shared_other, dest, weight, n_z, part, deps=()):
     n_rows, half = shared_own.shape
     cap = blocks[0].shape[0]
     topk = weight.shape[1]
+    n_here = n_z // 2
     vm = pl.BlockSpec(memory_space=pltpu.VMEM)
     return pl.pallas_call(
         with_deps(
-            functools.partial(combine_kernel, n_ep=len(blocks), n_z=n_z, topk=topk), len(deps), 1
+            functools.partial(combine_kernel, n_ep=len(blocks), n_z=n_z, topk=topk, part=part),
+            len(deps),
+            1,
         ),
-        out_shape=[jax.ShapeDtypeStruct((n_rows, half // n_z), BF16) for _ in range(n_z)],
+        out_shape=[jax.ShapeDtypeStruct((n_rows, half // n_z), BF16) for _ in range(n_here)],
         in_specs=[pl.BlockSpec(memory_space=pltpu.SMEM)]
         + anywhere(deps)
         + [vm] * (len(blocks) + 4),
-        out_specs=[vm] * n_z,
+        out_specs=[vm] * n_here,
         compiler_params=params(),
-        cost_estimate=cost(2 * topk * n_rows * len(blocks) * cap * half, 4 * n_rows * half),
+        cost_estimate=cost(topk * n_rows * len(blocks) * cap * half, 2 * n_rows * half),
         name="combine",
     )(z_idx, *deps, *blocks, shared_own, shared_other, dest, weight)
 
@@ -592,39 +614,40 @@
     )(ep_idx, *deps, *packs, queries, out_gate, gain, inner, stats, rows)
 
 
-def project_kernel(idx, *refs, n_tp):
-    mixed, (share, low_part, high_part, out, joined, sems) = refs[:n_tp], refs[n_tp:]
+def project_kernel(idx, *refs, n_tp, block):
+    mixed, rest = refs[:n_tp], refs[n_tp:]
+    share, low_part, high_part, out, joined, stage, sems = rest
     me = idx[0]
     _, part, _ = share.shape
+    length = mixed[0].shape[0]
     half_tp = n_tp // 2
-
-    @pl.when(pl.program_id(0) == 0)
-    def _():
-        waits = []
-        for j in range(n_tp):
-            source = me ^ j
-            low = source < half_tp
-            bit = jnp.where(low, idx[1], idx[2])
-            for h in range(2):
-                first = pl.multiple_of(j * 2 * part + (bit ^ h) * part, part)
-                dst, sem = joined.at[pl.ds(first, part), :], sems.at[2 * j + h]
-                if h == 0:
-                    pltpu.make_async_copy(share.at[source], dst, sem).start()
-                else:
-
-                    @pl.when(low)
-                    def _():
-                        pltpu.make_async_copy(low_part.at[source], dst, sem).start()
-
-                    @pl.when(jnp.logical_not(low))
-                    def _():
-                        pltpu.make_async_copy(high_part.at[source - half_tp], dst, sem).start()
-
-                waits.append(pltpu.make_async_copy(share.at[source], dst, sem))
-        wait_all(waits)
-
-    lhs = jnp.concatenate([m[...] for m in mixed], axis=1)
-    out[...] = dot(lhs, joined[...]).astype(BF16)
+    for j in range(n_tp):
+        source = me ^ j
+        low = source < half_tp
+        bit = jnp.where(low, idx[1], idx[2])
+        first = j * 2 * part
+        here = pl.ds(pl.multiple_of(first + bit * part, part), part)
+        there = pl.ds(pl.multiple_of(first + (bit ^ 1) * part, part), part)
+        joined[here, :] = share[source]
+
+        @pl.when(low)
+        def _():
+            joined[there, :] = low_part[source]
+
+        @pl.when(jnp.logical_not(low))
+        def _():
+            joined[there, :] = high_part[source - half_tp]
+
+    leaving = []
+    for b in range(length // block):
+        rows = slice(b * block, (b + 1) * block)
+        lhs = jnp.concatenate([m[rows, :] for m in mixed], axis=1)
+        stage[rows, :] = dot(lhs, joined[...]).astype(BF16)
+        span = pl.ds(b * block, block)
+        leaving += start_all(
+            [pltpu.make_async_copy(stage.at[span, :], out.at[span, :], sems.at[b])]
+        )
+    wait_all(leaving)
 
 
 def project(idx, mixed, share, low_part, high_part, deps=()):
@@ -632,22 +655,19 @@
     n_tp = len(mixed)
     cols = share.shape[-1]
     block = 256
+    hbm = pl.BlockSpec(memory_space=pl.ANY)
+    vm = pl.BlockSpec(memory_space=pltpu.VMEM)
     return pl.pallas_call(
-        with_deps(functools.partial(project_kernel, n_tp=n_tp), len(deps), 1),
+        with_deps(functools.partial(project_kernel, n_tp=n_tp, block=block), len(deps), 1),
         out_shape=jax.ShapeDtypeStruct((length, cols), BF16),
-        grid_spec=pltpu.PrefetchScalarGridSpec(
-            num_scalar_prefetch=1,
-            grid=(length // block,),
-            in_specs=anywhere(deps)
-            + [pl.BlockSpec((block, own), lambda i, idx: (i, 0)) for _ in mixed]
-            + anywhere((share, low_part, high_part)),
-            out_specs=pl.BlockSpec((block, cols), lambda i, idx: (i, 0)),
-            scratch_shapes=[
-                pltpu.VMEM((n_tp * own, cols), BF16),
-                pltpu.SemaphoreType.DMA((2 * n_tp,)),
-            ],
-        ),
-        compiler_params=params(semantics=("arbitrary",)),
+        in_specs=[pl.BlockSpec(memory_space=pltpu.SMEM)] + anywhere(deps) + [vm] * (n_tp + 3),
+        out_specs=hbm,
+        scratch_shapes=[
+            pltpu.VMEM((n_tp * own, cols), BF16),
+            pltpu.VMEM((length, cols), BF16),
+            pltpu.SemaphoreType.DMA((length // block,)),
+        ],
+        compiler_params=params(20),
         cost_estimate=cost(2 * length * n_tp * own * cols, 2 * length * n_tp * own),
         name="project",
     )(idx, *deps, *mixed, share, low_part, high_part)
@@ -693,10 +713,10 @@
 
     normed, dest, share, outgoing = prep(
         idx,
-        moe_rows,
+        *put([moe_rows], pltpu.HBM),
         moe_gain.reshape(1, -1),
         routes.astype(jnp.int32).T,
-        out_weight,
+        *put([out_weight], pltpu.HBM),
         n_ep,
         n_tp,
         cap,
@@ -713,7 +733,7 @@
         packs.append(swap(pack, "ep", k))
     inner, stats = cell_intra(queries, keys, values, gate_info, heads, [pack])
     mixed = cell_finish(
-        ep_idx, packs, queries, out_gate, out_gain.reshape(1, -1), inner, stats, gate_info, heads
+        ep_idx, put(packs, pltpu.VMEM), queries, out_gate, out_gain.reshape(1, -1), inner, stats, gate_info, heads
     )
     gathered = [mixed]
     for k in range(1, n_z):
@@ -724,27 +744,50 @@
     others = []
     for a in arrived:
         others.append(swap(a, "tp", 1))
-    send, hidden = expert(
-        core_idx, arrived, others, expert_gate, expert_up, expert_down, n_z, [mixed]
-    )
-    got = swap(send, "tp", 1)
+    dest_cols = dest.T
+    weight_cols = route_weight * jnp.ones((1, 1), F32)
+    project_idx = jnp.stack([me_tp, low_bit, high_bit]).astype(jnp.int32)
+    half_idx = jnp.stack([core, me_z // (n_z // 2)]).astype(jnp.int32)
+    *sends, hidden = expert(
+        half_idx, put(arrived, pltpu.VMEM), put(others, pltpu.VMEM), *put([expert_gate, expert_up, expert_down], pltpu.HBM), n_z, [mixed]
+    )
+    got = []
+    for part in range(2):
+        got.append(swap(sends[part], "tp", 1))
+    backs, dep = [], hidden
+    for part in range(2):
+        sums = pair_sum(
+            half_idx, hidden, *put([got[part]], pltpu.VMEM), *put([expert_down], pltpu.HBM), n_ep, n_z, part, [dep]
+        )
+        dep = sums[0]
+        back = [sums[0]]
+        for k in range(1, n_ep):
+            back.append(swap(sums[k], "ep", k))
+        backs.append(back)
     low_part = swap(share[:half_tp], "ep", 1)
     high_part = swap(share[half_tp:], "ep", n_ep // 2)
-    sums = pair_sum(core_idx, hidden, got, expert_down, n_ep, n_z)
-    back = [sums[0]]
-    for k in range(1, n_ep):
-        back.append(swap(sums[k], "ep", k))
     shared_send, shared_own = shared(
-        core_idx, normed, shared_gate, shared_up, shared_down, n_z, [sums[0]]
+        core_idx,
+        normed,
+        *put([shared_gate, shared_up, shared_down], pltpu.HBM),
+        n_z,
+        [dep, dest_cols, weight_cols, project_idx],
     )
     shared_other = swap(shared_send, "tp", 1)
-    part_out = combine(z_idx, back, shared_own, shared_other, dest.T, route_weight, n_z)
-    total = part_out[0].astype(F32)
+    parts, total, dep = [None] * n_z, None, shared_own
+    for part in range(2):
+        outs = combine(
+            z_idx, put(backs[part], pltpu.VMEM), shared_own, *put([shared_other], pltpu.VMEM), dest_cols, weight_cols, n_z, part, [dep]
+        )
+        dep = outs[0]
+        first = 0 if part else n_z // 2
+        parts[first : first + n_z // 2] = outs
+    total = parts[0].astype(F32)
     for k in range(1, n_z):
-        total = total + swap(part_out[k], "tp", 2 * k).astype(F32)
+        total = total + swap(parts[k], "tp", 2 * k).astype(F32)
     moe_out = total.astype(BF16)
     mixer_out = project(
-        jnp.stack([me_tp, low_bit, high_bit]).astype(jnp.int32), pieces, share, low_part, high_part
+        project_idx, put(pieces, pltpu.VMEM), *put([share, low_part, high_part], pltpu.VMEM), [dep]
     )
     return (mixer_out, moe_out)
 

time: 173 us -> 156 us (0.902)
  Pallas kernels: 48.3 us -> 36.1 us
  waiting for transfers between devices: 83.5 us -> 73.2 us
  starting transfers between devices: 32.9 us -> 37.7 us
    ppermute x27 -> x31, waiting for transfers between devices: 83.5 us -> 73.2 us  [swap(): return lax.ppermute(x, axis, xor_pairs(lax.axis_size(axis), k))]
    ppermute x27 -> x31, starting transfers between devices: 27.8 us -> 32.9 us  [swap(): return lax.ppermute(x, axis, xor_pairs(lax.axis_size(axis), k))]
    pallas_call x2 -> x3, Pallas kernels: 13.2 us -> 10.4 us  [the longest x2 5.92 us: pair_sum(): pl.pallas_call(with_deps(functools.partial(pair_kernel, n_z=n_z, part=par...]
    pallas_call x1, Pallas kernels: 5.58 us -> 3.41 us  [shared(): pl.pallas_call(with_deps(functools.partial(shared_kernel, n_z=n_z, chunk=...]
    pallas_call x1 -> x2, Pallas kernels: 3.11 us -> 1 us  [combine(): pl.pallas_call(with_deps(functools.partial(combine_kernel, n_ep=len(block...]
    pallas_call x1, Pallas kernels: 6.03 us -> 4.17 us  [cell_intra(): pl.pallas_call(with_deps(functools.partial(intra_kernel, block=256, heads...]
    unnamed x39 -> x31, local copies, waits for them, and re-layouts: 4.27 us -> 4.74 us
  transfers between devices with their start and end apart: 28 -> 32, of which waited for: 9 -> 12; matrix products, arithmetic and copies ran while one was open for 1% -> 1% of each run, Pallas kernels for 20% -> 18%
where the time goes in v2:
time: 156 us; the launch traced here: 155 us
  waiting for transfers between devices  73.2 us (47%)
  starting transfers between devices  37.7 us (24%)
  Pallas kernels  36.1 us (23%)
  local copies, waits for them, and re-layouts  4.9 us (3%)
  other arithmetic  1.91 us (1%)
    ppermute x31, waiting for transfers between devices, swap(): return lax.ppermute(x, axis, xor_pairs(lax.axis_size(axis), k))  73.2 us
    ppermute x31, starting transfers between devices, swap(): return lax.ppermute(x, axis, xor_pairs(lax.axis_size(axis), k))  32.9 us
    pallas_call x1, Pallas kernels, expert(): pl.pallas_call(with_deps(functools.partial(expert_kernel, n_ep=n_ep, n_z=...  9.48 us
    pallas_call x2, Pallas kernels, pair_sum(): pl.pallas_call(with_deps(functools.partial(pair_kernel, n_z=n_z, part=par...  5.92 us
    all_to_all x1, starting transfers between devices, local(): share = lax.all_to_all(share, 'tp', 0, 0, tiled=True)  4.88 us
    unnamed x31, local copies, waits for them, and re-layouts  4.74 us
    pallas_call x1, Pallas kernels, project(): pl.pallas_call(with_deps(functools.partial(project_kernel, n_tp=n_tp, blo...  4.5 us
    pallas_call x1, Pallas kernels, cell_intra(): pl.pallas_call(with_deps(functools.partial(intra_kernel, block=256, heads...  4.17 us
  transfers between devices with their start and end apart: 32, of which 12 were waited for; matrix products, arithmetic and copies ran while one was open for 1% of the time, Pallas kernels for 18%

profile of v2, /device:TPU:0, one launch (start us, length us, event | category | flops | bytes accessed | tf_op | source)
XLA Modules:
  0.0 155.0 jit_solution(11976036418696482835)
XLA Ops:
  0.8 0.8 copy-done.9
  1.5 0.7 copy-done.12
  2.2 3.9 %prep.1 = (bf16[128,4096]{1,0:T(8,128)(2,1)S(1)}, s32[8,128]{1,0:T(8,128)S(1)}, bf16[8,128,512]{2,1,0:T(8,128)(2,1)}, bf16[96,2048]{1,0:T(8,128)(2,1)S(1)}, bf16...) custom-call(s32[3]{0:T(128)S(1)} %pad_add_fusion.2.refs_0_, ...), custom_call_target="tpu_custom_call" | custom-call | flops 201326592 | bytes 2097152 | tf_op jit(solution)/shard_map/prep/pallas_call | solution.py:120
  6.2 3.0 %collective-permute-start.3 = (bf16[96,2048]{1,0:T(8,128)(2,1)S(1)}, bf16[96,2048]{1,0:T(8,128)(2,1)}, u32[]{:S(2)}, u32[]{:S(2)}) collective-permute-start(bf16[96,2048]{1,0:T(8,128)(2,1)S(1)} %get-tuple-element.36), channel_id=1, source_target_pairs={{0,8},{8,0},{16,24},{24,16},{1,9},{9,1},{17,25},{25,17},{2,10},{10... | collective-permute-start | bytes 1179656 | tf_op jit(solution)/shard_map/ppermute | solution.py:35
  9.2 1.5 collective-permute-start.4
  10.7 8.5 %collective-permute-done.3.refs_3_ = bf16[96,2048]{1,0:T(8,128)(2,1)} collective-permute-done((bf16[96,2048]{1,0:T(8,128)(2,1)S(1)}, bf16[96,2048]{1,0:T(8,128)(2,1)}, u32[]{:S(2)}, u32[]{:S(2)}) %collective-permute-start.3) | collective-permute-done | bytes 393248 | tf_op jit(solution)/shard_map/ppermute | solution.py:35
  19.3 9.0 %collective-permute-done.4.refs_4_ = bf16[96,2048]{1,0:T(8,128)(2,1)} collective-permute-done((bf16[96,2048]{1,0:T(8,128)(2,1)S(1)}, bf16[96,2048]{1,0:T(8,128)(2,1)}, u32[]{:S(2)}, u32[]{:S(2)}) %collective-permute-start.4) | collective-permute-done | bytes 393248 | tf_op jit(solution)/shard_map/ppermute | solution.py:35
  28.3 0.5 collective-permute-start.9
  28.8 1.3 cell_state.1
  30.1 0.6 copy-done.7
  30.7 0.7 collective-permute-start
  31.4 3.8 %collective-permute-done.refs_1_ = f32[136,128]{1,0:T(8,128)S(1)} collective-permute-done((f32[136,128]{1,0:T(8,128)}, f32[136,128]{1,0:T(8,128)S(1)}, u32[]{:S(2)}, u32[]{:S(2)}) %collective-permute-start) | collective-permute-done | bytes 69664 | tf_op jit(solution)/shard_map/ppermute | solution.py:35
  35.2 0.6 copy-done.5
  35.8 1.5 collective-permute-start.1
  37.4 4.9 %all-to-all-start = ((bf16[8,128,512]{2,1,0:T(8,128)(2,1)}), bf16[8,128,512]{2,1,0:T(8,128)(2,1)S(1)}, u32[]{:S(2)}, u32[]{:S(2)}) async-start(bf16[8,128,512]{2,1,0:T(8,128)(2,1)} %get-tuple-element.55), calls=%async_computation | async-start | bytes 2097152 | tf_op jit(solution)/shard_map/all_to_all | solution.py:728
  42.3 1.0 collective-permute-start.2
  43.4 0.8 copy-done.8
  44.3 4.2 %cell_intra.1 = (f32[1024,256]{1,0:T(8,128)S(1)}, f32[16,1024]{1,0:T(8,128)S(1)}) custom-call(f32[136,128]{1,0:T(8,128)} %get-tuple-element.31.refs_0_, bf16[1024,128]{1,0:T(8,128)(2,1)S(1)} %copy-done.3, bf16[1024,128]{1,0:T(8,128)(2,1)S(1)} %copy-done.2, bf16[1024,256]{1,0:T(8,128)(2,1)S(1)} %copy-done, f32[16,1024]{1,0:T(8,128)S(1)} %copy-done.8), custom_call_target="tpu_custom_call" | custom-call | flops 402653184 | bytes 2097152 | tf_op jit(solution)/shard_map/cell_intra/pallas_call | solution.py:524
  48.5 1.0 copy-done.1
  49.5 2.4 %cell_finish.1.refs_1_.refs_2_ = bf16[1024,256]{1,0:T(8,128)(2,1)S(1)} custom-call(s32[1]{0:T(128)} %bitcast.6.refs_0_, f32[136,128]{1,0:T(8,128)S(1)} %copy-done.6, f32[136,128]{1,0:T(8,128)} %collective-permute-done.1.refs_2_, f32[136,128]{1,0:T(8,128)S(1)} %collective-permute-done.2.refs_3_, bf16[1024,128]{1,0:T(8,128)(2,1)S(1)} %copy-done.4, ...), custom_call_target="tpu_custom_call" | custom-call | flops 67108864 | bytes 3145728 | tf_op jit(solution)/shard_map/cell_finish/pallas_call | solution.py:603
  52.0 9.5 %expert.1 = (bf16[384,1024]{1,0:T(8,128)(2,1)}, bf16[384,1024]{1,0:T(8,128)(2,1)}, bf16[384,512]{1,0:T(8,128)(2,1)S(1)}) custom-call(s32[2]{0:T(128)S(1)} %pad_add_fusion.1.refs_0_, bf16[1024,256]{1,0:T(8,128)(2,1)S(1)} %cell_finish.1.refs_1_.refs_2_, bf16[96,2048]{1,0:T(8,128)(2,1)S(1)} %get-tuple-element.35.refs_2_, ...), custom_call_target="tpu_custom_call" | custom-call | flops 4026531840 | bytes 16777216 | tf_op jit(solution)/shard_map/expert/pallas_call | solution.py:226
  62.3 1.8 %collective-permute-done.10.refs_3_ = bf16[384,1024]{1,0:T(8,128)(2,1)} collective-permute-done((bf16[384,1024]{1,0:T(8,128)(2,1)}, bf16[384,1024]{1,0:T(8,128)(2,1)}, u32[]{:S(2)}, u32[]{:S(2)}) %collective-permute-start.10) | collective-permute-done | bytes 786464 | tf_op jit(solution)/shard_map/ppermute | solution.py:35
  64.2 3.0 %pair_sum.2 = (bf16[96,1024]{1,0:T(8,128)(2,1)S(1)}, bf16[96,1024]{1,0:T(8,128)(2,1)S(1)}, bf16[96,1024]{1,0:T(8,128)(2,1)S(1)}, bf16[96,1024]{1,0:T(8,128)(2,1)S(1)}) custom-call(s32[2]{0:T(128)S(1)} %pad_add_fusion.1.refs_0_, bf16[384,512]{1,0:T(8,128)(2,1)S(1)} %get-tuple-element.39.refs_1_.refs_2_, ...), custom_call_target="tpu_custom_call" | custom-call | flops 402653184 | bytes 2621440 | tf_op jit(solution)/shard_map/pair_sum/pallas_call | solution.py:279
  67.1 3.0 %pair_sum.3 = (bf16[96,1024]{1,0:T(8,128)(2,1)S(1)}, bf16[96,1024]{1,0:T(8,128)(2,1)S(1)}, bf16[96,1024]{1,0:T(8,128)(2,1)S(1)}, bf16[96,1024]{1,0:T(8,128)(2,1)S(1)}) custom-call(s32[2]{0:T(128)S(1)} %pad_add_fusion.1.refs_0_, bf16[96,1024]{1,0:T(8,128)(2,1)S(1)} %get-tuple-element.41.refs_1_.refs_2_, ...), custom_call_target="tpu_custom_call" | custom-call | flops 402653184 | bytes 2621440 | tf_op jit(solution)/shard_map/pair_sum/pallas_call | solution.py:279
  70.1 3.4 %shared.1 = (bf16[128,2048]{1,0:T(8,128)(2,1)S(1)}, bf16[128,2048]{1,0:T(8,128)(2,1)S(1)}) custom-call(s32[1]{0:T(128)} %bitcast.4.refs_0_, bf16[96,1024]{1,0:T(8,128)(2,1)S(1)} %get-tuple-element.43.refs_1_.refs_2_, s32[128,8]{1,0:T(8,128)S(1)} %bitcast.12, f32[128,2]{1,0:T(8,128)S(1)} %copy.21.refs_3_.refs_9_, s32[3]{0:T(128)S(1)} %pad_add_fusion.refs_4_.refs_0_, ...), custom_call_target="tpu_custom_call" | custom-call | flops 805306368 | bytes 8388608 | tf_op jit(solution)/shard_map/shared/pallas_call | solution.py:327
  73.8 1.0 collective-permute-start.12
  74.8 1.5 collective-permute-start.13
  76.3 1.0 collective-permute-start.14
  77.2 1.9 %collective-permute-start.20 = (bf16[1024,256]{1,0:T(8,128)(2,1)S(1)}, bf16[1024,256]{1,0:T(8,128)(2,1)S(1)}, u32[]{:S(2)}, u32[]{:S(2)}) collective-permute-start(bf16[1024,256]{1,0:T(8,128)(2,1)S(1)} %cell_finish.1.refs_1_.refs_2_), channel_id=1, source_target_pairs={{0,2},{1,3},{2,0},{3,1},{4,6},{5,7},{6,4},{7,5},{8,10},{9,11},{10,... | collective-permute-start | bytes 1572872 | tf_op jit(solution)/shard_map/ppermute | solution.py:35
  79.2 2.4 %collective-permute-done.12.refs_3_ = bf16[96,1024]{1,0:T(8,128)(2,1)S(1)} collective-permute-done((bf16[96,1024]{1,0:T(8,128)(2,1)S(1)}, bf16[96,1024]{1,0:T(8,128)(2,1)S(1)}, u32[]{:S(2)}, u32[]{:S(2)}) %collective-permute-start.12) | collective-permute-done | bytes 196640 | tf_op jit(solution)/shard_map/ppermute | solution.py:35
  81.5 2.8 %collective-permute-start.22 = (bf16[1024,256]{1,0:T(8,128)(2,1)S(1)}, bf16[1024,256]{1,0:T(8,128)(2,1)S(1)}, u32[]{:S(2)}, u32[]{:S(2)}) collective-permute-start(bf16[1024,256]{1,0:T(8,128)(2,1)S(1)} %cell_finish.1.refs_1_.refs_2_), channel_id=1, source_target_pairs={{0,4},{1,5},{2,6},{3,7},{4,0},{5,1},{6,2},{7,3},{8,12},{9,13},{10,... | collective-permute-start | bytes 1572872 | tf_op jit(solution)/shard_map/ppermute | solution.py:35
  84.4 1.5 collective-permute-done.13.refs_4_
  85.9 2.1 %collective-permute-start.17 = (bf16[96,1024]{1,0:T(8,128)(2,1)S(1)}, bf16[96,1024]{1,0:T(8,128)(2,1)S(1)}, u32[]{:S(2)}, u32[]{:S(2)}) collective-permute-start(bf16[96,1024]{1,0:T(8,128)(2,1)S(1)} %get-tuple-element.52), channel_id=1, source_target_pairs={{0,16},{8,24},{16,0},{24,8},{1,17},{9,25},{17,1},{25,9},{2,18},{10... | collective-permute-start | bytes 589832 | tf_op jit(solution)/shard_map/ppermute | solution.py:35
  87.9 3.6 %collective-permute-done.16.refs_3_ = bf16[96,1024]{1,0:T(8,128)(2,1)S(1)} collective-permute-done((bf16[96,1024]{1,0:T(8,128)(2,1)S(1)}, bf16[96,1024]{1,0:T(8,128)(2,1)S(1)}, u32[]{:S(2)}, u32[]{:S(2)}) %collective-permute-start.16) | collective-permute-done | bytes 196640 | tf_op jit(solution)/shard_map/ppermute | solution.py:35
  91.5 3.4 %collective-permute-start.24 = (bf16[1024,256]{1,0:T(8,128)(2,1)S(1)}, bf16[1024,256]{1,0:T(8,128)(2,1)}, u32[]{:S(2)}, u32[]{:S(2)}) collective-permute-start(bf16[1024,256]{1,0:T(8,128)(2,1)S(1)} %cell_finish.1.refs_1_.refs_2_), channel_id=1, source_target_pairs={{0,6},{1,7},{2,4},{3,5},{4,2},{5,3},{6,0},{7,1},{8,14},{9,15},{10,... | collective-permute-start | bytes 1572872 | tf_op jit(solution)/shard_map/ppermute | solution.py:35
  94.9 1.6 %collective-permute-start.18 = (bf16[96,1024]{1,0:T(8,128)(2,1)S(1)}, bf16[96,1024]{1,0:T(8,128)(2,1)S(1)}, u32[]{:S(2)}, u32[]{:S(2)}) collective-permute-start(bf16[96,1024]{1,0:T(8,128)(2,1)S(1)} %get-tuple-element.53), channel_id=1, source_target_pairs={{0,24},{8,16},{16,8},{24,0},{1,25},{9,17},{17,9},{25,1},{2,26},{10... | collective-permute-start | bytes 589832 | tf_op jit(solution)/shard_map/ppermute | solution.py:35
  96.6 0.5 combine.2
  97.1 6.1 %collective-permute-done.18.refs_5_ = bf16[96,1024]{1,0:T(8,128)(2,1)S(1)} collective-permute-done((bf16[96,1024]{1,0:T(8,128)(2,1)S(1)}, bf16[96,1024]{1,0:T(8,128)(2,1)S(1)}, u32[]{:S(2)}, u32[]{:S(2)}) %collective-permute-start.18) | collective-permute-done | bytes 196640 | tf_op jit(solution)/shard_map/ppermute | solution.py:35
  103.7 1.4 collective-permute-start.28
  105.1 17.4 %collective-permute-done.22.refs_6_ = bf16[1024,256]{1,0:T(8,128)(2,1)S(1)} collective-permute-done((bf16[1024,256]{1,0:T(8,128)(2,1)S(1)}, bf16[1024,256]{1,0:T(8,128)(2,1)S(1)}, u32[]{:S(2)}, u32[]{:S(2)}) %collective-permute-start.22) | collective-permute-done | bytes 524320 | tf_op jit(solution)/shard_map/ppermute | solution.py:35
  122.5 3.7 %collective-permute-start.30 = (bf16[128,512]{1,0:T(8,128)(2,1)S(1)}, bf16[128,512]{1,0:T(8,128)(2,1)}, u32[]{:S(2)}, u32[]{:S(2)}) collective-permute-start(bf16[128,512]{1,0:T(8,128)(2,1)S(1)} %get-tuple-element.57), channel_id=1, source_target_pairs={{0,6},{1,7},{2,4},{3,5},{4,2},{5,3},{6,0},{7,1},{8,14},{9,15},{10,... | collective-permute-start | bytes 393224 | tf_op jit(solution)/shard_map/ppermute | solution.py:35
  127.0 12.1 %collective-permute-done.29 = bf16[128,512]{1,0:T(8,128)(2,1)} collective-permute-done((bf16[128,512]{1,0:T(8,128)(2,1)S(1)}, bf16[128,512]{1,0:T(8,128)(2,1)}, u32[]{:S(2)}, u32[]{:S(2)}) %collective-permute-start.29) | collective-permute-done | bytes 131104 | tf_op jit(solution)/shard_map/ppermute | solution.py:35
  139.1 1.0 collective-permute-start.26
  140.2 1.5 collective-permute-start.27
  141.7 1.7 %add_convert_fusion = bf16[128,512]{1,0:T(8,128)(2,1)} fusion(bf16[128,512]{1,0:T(8,128)(2,1)} %collective-permute-done.30, bf16[128,512]{1,0:T(8,128)(2,1)} %collective-permute-done.29, bf16[128,512]{1,0:T(8,128)(2,1)S(1)} %collective-permute-done.28, bf16[128,512]{1,0:T(8,128)(2,1)S(1)} %get-tuple-element.54.refs_1_), kind=kLoop, calls=%fused_computation | loop fusion | flops 524288 | bytes 655360 | tf_op jit(solution)/shard_map/convert_element_type | solution.py:788
  143.4 6.2 %collective-permute-done.26.refs_11_ = bf16[4,128,512]{2,1,0:T(8,128)(2,1)S(1)} collective-permute-done((bf16[4,128,512]{2,1,0:T(8,128)(2,1)S(1)}, bf16[4,128,512]{2,1,0:T(8,128)(2,1)S(1)}, u32[]{:S(2)}, u32[]{:S(2)}) %collective-permute-start.26) | collective-permute-done | bytes 524320 | tf_op jit(solution)/shard_map/ppermute | solution.py:35
  149.6 0.8 collective-permute-done.27.refs_12_
  150.3 4.5 %project.1 = bf16[1024,512]{1,0:T(8,128)(2,1)} custom-call(s32[3]{0:T(128)S(1)} %pad_add_fusion.refs_4_.refs_0_, bf16[128,512]{1,0:T(8,128)(2,1)S(1)} %get-tuple-element.54.refs_1_, bf16[1024,256]{1,0:T(8,128)(2,1)S(1)} %cell_finish.1.refs_1_.refs_2_, bf16[1024,256]{1,0:T(8,128)(2,1)} %collective-permute-done.19.refs_3_, ...), custom_call_target="tpu_custom_call" | custom-call | flops 2147483648 | bytes 4194304 | tf_op jit(solution)/shard_map/project/pallas_call | solution.py:660
  (64 shorter events, 2.6 us)
Async XLA Ops:
  0.6 28.2 %copy-start.2 = (bf16[1024,128]{1,0:T(8,128)(2,1)S(1)}, bf16[1024,128]{1,0:T(8,128)(2,1)}, u32[]{:S(2)}) copy-start(bf16[1024,128]{1,0:T(8,128)(2,1)} %refs_2_.3) | copy-start | bytes 786436
  0.6 28.2 %copy-start = (bf16[1024,256]{1,0:T(8,128)(2,1)S(1)}, bf16[1024,256]{1,0:T(8,128)(2,1)}, u32[]{:S(2)}) copy-start(bf16[1024,256]{1,0:T(8,128)(2,1)} %refs_3_.4) | copy-start | bytes 1572868
  0.8 0.8 copy-start.9
  1.5 0.7 copy-start.12
  2.2 26.6 %copy-start.10 = (f32[2,1024]{1,0:T(2,128)S(1)}, f32[2,1024]{1,0:T(2,128)}, u32[]{:S(2)}) copy-start(f32[2,1024]{1,0:T(2,128)} %refs_3_.3) | copy-start | bytes 24580
  2.2 26.6 %copy-start.11 = (f32[2,1024]{1,0:T(2,128)S(1)}, f32[2,1024]{1,0:T(2,128)}, u32[]{:S(2)}) copy-start(f32[2,1024]{1,0:T(2,128)} %refs_4_.6) | copy-start | bytes 24580
  6.1 37.3 %copy-start.3 = (bf16[1024,128]{1,0:T(8,128)(2,1)S(1)}, bf16[1024,128]{1,0:T(8,128)(2,1)}, u32[]{:S(2)}) copy-start(bf16[1024,128]{1,0:T(8,128)(2,1)} %refs_4_.7) | copy-start | bytes 786436
  6.2 13.1 %collective-permute-start.3 = (bf16[96,2048]{1,0:T(8,128)(2,1)S(1)}, bf16[96,2048]{1,0:T(8,128)(2,1)}, u32[]{:S(2)}, u32[]{:S(2)}) collective-permute-start(bf16[96,2048]{1,0:T(8,128)(2,1)S(1)} %get-tuple-element.36), channel_id=1, source_target_pairs={{0,8},{8,0},{16,24},{24,16},{1,9},{9,1},{17,25},{25,17},{2,10},{10... | collective-permute-start | bytes 1179656 | tf_op jit(solution)/shard_map/ppermute | solution.py:35
  9.2 19.1 %collective-permute-start.4 = (bf16[96,2048]{1,0:T(8,128)(2,1)S(1)}, bf16[96,2048]{1,0:T(8,128)(2,1)}, u32[]{:S(2)}, u32[]{:S(2)}) collective-permute-start(bf16[96,2048]{1,0:T(8,128)(2,1)S(1)} %get-tuple-element.37), channel_id=1, source_target_pairs={{0,16},{8,24},{16,0},{24,8},{1,17},{9,25},{17,1},{25,9},{2,18},{10... | collective-permute-start | bytes 1179656 | tf_op jit(solution)/shard_map/ppermute | solution.py:35
  10.7 17.6 %collective-permute-start.5 = (bf16[96,2048]{1,0:T(8,128)(2,1)S(1)}, bf16[96,2048]{1,0:T(8,128)(2,1)}, u32[]{:S(2)}, u32[]{:S(2)}) collective-permute-start(bf16[96,2048]{1,0:T(8,128)(2,1)S(1)} %get-tuple-element.38), channel_id=1, source_target_pairs={{0,24},{8,16},{16,8},{24,0},{1,25},{9,17},{17,9},{25,1},{2,26},{10... | collective-permute-start | bytes 1179656 | tf_op jit(solution)/shard_map/ppermute | solution.py:35
  10.7 41.2 %collective-permute-start.6 = (bf16[96,2048]{1,0:T(8,128)(2,1)S(1)}, bf16[96,2048]{1,0:T(8,128)(2,1)}, u32[]{:S(2)}, u32[]{:S(2)}) collective-permute-start(bf16[96,2048]{1,0:T(8,128)(2,1)S(1)} %get-tuple-element.35.refs_2_), channel_id=1, source_target_pairs={{0,1},{1,0},{2,3},{3,2},{4,5},{5,4},{6,7},{7,6},{8,9},{9,8},{10,11... | collective-permute-start | bytes 1179656 | tf_op jit(solution)/shard_map/ppermute | solution.py:35
  19.3 32.7 %collective-permute-start.7 = (bf16[96,2048]{1,0:T(8,128)(2,1)}, bf16[96,2048]{1,0:T(8,128)(2,1)}, u32[]{:S(2)}, u32[]{:S(2)}) collective-permute-start(bf16[96,2048]{1,0:T(8,128)(2,1)} %collective-permute-done.3.refs_3_), channel_id=1, source_target_pairs={{0,1},{1,0},{2,3},{3,2},{4,5},{5,4},{6,7},{7,6},{8,9},{9,8},{10,11... | collective-permute-start | bytes 1179656 | tf_op jit(solution)/shard_map/ppermute | solution.py:35
  28.3 23.7 %collective-permute-start.8 = (bf16[96,2048]{1,0:T(8,128)(2,1)}, bf16[96,2048]{1,0:T(8,128)(2,1)}, u32[]{:S(2)}, u32[]{:S(2)}) collective-permute-start(bf16[96,2048]{1,0:T(8,128)(2,1)} %collective-permute-done.4.refs_4_), channel_id=1, source_target_pairs={{0,1},{1,0},{2,3},{3,2},{4,5},{5,4},{6,7},{7,6},{8,9},{9,8},{10,11... | collective-permute-start | bytes 1179656 | tf_op jit(solution)/shard_map/ppermute | solution.py:35
  28.3 23.7 %collective-permute-start.9 = (bf16[96,2048]{1,0:T(8,128)(2,1)}, bf16[96,2048]{1,0:T(8,128)(2,1)}, u32[]{:S(2)}, u32[]{:S(2)}) collective-permute-start(bf16[96,2048]{1,0:T(8,128)(2,1)} %collective-permute-done.5.refs_5_), channel_id=1, source_target_pairs={{0,1},{1,0},{2,3},{3,2},{4,5},{5,4},{6,7},{7,6},{8,9},{9,8},{10,11... | collective-permute-start | bytes 1179656 | tf_op jit(solution)/shard_map/ppermute | solution.py:35
  30.1 0.6 copy-start.7
  30.7 4.5 %collective-permute-start = (f32[136,128]{1,0:T(8,128)}, f32[136,128]{1,0:T(8,128)S(1)}, u32[]{:S(2)}, u32[]{:S(2)}) collective-permute-start(f32[136,128]{1,0:T(8,128)} %get-tuple-element.31.refs_0_), channel_id=1, source_target_pairs={{0,8},{8,0},{16,24},{24,16},{1,9},{9,1},{17,25},{25,17},{2,10},{10... | collective-permute-start | bytes 208904 | tf_op jit(solution)/shard_map/ppermute | solution.py:35
  35.2 0.6 copy-start.5
  35.8 6.5 %collective-permute-start.1 = (f32[136,128]{1,0:T(8,128)}, f32[136,128]{1,0:T(8,128)}, u32[]{:S(2)}, u32[]{:S(2)}) collective-permute-start(f32[136,128]{1,0:T(8,128)} %get-tuple-element.31.refs_0_), channel_id=1, source_target_pairs={{0,16},{8,24},{16,0},{24,8},{1,17},{9,25},{17,1},{25,9},{2,18},{10... | collective-permute-start | bytes 208904 | tf_op jit(solution)/shard_map/ppermute | solution.py:35
  37.4 88.9 %all-to-all-start = ((bf16[8,128,512]{2,1,0:T(8,128)(2,1)}), bf16[8,128,512]{2,1,0:T(8,128)(2,1)S(1)}, u32[]{:S(2)}, u32[]{:S(2)}) async-start(bf16[8,128,512]{2,1,0:T(8,128)(2,1)} %get-tuple-element.55), calls=%async_computation | async-start | bytes 2097152 | tf_op jit(solution)/shard_map/all_to_all | solution.py:728
  42.3 6.2 %copy-start.13 = (f32[256]{0:T(256)S(1)}, f32[256]{0:T(256)}, u32[]{:S(2)}) copy-start(f32[256]{0:T(256)} %param.24) | copy-start | bytes 3076
  42.3 6.1 %copy-start.4 = (bf16[1024,128]{1,0:T(8,128)(2,1)S(1)}, bf16[1024,128]{1,0:T(8,128)(2,1)}, u32[]{:S(2)}) copy-start(bf16[1024,128]{1,0:T(8,128)(2,1)} %refs_4_.7) | copy-start | bytes 786436
  42.3 6.2 %copy-start.6 = (f32[136,128]{1,0:T(8,128)S(1)}, f32[136,128]{1,0:T(8,128)}, u32[]{:S(2)}) copy-start(f32[136,128]{1,0:T(8,128)} %copy-done.5) | copy-start | bytes 208900
  42.3 6.1 %collective-permute-start.2 = (f32[136,128]{1,0:T(8,128)}, f32[136,128]{1,0:T(8,128)S(1)}, u32[]{:S(2)}, u32[]{:S(2)}) collective-permute-start(f32[136,128]{1,0:T(8,128)} %get-tuple-element.31.refs_0_), channel_id=1, source_target_pairs={{0,24},{8,16},{16,8},{24,0},{1,25},{9,17},{17,9},{25,1},{2,26},{10... | collective-permute-start | bytes 208904 | tf_op jit(solution)/shard_map/ppermute | solution.py:35
  43.4 0.8 copy-start.8
  48.5 1.0 copy-start.1
  51.9 10.2 %copy-start.14 = (f32[128,2]{0,1:T(2,128)S(1)}, f32[128,2]{0,1:T(2,128)}, u32[]{:S(2)}) copy-start(f32[128,2]{0,1:T(2,128)} %param.29) | copy-start | bytes 3076
  61.5 2.7 %collective-permute-start.10 = (bf16[384,1024]{1,0:T(8,128)(2,1)}, bf16[384,1024]{1,0:T(8,128)(2,1)}, u32[]{:S(2)}, u32[]{:S(2)}) collective-permute-start(bf16[384,1024]{1,0:T(8,128)(2,1)} %get-tuple-element.40), channel_id=1, source_target_pairs={{0,1},{1,0},{2,3},{3,2},{4,5},{5,4},{6,7},{7,6},{8,9},{9,8},{10,11... | collective-permute-start | bytes 2359304 | tf_op jit(solution)/shard_map/ppermute | solution.py:35
  61.7 5.4 %collective-permute-start.11 = (bf16[384,1024]{1,0:T(8,128)(2,1)}, bf16[384,1024]{1,0:T(8,128)(2,1)}, u32[]{:S(2)}, u32[]{:S(2)}) collective-permute-start(bf16[384,1024]{1,0:T(8,128)(2,1)} %get-tuple-element.42), channel_id=1, source_target_pairs={{0,1},{1,0},{2,3},{3,2},{4,5},{5,4},{6,7},{7,6},{8,9},{9,8},{10,11... | collective-permute-start | bytes 2359304 | tf_op jit(solution)/shard_map/ppermute | solution.py:35
  73.5 21.4 %collective-permute-start.15 = (bf16[128,2048]{1,0:T(8,128)(2,1)S(1)}, bf16[128,2048]{1,0:T(8,128)(2,1)S(1)}, u32[]{:S(2)}, u32[]{:S(2)}) collective-permute-start(bf16[128,2048]{1,0:T(8,128)(2,1)S(1)} %get-tuple-element.49), channel_id=1, source_target_pairs={{0,1},{1,0},{2,3},{3,2},{4,5},{5,4},{6,7},{7,6},{8,9},{9,8},{10,11... | collective-permute-start | bytes 1572872 | tf_op jit(solution)/shard_map/ppermute | solution.py:35
  73.8 7.8 %collective-permute-start.12 = (bf16[96,1024]{1,0:T(8,128)(2,1)S(1)}, bf16[96,1024]{1,0:T(8,128)(2,1)S(1)}, u32[]{:S(2)}, u32[]{:S(2)}) collective-permute-start(bf16[96,1024]{1,0:T(8,128)(2,1)S(1)} %get-tuple-element.46), channel_id=1, source_target_pairs={{0,8},{8,0},{16,24},{24,16},{1,9},{9,1},{17,25},{25,17},{2,10},{10... | collective-permute-start | bytes 589832 | tf_op jit(solution)/shard_map/ppermute | solution.py:35
  74.8 11.1 %collective-permute-start.13 = (bf16[96,1024]{1,0:T(8,128)(2,1)S(1)}, bf16[96,1024]{1,0:T(8,128)(2,1)S(1)}, u32[]{:S(2)}, u32[]{:S(2)}) collective-permute-start(bf16[96,1024]{1,0:T(8,128)(2,1)S(1)} %get-tuple-element.47), channel_id=1, source_target_pairs={{0,16},{8,24},{16,0},{24,8},{1,17},{9,25},{17,1},{25,9},{2,18},{10... | collective-permute-start | bytes 589832 | tf_op jit(solution)/shard_map/ppermute | solution.py:35
  76.3 9.6 %collective-permute-start.14 = (bf16[96,1024]{1,0:T(8,128)(2,1)S(1)}, bf16[96,1024]{1,0:T(8,128)(2,1)S(1)}, u32[]{:S(2)}, u32[]{:S(2)}) collective-permute-start(bf16[96,1024]{1,0:T(8,128)(2,1)S(1)} %get-tuple-element.48), channel_id=1, source_target_pairs={{0,24},{8,16},{16,8},{24,0},{1,25},{9,17},{17,9},{25,1},{2,26},{10... | collective-permute-start | bytes 589832 | tf_op jit(solution)/shard_map/ppermute | solution.py:35
  77.2 26.4 %collective-permute-start.20 = (bf16[1024,256]{1,0:T(8,128)(2,1)S(1)}, bf16[1024,256]{1,0:T(8,128)(2,1)S(1)}, u32[]{:S(2)}, u32[]{:S(2)}) collective-permute-start(bf16[1024,256]{1,0:T(8,128)(2,1)S(1)} %cell_finish.1.refs_1_.refs_2_), channel_id=1, source_target_pairs={{0,2},{1,3},{2,0},{3,1},{4,6},{5,7},{6,4},{7,5},{8,10},{9,11},{10,... | collective-permute-start | bytes 1572872 | tf_op jit(solution)/shard_map/ppermute | solution.py:35
  81.5 41.0 %collective-permute-start.22 = (bf16[1024,256]{1,0:T(8,128)(2,1)S(1)}, bf16[1024,256]{1,0:T(8,128)(2,1)S(1)}, u32[]{:S(2)}, u32[]{:S(2)}) collective-permute-start(bf16[1024,256]{1,0:T(8,128)(2,1)S(1)} %cell_finish.1.refs_1_.refs_2_), channel_id=1, source_target_pairs={{0,4},{1,5},{2,6},{3,7},{4,0},{5,1},{6,2},{7,3},{8,12},{9,13},{10,... | collective-permute-start | bytes 1572872 | tf_op jit(solution)/shard_map/ppermute | solution.py:35
  85.9 5.7 %collective-permute-start.16 = (bf16[96,1024]{1,0:T(8,128)(2,1)S(1)}, bf16[96,1024]{1,0:T(8,128)(2,1)S(1)}, u32[]{:S(2)}, u32[]{:S(2)}) collective-permute-start(bf16[96,1024]{1,0:T(8,128)(2,1)S(1)} %get-tuple-element.51), channel_id=1, source_target_pairs={{0,8},{8,0},{16,24},{24,16},{1,9},{9,1},{17,25},{25,17},{2,10},{10... | collective-permute-start | bytes 589832 | tf_op jit(solution)/shard_map/ppermute | solution.py:35
  85.9 9.1 %collective-permute-start.17 = (bf16[96,1024]{1,0:T(8,128)(2,1)S(1)}, bf16[96,1024]{1,0:T(8,128)(2,1)S(1)}, u32[]{:S(2)}, u32[]{:S(2)}) collective-permute-start(bf16[96,1024]{1,0:T(8,128)(2,1)S(1)} %get-tuple-element.52), channel_id=1, source_target_pairs={{0,16},{8,24},{16,0},{24,8},{1,17},{9,25},{17,1},{25,9},{2,18},{10... | collective-permute-start | bytes 589832 | tf_op jit(solution)/shard_map/ppermute | solution.py:35
  91.5 34.8 %collective-permute-start.24 = (bf16[1024,256]{1,0:T(8,128)(2,1)S(1)}, bf16[1024,256]{1,0:T(8,128)(2,1)}, u32[]{:S(2)}, u32[]{:S(2)}) collective-permute-start(bf16[1024,256]{1,0:T(8,128)(2,1)S(1)} %cell_finish.1.refs_1_.refs_2_), channel_id=1, source_target_pairs={{0,6},{1,7},{2,4},{3,5},{4,2},{5,3},{6,0},{7,1},{8,14},{9,15},{10,... | collective-permute-start | bytes 1572872 | tf_op jit(solution)/shard_map/ppermute | solution.py:35
  94.9 31.5 %collective-permute-start.19 = (bf16[1024,256]{1,0:T(8,128)(2,1)S(1)}, bf16[1024,256]{1,0:T(8,128)(2,1)}, u32[]{:S(2)}, u32[]{:S(2)}) collective-permute-start(bf16[1024,256]{1,0:T(8,128)(2,1)S(1)} %cell_finish.1.refs_1_.refs_2_), channel_id=1, source_target_pairs={{0,1},{1,0},{2,3},{3,2},{4,5},{5,4},{6,7},{7,6},{8,9},{9,8},{10,11... | collective-permute-start | bytes 1572872 | tf_op jit(solution)/shard_map/ppermute | solution.py:35
  94.9 8.2 %collective-permute-start.18 = (bf16[96,1024]{1,0:T(8,128)(2,1)S(1)}, bf16[96,1024]{1,0:T(8,128)(2,1)S(1)}, u32[]{:S(2)}, u32[]{:S(2)}) collective-permute-start(bf16[96,1024]{1,0:T(8,128)(2,1)S(1)} %get-tuple-element.53), channel_id=1, source_target_pairs={{0,24},{8,16},{16,8},{24,0},{1,25},{9,17},{17,9},{25,1},{2,26},{10... | collective-permute-start | bytes 589832 | tf_op jit(solution)/shard_map/ppermute | solution.py:35
  103.1 36.0 %collective-permute-start.29 = (bf16[128,512]{1,0:T(8,128)(2,1)S(1)}, bf16[128,512]{1,0:T(8,128)(2,1)}, u32[]{:S(2)}, u32[]{:S(2)}) collective-permute-start(bf16[128,512]{1,0:T(8,128)(2,1)S(1)} %get-tuple-element.50.refs_1_), channel_id=1, source_target_pairs={{0,4},{1,5},{2,6},{3,7},{4,0},{5,1},{6,2},{7,3},{8,12},{9,13},{10,... | collective-permute-start | bytes 393224 | tf_op jit(solution)/shard_map/ppermute | solution.py:35
  103.7 23.3 %collective-permute-start.28 = (bf16[128,512]{1,0:T(8,128)(2,1)S(1)}, bf16[128,512]{1,0:T(8,128)(2,1)S(1)}, u32[]{:S(2)}, u32[]{:S(2)}) collective-permute-start(bf16[128,512]{1,0:T(8,128)(2,1)S(1)} %get-tuple-element.56), channel_id=1, source_target_pairs={{0,2},{1,3},{2,0},{3,1},{4,6},{5,7},{6,4},{7,5},{8,10},{9,11},{10,... | collective-permute-start | bytes 393224 | tf_op jit(solution)/shard_map/ppermute | solution.py:35
  122.5 17.6 %collective-permute-start.30 = (bf16[128,512]{1,0:T(8,128)(2,1)S(1)}, bf16[128,512]{1,0:T(8,128)(2,1)}, u32[]{:S(2)}, u32[]{:S(2)}) collective-permute-start(bf16[128,512]{1,0:T(8,128)(2,1)S(1)} %get-tuple-element.57), channel_id=1, source_target_pairs={{0,6},{1,7},{2,4},{3,5},{4,2},{5,3},{6,0},{7,1},{8,14},{9,15},{10,... | collective-permute-start | bytes 393224 | tf_op jit(solution)/shard_map/ppermute | solution.py:35
  126.4 17.0 %collective-permute-start.21 = (bf16[1024,256]{1,0:T(8,128)(2,1)S(1)}, bf16[1024,256]{1,0:T(8,128)(2,1)S(1)}, u32[]{:S(2)}, u32[]{:S(2)}) collective-permute-start(bf16[1024,256]{1,0:T(8,128)(2,1)S(1)} %collective-permute-done.20.refs_4_), channel_id=1, source_target_pairs={{0,1},{1,0},{2,3},{3,2},{4,5},{5,4},{6,7},{7,6},{8,9},{9,8},{10,11... | collective-permute-start | bytes 1572872 | tf_op jit(solution)/shard_map/ppermute | solution.py:35
  126.5 16.9 %collective-permute-start.23 = (bf16[1024,256]{1,0:T(8,128)(2,1)S(1)}, bf16[1024,256]{1,0:T(8,128)(2,1)S(1)}, u32[]{:S(2)}, u32[]{:S(2)}) collective-permute-start(bf16[1024,256]{1,0:T(8,128)(2,1)S(1)} %collective-permute-done.22.refs_6_), channel_id=1, source_target_pairs={{0,1},{1,0},{2,3},{3,2},{4,5},{5,4},{6,7},{7,6},{8,9},{9,8},{10,11... | collective-permute-start | bytes 1572872 | tf_op jit(solution)/shard_map/ppermute | solution.py:35
  126.9 16.4 %collective-permute-start.25 = (bf16[1024,256]{1,0:T(8,128)(2,1)}, bf16[1024,256]{1,0:T(8,128)(2,1)S(1)}, u32[]{:S(2)}, u32[]{:S(2)}) collective-permute-start(bf16[1024,256]{1,0:T(8,128)(2,1)} %collective-permute-done.24.refs_8_), channel_id=1, source_target_pairs={{0,1},{1,0},{2,3},{3,2},{4,5},{5,4},{6,7},{7,6},{8,9},{9,8},{10,11... | collective-permute-start | bytes 1572872 | tf_op jit(solution)/shard_map/ppermute | solution.py:35
  139.1 10.5 %collective-permute-start.26 = (bf16[4,128,512]{2,1,0:T(8,128)(2,1)S(1)}, bf16[4,128,512]{2,1,0:T(8,128)(2,1)S(1)}, u32[]{:S(2)}, u32[]{:S(2)}) collective-permute-start(bf16[4,128,512]{2,1,0:T(8,128)(2,1)S(1)} %get-tuple-element.59), channel_id=1, source_target_pairs={{0,8},{8,0},{16,24},{24,16},{1,9},{9,1},{17,25},{25,17},{2,10},{10... | collective-permute-start | bytes 1572872 | tf_op jit(solution)/shard_map/ppermute | solution.py:35
  140.2 10.2 %collective-permute-start.27 = (bf16[4,128,512]{2,1,0:T(8,128)(2,1)S(1)}, bf16[4,128,512]{2,1,0:T(8,128)(2,1)S(1)}, u32[]{:S(2)}, u32[]{:S(2)}) collective-permute-start(bf16[4,128,512]{2,1,0:T(8,128)(2,1)S(1)} %get-tuple-element.58), channel_id=1, source_target_pairs={{0,16},{8,24},{16,0},{24,8},{1,17},{9,25},{17,1},{25,9},{2,18},{10... | collective-permute-start | bytes 1572872 | tf_op jit(solution)/shard_map/ppermute | solution.py:35

commit v3 on v2

--- a/solution.py
+++ b/solution.py
@@ -641,7 +641,8 @@
     leaving = []
     for b in range(length // block):
         rows = slice(b * block, (b + 1) * block)
-        lhs = jnp.concatenate([m[rows, :] for m in mixed], axis=1)
+        parts = [m[rows, :] for m in mixed]
+        lhs = jnp.concatenate(parts, axis=1)
         stage[rows, :] = dot(lhs, joined[...]).astype(BF16)
         span = pl.ds(b * block, block)
         leaving += start_all(
@@ -652,7 +653,7 @@
 
 def project(idx, mixed, share, low_part, high_part, deps=()):
     length, own = mixed[0].shape
-    n_tp = len(mixed)
+    n_tp = share.shape[0]
     cols = share.shape[-1]
     block = 256
     hbm = pl.BlockSpec(memory_space=pl.ANY)
@@ -660,7 +661,7 @@
     return pl.pallas_call(
         with_deps(functools.partial(project_kernel, n_tp=n_tp, block=block), len(deps), 1),
         out_shape=jax.ShapeDtypeStruct((length, cols), BF16),
-        in_specs=[pl.BlockSpec(memory_space=pltpu.SMEM)] + anywhere(deps) + [vm] * (n_tp + 3),
+        in_specs=[pl.BlockSpec(memory_space=pltpu.SMEM)] + anywhere(deps) + [vm] * (len(mixed) + 3),
         out_specs=hbm,
         scratch_shapes=[
             pltpu.VMEM((n_tp * own, cols), BF16),
@@ -671,6 +672,10 @@
         cost_estimate=cost(2 * length * n_tp * own * cols, 2 * length * n_tp * own),
         name="project",
     )(idx, *deps, *mixed, share, low_part, high_part)
+
+
+def passed_on(k, n_z):
+    return n_z == 4 and k == 2
 
 
 def local(
@@ -735,12 +740,16 @@
     mixed = cell_finish(
         ep_idx, put(packs, pltpu.VMEM), queries, out_gate, out_gain.reshape(1, -1), inner, stats, gate_info, heads
     )
-    gathered = [mixed]
+    pieces, gathered = [], [mixed] + [None] * (n_z - 1)
     for k in range(1, n_z):
-        gathered.append(swap(mixed, "tp", 2 * k))
-    pieces = []
+        if not passed_on(k, n_z):
+            gathered[k] = swap(mixed, "tp", 2 * k)
+    for k in range(1, n_z):
+        if passed_on(k, n_z):
+            gathered[k] = swap(gathered[n_z - 1], "tp", 2 * (n_z - 1 - k))
     for g in gathered:
         pieces += [g, swap(g, "tp", 1)]
+
     others = []
     for a in arrived:
         others.append(swap(a, "tp", 1))

time: 156 us -> 142 us (0.910)
  waiting for transfers between devices: 73.2 us -> 50 us
  starting transfers between devices: 37.7 us -> 47.1 us
    ppermute x31, waiting for transfers between devices: 73.2 us -> 50 us  [swap(): return lax.ppermute(x, axis, xor_pairs(lax.axis_size(axis), k))]
    ppermute x31, starting transfers between devices: 32.9 us -> 42.3 us  [swap(): return lax.ppermute(x, axis, xor_pairs(lax.axis_size(axis), k))]
  transfers between devices with their start and end apart: 32 -> 32, of which waited for: 12 -> 12; matrix products, arithmetic and copies ran while one was open for 1% -> 1% of each run, Pallas kernels for 18% -> 20%
where the time goes in v3:
time: 142 us
  waiting for transfers between devices  50 us (35%)
  starting transfers between devices  47.1 us (33%)
  Pallas kernels  36.7 us (26%)
  local copies, waits for them, and re-layouts  4.9 us (3%)
  other arithmetic  1.85 us (1%)
    ppermute x31, waiting for transfers between devices, swap(): return lax.ppermute(x, axis, xor_pairs(lax.axis_size(axis), k))  50 us
    ppermute x31, starting transfers between devices, swap(): return lax.ppermute(x, axis, xor_pairs(lax.axis_size(axis), k))  42.3 us
    pallas_call x1, Pallas kernels, expert(): pl.pallas_call(with_deps(functools.partial(expert_kernel, n_ep=n_ep, n_z=...  9.48 us
    pallas_call x2, Pallas kernels, pair_sum(): pl.pallas_call(with_deps(functools.partial(pair_kernel, n_z=n_z, part=par...  5.92 us
    all_to_all x1, starting transfers between devices, local(): share = lax.all_to_all(share, 'tp', 0, 0, tiled=True)  4.88 us
    unnamed x31, local copies, waits for them, and re-layouts  4.74 us
    pallas_call x1, Pallas kernels, project(): pl.pallas_call(with_deps(functools.partial(project_kernel, n_tp=n_tp, blo...  4.5 us
    pallas_call x1, Pallas kernels, cell_intra(): pl.pallas_call(with_deps(functools.partial(intra_kernel, block=256, heads...  4.17 us
  transfers between devices with their start and end apart: 32, of which 12 were waited for; matrix products, arithmetic and copies ran while one was open for 1% of the time, Pallas kernels for 20%

profile of v3, /device:TPU:0, one launch (start us, length us, event | category | flops | bytes accessed | tf_op | source)
XLA Modules:
  0.0 141.7 jit_solution(7865761715105180567)
XLA Ops:
  0.8 0.8 copy-done.9
  1.5 0.7 copy-done.12
  2.2 3.9 %prep.1 = (bf16[128,4096]{1,0:T(8,128)(2,1)S(1)}, s32[8,128]{1,0:T(8,128)S(1)}, bf16[8,128,512]{2,1,0:T(8,128)(2,1)}, bf16[96,2048]{1,0:T(8,128)(2,1)S(1)}, bf16...) custom-call(s32[3]{0:T(128)S(1)} %pad_add_fusion.2.refs_0_, ...), custom_call_target="tpu_custom_call" | custom-call | flops 201326592 | bytes 2097152 | tf_op jit(solution)/shard_map/prep/pallas_call | solution.py:120
  6.2 3.0 %collective-permute-start.3 = (bf16[96,2048]{1,0:T(8,128)(2,1)S(1)}, bf16[96,2048]{1,0:T(8,128)(2,1)}, u32[]{:S(2)}, u32[]{:S(2)}) collective-permute-start(bf16[96,2048]{1,0:T(8,128)(2,1)S(1)} %get-tuple-element.36), channel_id=1, source_target_pairs={{0,8},{8,0},{16,24},{24,16},{1,9},{9,1},{17,25},{25,17},{2,10},{10... | collective-permute-start | bytes 1179656 | tf_op jit(solution)/shard_map/ppermute | solution.py:35
  9.2 1.5 %collective-permute-start.4 = (bf16[96,2048]{1,0:T(8,128)(2,1)S(1)}, bf16[96,2048]{1,0:T(8,128)(2,1)}, u32[]{:S(2)}, u32[]{:S(2)}) collective-permute-start(bf16[96,2048]{1,0:T(8,128)(2,1)S(1)} %get-tuple-element.37), channel_id=1, source_target_pairs={{0,16},{8,24},{16,0},{24,8},{1,17},{9,25},{17,1},{25,9},{2,18},{10... | collective-permute-start | bytes 1179656 | tf_op jit(solution)/shard_map/ppermute | solution.py:35
  10.7 8.5 %collective-permute-done.3.refs_3_ = bf16[96,2048]{1,0:T(8,128)(2,1)} collective-permute-done((bf16[96,2048]{1,0:T(8,128)(2,1)S(1)}, bf16[96,2048]{1,0:T(8,128)(2,1)}, u32[]{:S(2)}, u32[]{:S(2)}) %collective-permute-start.3) | collective-permute-done | bytes 393248 | tf_op jit(solution)/shard_map/ppermute | solution.py:35
  19.3 9.0 %collective-permute-done.4.refs_4_ = bf16[96,2048]{1,0:T(8,128)(2,1)} collective-permute-done((bf16[96,2048]{1,0:T(8,128)(2,1)S(1)}, bf16[96,2048]{1,0:T(8,128)(2,1)}, u32[]{:S(2)}, u32[]{:S(2)}) %collective-permute-start.4) | collective-permute-done | bytes 393248 | tf_op jit(solution)/shard_map/ppermute | solution.py:35
  28.3 0.5 collective-permute-start.9
  28.8 1.3 cell_state.1
  30.1 0.6 copy-done.7
  30.7 0.7 collective-permute-start
  31.4 3.8 %collective-permute-done.refs_1_ = f32[136,128]{1,0:T(8,128)S(1)} collective-permute-done((f32[136,128]{1,0:T(8,128)}, f32[136,128]{1,0:T(8,128)S(1)}, u32[]{:S(2)}, u32[]{:S(2)}) %collective-permute-start) | collective-permute-done | bytes 69664 | tf_op jit(solution)/shard_map/ppermute | solution.py:35
  35.2 0.6 copy-done.5
  35.8 1.5 %collective-permute-start.1 = (f32[136,128]{1,0:T(8,128)}, f32[136,128]{1,0:T(8,128)}, u32[]{:S(2)}, u32[]{:S(2)}) collective-permute-start(f32[136,128]{1,0:T(8,128)} %get-tuple-element.31.refs_0_), channel_id=1, source_target_pairs={{0,16},{8,24},{16,0},{24,8},{1,17},{9,25},{17,1},{25,9},{2,18},{10... | collective-permute-start | bytes 208904 | tf_op jit(solution)/shard_map/ppermute | solution.py:35
  37.4 4.9 %all-to-all-start = ((bf16[8,128,512]{2,1,0:T(8,128)(2,1)}), bf16[8,128,512]{2,1,0:T(8,128)(2,1)S(1)}, u32[]{:S(2)}, u32[]{:S(2)}) async-start(bf16[8,128,512]{2,1,0:T(8,128)(2,1)} %get-tuple-element.55), calls=%async_computation | async-start | bytes 2097152 | tf_op jit(solution)/shard_map/all_to_all | solution.py:733
  42.3 1.0 collective-permute-start.2
  43.4 0.8 copy-done.8
  44.3 4.2 %cell_intra.1 = (f32[1024,256]{1,0:T(8,128)S(1)}, f32[16,1024]{1,0:T(8,128)S(1)}) custom-call(f32[136,128]{1,0:T(8,128)} %get-tuple-element.31.refs_0_, bf16[1024,128]{1,0:T(8,128)(2,1)S(1)} %copy-done.3, bf16[1024,128]{1,0:T(8,128)(2,1)S(1)} %copy-done.2, bf16[1024,256]{1,0:T(8,128)(2,1)S(1)} %copy-done, f32[16,1024]{1,0:T(8,128)S(1)} %copy-done.8), custom_call_target="tpu_custom_call" | custom-call | flops 402653184 | bytes 2097152 | tf_op jit(solution)/shard_map/cell_intra/pallas_call | solution.py:524
  48.5 1.0 copy-done.1
  49.5 2.4 %cell_finish.1.refs_1_.refs_2_ = bf16[1024,256]{1,0:T(8,128)(2,1)S(1)} custom-call(s32[1]{0:T(128)} %bitcast.6.refs_0_, f32[136,128]{1,0:T(8,128)S(1)} %copy-done.6, f32[136,128]{1,0:T(8,128)} %collective-permute-done.1.refs_2_, f32[136,128]{1,0:T(8,128)S(1)} %collective-permute-done.2.refs_3_, bf16[1024,128]{1,0:T(8,128)(2,1)S(1)} %copy-done.4, ...), custom_call_target="tpu_custom_call" | custom-call | flops 67108864 | bytes 3145728 | tf_op jit(solution)/shard_map/cell_finish/pallas_call | solution.py:603
  52.0 9.5 %expert.1 = (bf16[384,1024]{1,0:T(8,128)(2,1)}, bf16[384,1024]{1,0:T(8,128)(2,1)}, bf16[384,512]{1,0:T(8,128)(2,1)S(1)}) custom-call(s32[2]{0:T(128)S(1)} %pad_add_fusion.1.refs_0_, bf16[1024,256]{1,0:T(8,128)(2,1)S(1)} %cell_finish.1.refs_1_.refs_2_, bf16[96,2048]{1,0:T(8,128)(2,1)S(1)} %get-tuple-element.35.refs_2_, ...), custom_call_target="tpu_custom_call" | custom-call | flops 4026531840 | bytes 16777216 | tf_op jit(solution)/shard_map/expert/pallas_call | solution.py:226
  61.7 0.3 collective-permute-start.11
  62.3 3.8 %collective-permute-start.22 = (bf16[1024,256]{1,0:T(8,128)(2,1)S(1)}, bf16[1024,256]{1,0:T(8,128)(2,1)}, u32[]{:S(2)}, u32[]{:S(2)}) collective-permute-start(bf16[1024,256]{1,0:T(8,128)(2,1)S(1)} %cell_finish.1.refs_1_.refs_2_), channel_id=1, source_target_pairs={{0,6},{1,7},{2,4},{3,5},{4,2},{5,3},{6,0},{7,1},{8,14},{9,15},{10,... | collective-permute-start | bytes 1572872 | tf_op jit(solution)/shard_map/ppermute | solution.py:35
  66.2 3.0 %pair_sum.2 = (bf16[96,1024]{1,0:T(8,128)(2,1)S(1)}, bf16[96,1024]{1,0:T(8,128)(2,1)S(1)}, bf16[96,1024]{1,0:T(8,128)(2,1)S(1)}, bf16[96,1024]{1,0:T(8,128)(2,1)S(1)}) custom-call(s32[2]{0:T(128)S(1)} %pad_add_fusion.1.refs_0_, bf16[384,512]{1,0:T(8,128)(2,1)S(1)} %get-tuple-element.39.refs_1_.refs_2_, ...), custom_call_target="tpu_custom_call" | custom-call | flops 402653184 | bytes 2621440 | tf_op jit(solution)/shard_map/pair_sum/pallas_call | solution.py:279
  69.2 3.0 %pair_sum.3 = (bf16[96,1024]{1,0:T(8,128)(2,1)S(1)}, bf16[96,1024]{1,0:T(8,128)(2,1)S(1)}, bf16[96,1024]{1,0:T(8,128)(2,1)S(1)}, bf16[96,1024]{1,0:T(8,128)(2,1)S(1)}) custom-call(s32[2]{0:T(128)S(1)} %pad_add_fusion.1.refs_0_, bf16[96,1024]{1,0:T(8,128)(2,1)S(1)} %get-tuple-element.41.refs_1_.refs_2_, ...), custom_call_target="tpu_custom_call" | custom-call | flops 402653184 | bytes 2621440 | tf_op jit(solution)/shard_map/pair_sum/pallas_call | solution.py:279
  72.1 3.4 %shared.1 = (bf16[128,2048]{1,0:T(8,128)(2,1)S(1)}, bf16[128,2048]{1,0:T(8,128)(2,1)S(1)}) custom-call(s32[1]{0:T(128)} %bitcast.4.refs_0_, bf16[96,1024]{1,0:T(8,128)(2,1)S(1)} %get-tuple-element.43.refs_1_.refs_2_, s32[128,8]{1,0:T(8,128)S(1)} %bitcast.12, f32[128,2]{1,0:T(8,128)S(1)} %copy.21.refs_3_.refs_9_, s32[3]{0:T(128)S(1)} %pad_add_fusion.refs_4_.refs_0_, ...), custom_call_target="tpu_custom_call" | custom-call | flops 805306368 | bytes 8388608 | tf_op jit(solution)/shard_map/shared/pallas_call | solution.py:327
  75.6 1.1 collective-permute-start.12
  76.7 1.5 %collective-permute-start.13 = (bf16[96,1024]{1,0:T(8,128)(2,1)S(1)}, bf16[96,1024]{1,0:T(8,128)(2,1)S(1)}, u32[]{:S(2)}, u32[]{:S(2)}) collective-permute-start(bf16[96,1024]{1,0:T(8,128)(2,1)S(1)} %get-tuple-element.47), channel_id=1, source_target_pairs={{0,16},{8,24},{16,0},{24,8},{1,17},{9,25},{17,1},{25,9},{2,18},{10... | collective-permute-start | bytes 589832 | tf_op jit(solution)/shard_map/ppermute | solution.py:35
  78.5 2.0 %collective-permute-start.14 = (bf16[96,1024]{1,0:T(8,128)(2,1)S(1)}, bf16[96,1024]{1,0:T(8,128)(2,1)S(1)}, u32[]{:S(2)}, u32[]{:S(2)}) collective-permute-start(bf16[96,1024]{1,0:T(8,128)(2,1)S(1)} %get-tuple-element.48), channel_id=1, source_target_pairs={{0,24},{8,16},{16,8},{24,0},{1,25},{9,17},{17,9},{25,1},{2,26},{10... | collective-permute-start | bytes 589832 | tf_op jit(solution)/shard_map/ppermute | solution.py:35
  80.4 3.0 %collective-permute-done.12.refs_3_ = bf16[96,1024]{1,0:T(8,128)(2,1)S(1)} collective-permute-done((bf16[96,1024]{1,0:T(8,128)(2,1)S(1)}, bf16[96,1024]{1,0:T(8,128)(2,1)S(1)}, u32[]{:S(2)}, u32[]{:S(2)}) %collective-permute-start.12) | collective-permute-done | bytes 196640 | tf_op jit(solution)/shard_map/ppermute | solution.py:35
  83.4 1.0 collective-permute-start.16
  84.5 3.1 %collective-permute-done.13.refs_4_ = bf16[96,1024]{1,0:T(8,128)(2,1)S(1)} collective-permute-done((bf16[96,1024]{1,0:T(8,128)(2,1)S(1)}, bf16[96,1024]{1,0:T(8,128)(2,1)S(1)}, u32[]{:S(2)}, u32[]{:S(2)}) %collective-permute-start.13) | collective-permute-done | bytes 196640 | tf_op jit(solution)/shard_map/ppermute | solution.py:35
  87.5 0.6 collective-permute-done.14.refs_5_
  88.2 12.4 %collective-permute-start.23 = (bf16[1024,256]{1,0:T(8,128)(2,1)}, bf16[1024,256]{1,0:T(8,128)(2,1)}, u32[]{:S(2)}, u32[]{:S(2)}) collective-permute-start(bf16[1024,256]{1,0:T(8,128)(2,1)} %collective-permute-done.22.refs_8_), channel_id=1, source_target_pairs={{0,2},{1,3},{2,0},{3,1},{4,6},{5,7},{6,4},{7,5},{8,10},{9,11},{10,... | collective-permute-start | bytes 1572872 | tf_op jit(solution)/shard_map/ppermute | solution.py:35
  100.6 0.5 collective-permute-start.17
  101.1 1.5 %collective-permute-start.18 = (bf16[96,1024]{1,0:T(8,128)(2,1)S(1)}, bf16[96,1024]{1,0:T(8,128)(2,1)S(1)}, u32[]{:S(2)}, u32[]{:S(2)}) collective-permute-start(bf16[96,1024]{1,0:T(8,128)(2,1)S(1)} %get-tuple-element.53), channel_id=1, source_target_pairs={{0,24},{8,16},{16,8},{24,0},{1,25},{9,17},{17,9},{25,1},{2,26},{10... | collective-permute-start | bytes 589832 | tf_op jit(solution)/shard_map/ppermute | solution.py:35
  102.6 1.1 combine.2
  103.8 4.9 %collective-permute-done.17.refs_4_ = bf16[96,1024]{1,0:T(8,128)(2,1)S(1)} collective-permute-done((bf16[96,1024]{1,0:T(8,128)(2,1)S(1)}, bf16[96,1024]{1,0:T(8,128)(2,1)S(1)}, u32[]{:S(2)}, u32[]{:S(2)}) %collective-permute-start.17) | collective-permute-done | bytes 196640 | tf_op jit(solution)/shard_map/ppermute | solution.py:35
  108.6 4.4 %collective-permute-start.29 = (bf16[128,512]{1,0:T(8,128)(2,1)S(1)}, bf16[128,512]{1,0:T(8,128)(2,1)S(1)}, u32[]{:S(2)}, u32[]{:S(2)}) collective-permute-start(bf16[128,512]{1,0:T(8,128)(2,1)S(1)} %get-tuple-element.50.refs_1_), channel_id=1, source_target_pairs={{0,4},{1,5},{2,6},{3,7},{4,0},{5,1},{6,2},{7,3},{8,12},{9,13},{10,... | collective-permute-start | bytes 393224 | tf_op jit(solution)/shard_map/ppermute | solution.py:35
  113.0 0.5 combine.3
  113.6 1.6 %collective-permute-start.30 = (bf16[128,512]{1,0:T(8,128)(2,1)}, bf16[128,512]{1,0:T(8,128)(2,1)}, u32[]{:S(2)}, u32[]{:S(2)}) collective-permute-start(bf16[128,512]{1,0:T(8,128)(2,1)} %get-tuple-element.57), channel_id=1, source_target_pairs={{0,6},{1,7},{2,4},{3,5},{4,2},{5,3},{6,0},{7,1},{8,14},{9,15},{10,... | collective-permute-start | bytes 393224 | tf_op jit(solution)/shard_map/ppermute | solution.py:35
  115.4 0.5 collective-permute-start.21
  115.9 6.0 %collective-permute-done.28 = bf16[128,512]{1,0:T(8,128)(2,1)S(1)} collective-permute-done((bf16[128,512]{1,0:T(8,128)(2,1)S(1)}, bf16[128,512]{1,0:T(8,128)(2,1)S(1)}, u32[]{:S(2)}, u32[]{:S(2)}) %collective-permute-start.28) | collective-permute-done | bytes 131104 | tf_op jit(solution)/shard_map/ppermute | solution.py:35
  122.0 2.8 %collective-permute-start.27 = (bf16[4,128,512]{2,1,0:T(8,128)(2,1)S(1)}, bf16[4,128,512]{2,1,0:T(8,128)(2,1)S(1)}, u32[]{:S(2)}, u32[]{:S(2)}) collective-permute-start(bf16[4,128,512]{2,1,0:T(8,128)(2,1)S(1)} %get-tuple-element.58), channel_id=1, source_target_pairs={{0,16},{8,24},{16,0},{24,8},{1,17},{9,25},{17,1},{25,9},{2,18},{10... | collective-permute-start | bytes 1572872 | tf_op jit(solution)/shard_map/ppermute | solution.py:35
  124.7 1.6 %add_convert_fusion = bf16[128,512]{1,0:T(8,128)(2,1)} fusion(bf16[128,512]{1,0:T(8,128)(2,1)} %collective-permute-done.30, bf16[128,512]{1,0:T(8,128)(2,1)S(1)} %collective-permute-done.29, bf16[128,512]{1,0:T(8,128)(2,1)S(1)} %collective-permute-done.28, bf16[128,512]{1,0:T(8,128)(2,1)S(1)} %get-tuple-element.54.refs_1_), kind=kLoop, calls=%fused_computation | loop fusion | flops 524288 | bytes 655360 | tf_op jit(solution)/shard_map/convert_element_type | solution.py:797
  126.4 9.9 %collective-permute-done.26.refs_11_ = bf16[4,128,512]{2,1,0:T(8,128)(2,1)S(1)} collective-permute-done((bf16[4,128,512]{2,1,0:T(8,128)(2,1)S(1)}, bf16[4,128,512]{2,1,0:T(8,128)(2,1)S(1)}, u32[]{:S(2)}, u32[]{:S(2)}) %collective-permute-start.26) | collective-permute-done | bytes 524320 | tf_op jit(solution)/shard_map/ppermute | solution.py:35
  136.2 0.8 collective-permute-done.27.refs_12_
  137.0 4.5 %project.1 = bf16[1024,512]{1,0:T(8,128)(2,1)} custom-call(s32[3]{0:T(128)S(1)} %pad_add_fusion.refs_4_.refs_0_, bf16[128,512]{1,0:T(8,128)(2,1)S(1)} %get-tuple-element.54.refs_1_, bf16[1024,256]{1,0:T(8,128)(2,1)S(1)} %cell_finish.1.refs_1_.refs_2_, bf16[1024,256]{1,0:T(8,128)(2,1)S(1)} %collective-permute-done.19.refs_3_, ...), custom_call_target="tpu_custom_call" | custom-call | flops 2147483648 | bytes 4194304 | tf_op jit(solution)/shard_map/project/pallas_call | solution.py:661
  (64 shorter events, 1.4 us)
Async XLA Ops:
  0.6 28.2 %copy-start.2 = (bf16[1024,128]{1,0:T(8,128)(2,1)S(1)}, bf16[1024,128]{1,0:T(8,128)(2,1)}, u32[]{:S(2)}) copy-start(bf16[1024,128]{1,0:T(8,128)(2,1)} %refs_2_.3) | copy-start | bytes 786436
  0.6 28.2 %copy-start = (bf16[1024,256]{1,0:T(8,128)(2,1)S(1)}, bf16[1024,256]{1,0:T(8,128)(2,1)}, u32[]{:S(2)}) copy-start(bf16[1024,256]{1,0:T(8,128)(2,1)} %refs_3_.4) | copy-start | bytes 1572868
  0.8 0.8 copy-start.9
  1.5 0.7 copy-start.12
  2.2 26.6 %copy-start.10 = (f32[2,1024]{1,0:T(2,128)S(1)}, f32[2,1024]{1,0:T(2,128)}, u32[]{:S(2)}) copy-start(f32[2,1024]{1,0:T(2,128)} %refs_3_.3) | copy-start | bytes 24580
  2.2 26.6 %copy-start.11 = (f32[2,1024]{1,0:T(2,128)S(1)}, f32[2,1024]{1,0:T(2,128)}, u32[]{:S(2)}) copy-start(f32[2,1024]{1,0:T(2,128)} %refs_4_.6) | copy-start | bytes 24580
  6.1 37.3 %copy-start.3 = (bf16[1024,128]{1,0:T(8,128)(2,1)S(1)}, bf16[1024,128]{1,0:T(8,128)(2,1)}, u32[]{:S(2)}) copy-start(bf16[1024,128]{1,0:T(8,128)(2,1)} %refs_4_.7) | copy-start | bytes 786436
  6.2 13.1 %collective-permute-start.3 = (bf16[96,2048]{1,0:T(8,128)(2,1)S(1)}, bf16[96,2048]{1,0:T(8,128)(2,1)}, u32[]{:S(2)}, u32[]{:S(2)}) collective-permute-start(bf16[96,2048]{1,0:T(8,128)(2,1)S(1)} %get-tuple-element.36), channel_id=1, source_target_pairs={{0,8},{8,0},{16,24},{24,16},{1,9},{9,1},{17,25},{25,17},{2,10},{10... | collective-permute-start | bytes 1179656 | tf_op jit(solution)/shard_map/ppermute | solution.py:35
  9.2 19.1 %collective-permute-start.4 = (bf16[96,2048]{1,0:T(8,128)(2,1)S(1)}, bf16[96,2048]{1,0:T(8,128)(2,1)}, u32[]{:S(2)}, u32[]{:S(2)}) collective-permute-start(bf16[96,2048]{1,0:T(8,128)(2,1)S(1)} %get-tuple-element.37), channel_id=1, source_target_pairs={{0,16},{8,24},{16,0},{24,8},{1,17},{9,25},{17,1},{25,9},{2,18},{10... | collective-permute-start | bytes 1179656 | tf_op jit(solution)/shard_map/ppermute | solution.py:35
  10.7 17.6 %collective-permute-start.5 = (bf16[96,2048]{1,0:T(8,128)(2,1)S(1)}, bf16[96,2048]{1,0:T(8,128)(2,1)}, u32[]{:S(2)}, u32[]{:S(2)}) collective-permute-start(bf16[96,2048]{1,0:T(8,128)(2,1)S(1)} %get-tuple-element.38), channel_id=1, source_target_pairs={{0,24},{8,16},{16,8},{24,0},{1,25},{9,17},{17,9},{25,1},{2,26},{10... | collective-permute-start | bytes 1179656 | tf_op jit(solution)/shard_map/ppermute | solution.py:35
  10.7 41.2 %collective-permute-start.6 = (bf16[96,2048]{1,0:T(8,128)(2,1)S(1)}, bf16[96,2048]{1,0:T(8,128)(2,1)}, u32[]{:S(2)}, u32[]{:S(2)}) collective-permute-start(bf16[96,2048]{1,0:T(8,128)(2,1)S(1)} %get-tuple-element.35.refs_2_), channel_id=1, source_target_pairs={{0,1},{1,0},{2,3},{3,2},{4,5},{5,4},{6,7},{7,6},{8,9},{9,8},{10,11... | collective-permute-start | bytes 1179656 | tf_op jit(solution)/shard_map/ppermute | solution.py:35
  19.3 32.7 %collective-permute-start.7 = (bf16[96,2048]{1,0:T(8,128)(2,1)}, bf16[96,2048]{1,0:T(8,128)(2,1)}, u32[]{:S(2)}, u32[]{:S(2)}) collective-permute-start(bf16[96,2048]{1,0:T(8,128)(2,1)} %collective-permute-done.3.refs_3_), channel_id=1, source_target_pairs={{0,1},{1,0},{2,3},{3,2},{4,5},{5,4},{6,7},{7,6},{8,9},{9,8},{10,11... | collective-permute-start | bytes 1179656 | tf_op jit(solution)/shard_map/ppermute | solution.py:35
  28.3 23.7 %collective-permute-start.8 = (bf16[96,2048]{1,0:T(8,128)(2,1)}, bf16[96,2048]{1,0:T(8,128)(2,1)}, u32[]{:S(2)}, u32[]{:S(2)}) collective-permute-start(bf16[96,2048]{1,0:T(8,128)(2,1)} %collective-permute-done.4.refs_4_), channel_id=1, source_target_pairs={{0,1},{1,0},{2,3},{3,2},{4,5},{5,4},{6,7},{7,6},{8,9},{9,8},{10,11... | collective-permute-start | bytes 1179656 | tf_op jit(solution)/shard_map/ppermute | solution.py:35
  28.3 23.7 %collective-permute-start.9 = (bf16[96,2048]{1,0:T(8,128)(2,1)}, bf16[96,2048]{1,0:T(8,128)(2,1)}, u32[]{:S(2)}, u32[]{:S(2)}) collective-permute-start(bf16[96,2048]{1,0:T(8,128)(2,1)} %collective-permute-done.5.refs_5_), channel_id=1, source_target_pairs={{0,1},{1,0},{2,3},{3,2},{4,5},{5,4},{6,7},{7,6},{8,9},{9,8},{10,11... | collective-permute-start | bytes 1179656 | tf_op jit(solution)/shard_map/ppermute | solution.py:35
  30.1 0.6 copy-start.7
  30.7 4.5 %collective-permute-start = (f32[136,128]{1,0:T(8,128)}, f32[136,128]{1,0:T(8,128)S(1)}, u32[]{:S(2)}, u32[]{:S(2)}) collective-permute-start(f32[136,128]{1,0:T(8,128)} %get-tuple-element.31.refs_0_), channel_id=1, source_target_pairs={{0,8},{8,0},{16,24},{24,16},{1,9},{9,1},{17,25},{25,17},{2,10},{10... | collective-permute-start | bytes 208904 | tf_op jit(solution)/shard_map/ppermute | solution.py:35
  35.2 0.6 copy-start.5
  35.8 6.5 %collective-permute-start.1 = (f32[136,128]{1,0:T(8,128)}, f32[136,128]{1,0:T(8,128)}, u32[]{:S(2)}, u32[]{:S(2)}) collective-permute-start(f32[136,128]{1,0:T(8,128)} %get-tuple-element.31.refs_0_), channel_id=1, source_target_pairs={{0,16},{8,24},{16,0},{24,8},{1,17},{9,25},{17,1},{25,9},{2,18},{10... | collective-permute-start | bytes 208904 | tf_op jit(solution)/shard_map/ppermute | solution.py:35
  37.4 77.8 %all-to-all-start = ((bf16[8,128,512]{2,1,0:T(8,128)(2,1)}), bf16[8,128,512]{2,1,0:T(8,128)(2,1)S(1)}, u32[]{:S(2)}, u32[]{:S(2)}) async-start(bf16[8,128,512]{2,1,0:T(8,128)(2,1)} %get-tuple-element.55), calls=%async_computation | async-start | bytes 2097152 | tf_op jit(solution)/shard_map/all_to_all | solution.py:733
  42.3 6.2 %copy-start.13 = (f32[256]{0:T(256)S(1)}, f32[256]{0:T(256)}, u32[]{:S(2)}) copy-start(f32[256]{0:T(256)} %param.24) | copy-start | bytes 3076
  42.3 6.1 %copy-start.4 = (bf16[1024,128]{1,0:T(8,128)(2,1)S(1)}, bf16[1024,128]{1,0:T(8,128)(2,1)}, u32[]{:S(2)}) copy-start(bf16[1024,128]{1,0:T(8,128)(2,1)} %refs_4_.7) | copy-start | bytes 786436
  42.3 6.2 %copy-start.6 = (f32[136,128]{1,0:T(8,128)S(1)}, f32[136,128]{1,0:T(8,128)}, u32[]{:S(2)}) copy-start(f32[136,128]{1,0:T(8,128)} %copy-done.5) | copy-start | bytes 208900
  42.3 6.1 %collective-permute-start.2 = (f32[136,128]{1,0:T(8,128)}, f32[136,128]{1,0:T(8,128)S(1)}, u32[]{:S(2)}, u32[]{:S(2)}) collective-permute-start(f32[136,128]{1,0:T(8,128)} %get-tuple-element.31.refs_0_), channel_id=1, source_target_pairs={{0,24},{8,16},{16,8},{24,0},{1,25},{9,17},{17,9},{25,1},{2,26},{10... | collective-permute-start | bytes 208904 | tf_op jit(solution)/shard_map/ppermute | solution.py:35
  43.4 0.8 copy-start.8
  48.5 1.0 copy-start.1
  51.9 10.2 %copy-start.14 = (f32[128,2]{0,1:T(2,128)S(1)}, f32[128,2]{0,1:T(2,128)}, u32[]{:S(2)}) copy-start(f32[128,2]{0,1:T(2,128)} %param.29) | copy-start | bytes 3076
  61.5 4.7 %collective-permute-start.10 = (bf16[384,1024]{1,0:T(8,128)(2,1)}, bf16[384,1024]{1,0:T(8,128)(2,1)}, u32[]{:S(2)}, u32[]{:S(2)}) collective-permute-start(bf16[384,1024]{1,0:T(8,128)(2,1)} %get-tuple-element.40), channel_id=1, source_target_pairs={{0,1},{1,0},{2,3},{3,2},{4,5},{5,4},{6,7},{7,6},{8,9},{9,8},{10,11... | collective-permute-start | bytes 2359304 | tf_op jit(solution)/shard_map/ppermute | solution.py:35
  61.7 7.4 %collective-permute-start.11 = (bf16[384,1024]{1,0:T(8,128)(2,1)}, bf16[384,1024]{1,0:T(8,128)(2,1)}, u32[]{:S(2)}, u32[]{:S(2)}) collective-permute-start(bf16[384,1024]{1,0:T(8,128)(2,1)} %get-tuple-element.42), channel_id=1, source_target_pairs={{0,1},{1,0},{2,3},{3,2},{4,5},{5,4},{6,7},{7,6},{8,9},{9,8},{10,11... | collective-permute-start | bytes 2359304 | tf_op jit(solution)/shard_map/ppermute | solution.py:35
  62.3 16.2 %collective-permute-start.22 = (bf16[1024,256]{1,0:T(8,128)(2,1)S(1)}, bf16[1024,256]{1,0:T(8,128)(2,1)}, u32[]{:S(2)}, u32[]{:S(2)}) collective-permute-start(bf16[1024,256]{1,0:T(8,128)(2,1)S(1)} %cell_finish.1.refs_1_.refs_2_), channel_id=1, source_target_pairs={{0,6},{1,7},{2,4},{3,5},{4,2},{5,3},{6,0},{7,1},{8,14},{9,15},{10,... | collective-permute-start | bytes 1572872 | tf_op jit(solution)/shard_map/ppermute | solution.py:35
  75.5 25.6 %collective-permute-start.15 = (bf16[128,2048]{1,0:T(8,128)(2,1)S(1)}, bf16[128,2048]{1,0:T(8,128)(2,1)S(1)}, u32[]{:S(2)}, u32[]{:S(2)}) collective-permute-start(bf16[128,2048]{1,0:T(8,128)(2,1)S(1)} %get-tuple-element.49), channel_id=1, source_target_pairs={{0,1},{1,0},{2,3},{3,2},{4,5},{5,4},{6,7},{7,6},{8,9},{9,8},{10,11... | collective-permute-start | bytes 1572872 | tf_op jit(solution)/shard_map/ppermute | solution.py:35
  75.6 7.8 %collective-permute-start.12 = (bf16[96,1024]{1,0:T(8,128)(2,1)S(1)}, bf16[96,1024]{1,0:T(8,128)(2,1)S(1)}, u32[]{:S(2)}, u32[]{:S(2)}) collective-permute-start(bf16[96,1024]{1,0:T(8,128)(2,1)S(1)} %get-tuple-element.46), channel_id=1, source_target_pairs={{0,8},{8,0},{16,24},{24,16},{1,9},{9,1},{17,25},{25,17},{2,10},{10... | collective-permute-start | bytes 589832 | tf_op jit(solution)/shard_map/ppermute | solution.py:35
  76.7 36.9 %collective-permute-start.20 = (bf16[1024,256]{1,0:T(8,128)(2,1)S(1)}, bf16[1024,256]{1,0:T(8,128)(2,1)S(1)}, u32[]{:S(2)}, u32[]{:S(2)}) collective-permute-start(bf16[1024,256]{1,0:T(8,128)(2,1)S(1)} %cell_finish.1.refs_1_.refs_2_), channel_id=1, source_target_pairs={{0,2},{1,3},{2,0},{3,1},{4,6},{5,7},{6,4},{7,5},{8,10},{9,11},{10,... | collective-permute-start | bytes 1572872 | tf_op jit(solution)/shard_map/ppermute | solution.py:35
  76.7 10.8 %collective-permute-start.13 = (bf16[96,1024]{1,0:T(8,128)(2,1)S(1)}, bf16[96,1024]{1,0:T(8,128)(2,1)S(1)}, u32[]{:S(2)}, u32[]{:S(2)}) collective-permute-start(bf16[96,1024]{1,0:T(8,128)(2,1)S(1)} %get-tuple-element.47), channel_id=1, source_target_pairs={{0,16},{8,24},{16,0},{24,8},{1,17},{9,25},{17,1},{25,9},{2,18},{10... | collective-permute-start | bytes 589832 | tf_op jit(solution)/shard_map/ppermute | solution.py:35
  78.5 9.7 %collective-permute-start.14 = (bf16[96,1024]{1,0:T(8,128)(2,1)S(1)}, bf16[96,1024]{1,0:T(8,128)(2,1)S(1)}, u32[]{:S(2)}, u32[]{:S(2)}) collective-permute-start(bf16[96,1024]{1,0:T(8,128)(2,1)S(1)} %get-tuple-element.48), channel_id=1, source_target_pairs={{0,24},{8,16},{16,8},{24,0},{1,25},{9,17},{17,9},{25,1},{2,26},{10... | collective-permute-start | bytes 589832 | tf_op jit(solution)/shard_map/ppermute | solution.py:35
  83.4 17.2 %collective-permute-start.16 = (bf16[96,1024]{1,0:T(8,128)(2,1)S(1)}, bf16[96,1024]{1,0:T(8,128)(2,1)S(1)}, u32[]{:S(2)}, u32[]{:S(2)}) collective-permute-start(bf16[96,1024]{1,0:T(8,128)(2,1)S(1)} %get-tuple-element.51), channel_id=1, source_target_pairs={{0,8},{8,0},{16,24},{24,16},{1,9},{9,1},{17,25},{25,17},{2,10},{10... | collective-permute-start | bytes 589832 | tf_op jit(solution)/shard_map/ppermute | solution.py:35
  87.5 27.7 %collective-permute-start.19 = (bf16[1024,256]{1,0:T(8,128)(2,1)S(1)}, bf16[1024,256]{1,0:T(8,128)(2,1)S(1)}, u32[]{:S(2)}, u32[]{:S(2)}) collective-permute-start(bf16[1024,256]{1,0:T(8,128)(2,1)S(1)} %cell_finish.1.refs_1_.refs_2_), channel_id=1, source_target_pairs={{0,1},{1,0},{2,3},{3,2},{4,5},{5,4},{6,7},{7,6},{8,9},{9,8},{10,11... | collective-permute-start | bytes 1572872 | tf_op jit(solution)/shard_map/ppermute | solution.py:35
  88.2 27.2 %collective-permute-start.23 = (bf16[1024,256]{1,0:T(8,128)(2,1)}, bf16[1024,256]{1,0:T(8,128)(2,1)}, u32[]{:S(2)}, u32[]{:S(2)}) collective-permute-start(bf16[1024,256]{1,0:T(8,128)(2,1)} %collective-permute-done.22.refs_8_), channel_id=1, source_target_pairs={{0,2},{1,3},{2,0},{3,1},{4,6},{5,7},{6,4},{7,5},{8,10},{9,11},{10,... | collective-permute-start | bytes 1572872 | tf_op jit(solution)/shard_map/ppermute | solution.py:35
  100.6 8.0 %collective-permute-start.17 = (bf16[96,1024]{1,0:T(8,128)(2,1)S(1)}, bf16[96,1024]{1,0:T(8,128)(2,1)S(1)}, u32[]{:S(2)}, u32[]{:S(2)}) collective-permute-start(bf16[96,1024]{1,0:T(8,128)(2,1)S(1)} %get-tuple-element.52), channel_id=1, source_target_pairs={{0,16},{8,24},{16,0},{24,8},{1,17},{9,25},{17,1},{25,9},{2,18},{10... | collective-permute-start | bytes 589832 | tf_op jit(solution)/shard_map/ppermute | solution.py:35
  101.1 11.9 %collective-permute-start.18 = (bf16[96,1024]{1,0:T(8,128)(2,1)S(1)}, bf16[96,1024]{1,0:T(8,128)(2,1)S(1)}, u32[]{:S(2)}, u32[]{:S(2)}) collective-permute-start(bf16[96,1024]{1,0:T(8,128)(2,1)S(1)} %get-tuple-element.53), channel_id=1, source_target_pairs={{0,24},{8,16},{16,8},{24,0},{1,25},{9,17},{17,9},{25,1},{2,26},{10... | collective-permute-start | bytes 589832 | tf_op jit(solution)/shard_map/ppermute | solution.py:35
  108.6 13.3 %collective-permute-start.29 = (bf16[128,512]{1,0:T(8,128)(2,1)S(1)}, bf16[128,512]{1,0:T(8,128)(2,1)S(1)}, u32[]{:S(2)}, u32[]{:S(2)}) collective-permute-start(bf16[128,512]{1,0:T(8,128)(2,1)S(1)} %get-tuple-element.50.refs_1_), channel_id=1, source_target_pairs={{0,4},{1,5},{2,6},{3,7},{4,0},{5,1},{6,2},{7,3},{8,12},{9,13},{10,... | collective-permute-start | bytes 393224 | tf_op jit(solution)/shard_map/ppermute | solution.py:35
  113.5 8.4 %collective-permute-start.28 = (bf16[128,512]{1,0:T(8,128)(2,1)S(1)}, bf16[128,512]{1,0:T(8,128)(2,1)S(1)}, u32[]{:S(2)}, u32[]{:S(2)}) collective-permute-start(bf16[128,512]{1,0:T(8,128)(2,1)S(1)} %get-tuple-element.56), channel_id=1, source_target_pairs={{0,2},{1,3},{2,0},{3,1},{4,6},{5,7},{6,4},{7,5},{8,10},{9,11},{10,... | collective-permute-start | bytes 393224 | tf_op jit(solution)/shard_map/ppermute | solution.py:35
  113.6 8.4 %collective-permute-start.30 = (bf16[128,512]{1,0:T(8,128)(2,1)}, bf16[128,512]{1,0:T(8,128)(2,1)}, u32[]{:S(2)}, u32[]{:S(2)}) collective-permute-start(bf16[128,512]{1,0:T(8,128)(2,1)} %get-tuple-element.57), channel_id=1, source_target_pairs={{0,6},{1,7},{2,4},{3,5},{4,2},{5,3},{6,0},{7,1},{8,14},{9,15},{10,... | collective-permute-start | bytes 393224 | tf_op jit(solution)/shard_map/ppermute | solution.py:35
  115.3 11.1 %collective-permute-start.25 = (bf16[1024,256]{1,0:T(8,128)(2,1)}, bf16[1024,256]{1,0:T(8,128)(2,1)S(1)}, u32[]{:S(2)}, u32[]{:S(2)}) collective-permute-start(bf16[1024,256]{1,0:T(8,128)(2,1)} %collective-permute-done.22.refs_8_), channel_id=1, source_target_pairs={{0,1},{1,0},{2,3},{3,2},{4,5},{5,4},{6,7},{7,6},{8,9},{9,8},{10,11... | collective-permute-start | bytes 1572872 | tf_op jit(solution)/shard_map/ppermute | solution.py:35
  115.4 11.0 %collective-permute-start.21 = (bf16[1024,256]{1,0:T(8,128)(2,1)S(1)}, bf16[1024,256]{1,0:T(8,128)(2,1)S(1)}, u32[]{:S(2)}, u32[]{:S(2)}) collective-permute-start(bf16[1024,256]{1,0:T(8,128)(2,1)S(1)} %collective-permute-done.20.refs_4_), channel_id=1, source_target_pairs={{0,1},{1,0},{2,3},{3,2},{4,5},{5,4},{6,7},{7,6},{8,9},{9,8},{10,11... | collective-permute-start | bytes 1572872 | tf_op jit(solution)/shard_map/ppermute | solution.py:35
  121.9 4.5 %collective-permute-start.24 = (bf16[1024,256]{1,0:T(8,128)(2,1)}, bf16[1024,256]{1,0:T(8,128)(2,1)S(1)}, u32[]{:S(2)}, u32[]{:S(2)}) collective-permute-start(bf16[1024,256]{1,0:T(8,128)(2,1)} %collective-permute-done.23.refs_6_), channel_id=1, source_target_pairs={{0,1},{1,0},{2,3},{3,2},{4,5},{5,4},{6,7},{7,6},{8,9},{9,8},{10,11... | collective-permute-start | bytes 1572872 | tf_op jit(solution)/shard_map/ppermute | solution.py:35
  121.9 14.3 %collective-permute-start.26 = (bf16[4,128,512]{2,1,0:T(8,128)(2,1)S(1)}, bf16[4,128,512]{2,1,0:T(8,128)(2,1)S(1)}, u32[]{:S(2)}, u32[]{:S(2)}) collective-permute-start(bf16[4,128,512]{2,1,0:T(8,128)(2,1)S(1)} %get-tuple-element.59), channel_id=1, source_target_pairs={{0,8},{8,0},{16,24},{24,16},{1,9},{9,1},{17,25},{25,17},{2,10},{10... | collective-permute-start | bytes 1572872 | tf_op jit(solution)/shard_map/ppermute | solution.py:35
  122.0 15.1 %collective-permute-start.27 = (bf16[4,128,512]{2,1,0:T(8,128)(2,1)S(1)}, bf16[4,128,512]{2,1,0:T(8,128)(2,1)S(1)}, u32[]{:S(2)}, u32[]{:S(2)}) collective-permute-start(bf16[4,128,512]{2,1,0:T(8,128)(2,1)S(1)} %get-tuple-element.58), channel_id=1, source_target_pairs={{0,16},{8,24},{16,0},{24,8},{1,17},{9,25},{17,1},{25,9},{2,18},{10... | collective-permute-start | bytes 1572872 | tf_op jit(solution)/shard_map/ppermute | solution.py:35
